TPU v7x, 512 devices: a whole 4x4x16 slice. The times are simulated.
512 devices in a mesh: sp: 16 (over z), fs: 4 (over y), tp: 8 (over x, core).
Axes of the slice: x: 4, y: 4, z: 16, core: 2. Of those that a mesh axis runs over, the one named last changes fastest.
Arguments:
- tokens: bfloat16 [4, 4096, 2048], P('fs', 'sp'), may hold values from -6 to 6
- norm_gain: float32 [2048], replicated, may hold values from 0.1 to 1.9
- w_state_in: bfloat16 [2048, 1024], P(('sp', 'fs'), 'tp'), may hold values from -0.125 to 0.125
- w_value: bfloat16 [2048, 1024], P(('sp', 'fs'), 'tp'), may hold values from -0.125 to 0.125
- w_outer: bfloat16 [2048, 1024], P(('sp', 'fs'), 'tp'), may hold values from -0.125 to 0.125
- w_inner: bfloat16 [2048, 1024], P(('sp', 'fs'), 'tp'), may hold values from -0.125 to 0.125
- w_state_out: bfloat16 [2048, 1024], P(('sp', 'fs'), 'tp'), may hold values from -0.125 to 0.125
- w_conv_out: bfloat16 [2048, 1024], P(('sp', 'fs'), 'tp'), may hold values from -0.125 to 0.125
- log_step: float32 [64], P('tp'), may hold values from -4.6 to -3.2
- decay_real: float32 [64, 64], P('tp'), may hold values from -5 to 0
- frequency: float32 [64, 64], P('tp'), may hold values from 1 to 192
- step_rate: float32 [4, 4096], P('fs', 'sp'), may hold values from 0.4 to 2.5
- input_real: float32 [64, 64, 16], P('tp'), may hold values from -1 to 1
- input_imag: float32 [64, 64, 16], P('tp'), may hold values from -1 to 1
- read_real: float32 [64, 16, 64], P('tp'), may hold values from -0.75 to 0.75
- read_imag: float32 [64, 16, 64], P('tp'), may hold values from -0.75 to 0.75
- skip_gain: float32 [64, 16], P('tp'), may hold values from -4 to 4
- conv_taps: float32 [3, 1024], P(None, 'tp'), may hold values from -3.5 to 3.5
- initial_state: float32 [4, 2, 64, 64], P('fs', None, 'tp'), may hold values from -6 to 6
Outputs:
- mixed: bfloat16 [4, 4096, 2048], P('fs', ('sp', 'tp'))
- final_state: float32 [4, 2, 64, 64], P('fs', None, 'tp', 'sp')
All inputs are finite; a program needn't handle non-finite values.
Results may differ from a plain program's by a relative error of at most 0.018.
Values may be sent and summed in bfloat16 or wider, within the bound.
No kernel may reach another device: no remote copies, remote signals or barrier semaphores. Data moves between devices by JAX's collectives and lax.ppermute only.
A program may use at most 64 MiB of HBM per device.

v0:
```python
import jax
import jax.numpy as jnp
from jax import lax
from jax.sharding import PartitionSpec as P

HIGHEST = lax.Precision.HIGHEST


def in_one_piece(arrays, axis, dim, along):
    ends, at = ([], 0)
    for a in arrays[:-1]:
        at += a.shape[along]
        ends.append(at)
    both = jnp.concatenate(arrays, axis=along)
    return tuple(jnp.split(lax.all_gather(both, axis, axis=dim, tiled=True), ends, axis=along))


def laid_out(parts, dim):
    parts = jnp.moveaxis(parts, 0, dim)
    dims = parts.shape
    return parts.reshape(*dims[:dim], dims[dim] * dims[dim + 1], *dims[dim + 2 :])


def gather_together(arrays, axis, dims):
    ravelled = jnp.concatenate([a.reshape(-1) for a in arrays])
    lines, at, done = (lax.all_gather(ravelled, axis), 0, [])
    for a, dim in zip(arrays, dims):
        parts = lines[:, at : at + a.size].reshape(-1, *a.shape)
        done.append(laid_out(parts, dim))
        at += a.size
    return tuple(done)


def shifted(value, axis, steps):
    count = lax.axis_size(axis)
    initial, last = (max(0, -steps), min(count, count - steps))
    return lax.ppermute(value, axis, [(source, source + steps) for source in range(initial, last)])


def in_blocks(x, dim, length):
    before, after = (x.shape[:dim], x.shape[dim + 1 :])
    return jnp.moveaxis(x.reshape(*before, length, -1, *after), dim, 0)


def summed_on_arrival(x, axis, dim):
    length = lax.axis_size(axis)
    parts = lax.all_to_all(in_blocks(x, dim, length), axis, 0, 0, tiled=True)
    return jnp.sum(parts.astype(jnp.float32), axis=0)


def complex_product(left_real, left_imag, right_real, right_imag):
    return (
        left_real * right_real - left_imag * right_imag,
        left_real * right_imag + left_imag * right_real,
    )


def chain_pair(earlier, later):
    first_real, first_imag = complex_product(later[0], later[1], earlier[0], earlier[1])
    carry_real, carry_imag = complex_product(later[0], later[1], earlier[2], earlier[3])
    return (first_real, first_imag, carry_real + later[2], carry_imag + later[3])


def apply_map(summary, start_real, start_imag):
    moved_real, moved_imag = complex_product(summary[0], summary[1], start_real, start_imag)
    return (moved_real + summary[2], moved_imag + summary[3])


def body(
    tokens,
    norm_gain,
    w_state_in,
    w_value,
    w_outer,
    w_inner,
    w_state_out,
    w_conv_out,
    log_step,
    decay_real,
    frequency,
    step_rate,
    input_real,
    input_imag,
    read_real,
    read_imag,
    skip_gain,
    conv_taps,
    initial_state,
):
    rows = tokens.shape[1]
    features = tokens[0].astype(jnp.float32)
    mean_square = jnp.mean(features * features, axis=-1, keepdims=True)
    normed = (features * lax.rsqrt(mean_square + 1e-06) * norm_gain).astype(jnp.bfloat16)
    weights = in_one_piece(
        (w_state_in, w_value, w_outer, w_inner, w_state_out, w_conv_out), ("sp", "fs"), 0, 1
    )

    def project(matrix):
        return jnp.dot(normed, matrix, preferred_element_type=jnp.float32).astype(jnp.bfloat16)

    state_in = project(weights[0])
    value = project(weights[1])
    outer = project(weights[2])
    inner = project(weights[3])
    groups, states = decay_real.shape
    group = skip_gain.shape[1]
    flat = groups * states
    decay = decay_real.reshape(flat)
    turn_rate = frequency.reshape(flat)
    step = jnp.exp(log_step)[None, :] * step_rate[0][:, None]
    step_flat = jnp.repeat(step, states, axis=1)
    grow = jnp.exp(step_flat * decay)
    angle = step_flat * turn_rate
    bar_real = grow * jnp.cos(angle)
    bar_imag = grow * jnp.sin(angle)
    modulus = decay * decay + turn_rate * turn_rate
    less_real = bar_real - 1.0
    hold_real = (less_real * decay + bar_imag * turn_rate) / modulus
    hold_imag = (bar_imag * decay - less_real * turn_rate) / modulus
    channels = state_in.astype(jnp.float32).reshape(rows, groups, group)
    coupling = jnp.concatenate([input_real, input_imag], axis=1)
    driven = jnp.einsum("tgh,gqh->tgq", channels, coupling, precision=HIGHEST)
    drive_real = driven[:, :, :states].reshape(rows, flat)
    drive_imag = driven[:, :, states:].reshape(rows, flat)
    push_real, push_imag = complex_product(hold_real, hold_imag, drive_real, drive_imag)
    span = 16
    blocks = rows // span
    lower = (
        lax.broadcasted_iota(jnp.int32, (span, span), 0)
        >= lax.broadcasted_iota(jnp.int32, (span, span), 1)
    ).astype(jnp.float32)
    elapsed = jnp.einsum(
        "ts,bsf->btf", lower, step_flat.reshape(blocks, span, flat), precision=HIGHEST
    )
    rise = jnp.exp(decay * elapsed)
    phase = turn_rate * elapsed
    carry_real = rise * jnp.cos(phase)
    carry_imag = rise * jnp.sin(phase)
    fall = jnp.exp(-decay * elapsed)
    undo_real, undo_imag = complex_product(
        fall * jnp.cos(phase),
        -fall * jnp.sin(phase),
        push_real.reshape(blocks, span, flat),
        push_imag.reshape(blocks, span, flat),
    )
    summed = jnp.einsum(
        "ts,cbsf->cbtf", lower, jnp.stack([undo_real, undo_imag]), precision=HIGHEST
    )
    local_real, local_imag = complex_product(carry_real, carry_imag, summed[0], summed[1])
    ends = (carry_real[:, -1], carry_imag[:, -1], local_real[:, -1], local_imag[:, -1])
    inclusive = lax.associative_scan(chain_pair, ends, axis=0)
    unit_row = jnp.ones((1, flat), jnp.float32)
    empty_row = jnp.zeros((1, flat), jnp.float32)
    before = (
        jnp.concatenate([unit_row, inclusive[0][:-1]], axis=0),
        jnp.concatenate([empty_row, inclusive[1][:-1]], axis=0),
        jnp.concatenate([empty_row, inclusive[2][:-1]], axis=0),
        jnp.concatenate([empty_row, inclusive[3][:-1]], axis=0),
    )
    summary = (inclusive[0][-1], inclusive[1][-1], inclusive[2][-1], inclusive[3][-1])
    opening_state = initial_state[0].reshape(2, flat)
    every = gather_together(
        (summary[0][None], summary[1][None], summary[2][None], summary[3][None]), "sp", (0, 0, 0, 0)
    )
    running = lax.associative_scan(chain_pair, every, axis=0)
    position = lax.axis_index("sp")
    earlier = jnp.maximum(position - 1, 0)
    picked = [lax.dynamic_index_in_dim(piece, earlier, 0, keepdims=False) for piece in running]
    opening = position == 0
    prefix = (
        jnp.where(opening, 1.0, picked[0]),
        jnp.where(opening, 0.0, picked[1]),
        jnp.where(opening, 0.0, picked[2]),
        jnp.where(opening, 0.0, picked[3]),
    )
    enter_real, enter_imag = apply_map(prefix, opening_state[0], opening_state[1])
    total_map = (running[0][-1], running[1][-1], running[2][-1], running[3][-1])
    closing_real, closing_imag = apply_map(total_map, opening_state[0], opening_state[1])
    closing = jnp.stack([closing_real, closing_imag])
    block_real, block_imag = apply_map(before, enter_real[None], enter_imag[None])
    shift_real, shift_imag = complex_product(
        carry_real, carry_imag, block_real[:, None], block_imag[:, None]
    )
    hidden_real = (local_real + shift_real).reshape(rows, groups, states)
    hidden_imag = (local_imag + shift_imag).reshape(rows, groups, states)
    reading = jnp.concatenate([read_real, -read_imag], axis=2)
    joined = jnp.concatenate([hidden_real, hidden_imag], axis=2)
    response = jnp.einsum("tgq,ghq->tgh", joined, reading, precision=HIGHEST) + skip_gain * channels
    state_mix = jax.nn.gelu(response).reshape(rows, groups * group).astype(jnp.bfloat16)
    gated = (inner.astype(jnp.float32) * value.astype(jnp.float32)).astype(jnp.bfloat16)
    reach = conv_taps.shape[0] - 1
    earlier_rows = shifted(gated[rows - reach :], "sp", 1)
    extended = jnp.concatenate([earlier_rows, gated], axis=0).astype(jnp.float32)
    filtered = conv_taps[0] * extended[0:rows]
    for tap in range(1, reach + 1):
        filtered = filtered + conv_taps[tap] * extended[tap : tap + rows]
    conv_mix = (outer.astype(jnp.float32) * filtered).astype(jnp.bfloat16)
    mixed = summed_on_arrival(
        (
            jnp.einsum("rc,dc->rd", state_mix, weights[4], preferred_element_type=jnp.float32)
            + jnp.einsum("rc,dc->rd", conv_mix, weights[5], preferred_element_type=jnp.float32)
        ).astype(jnp.bfloat16),
        "tp",
        0,
    ).astype(jnp.bfloat16)
    share = states // lax.axis_size("sp")
    closing_grid = closing.reshape(2, groups, states)
    own_share = lax.dynamic_slice_in_dim(closing_grid, lax.axis_index("sp") * share, share, 2)
    return (mixed[None], own_share[None])


def solution(mesh):
    return jax.shard_map(
        body,
        mesh=mesh,
        in_specs=(
            P("fs", "sp", None),
            P(),
            P(("sp", "fs"), "tp"),
            P(("sp", "fs"), "tp"),
            P(("sp", "fs"), "tp"),
            P(("sp", "fs"), "tp"),
            P(("sp", "fs"), "tp"),
            P(("sp", "fs"), "tp"),
            P("tp"),
            P("tp", None),
            P("tp", None),
            P("fs", "sp"),
            P("tp", None, None),
            P("tp", None, None),
            P("tp", None, None),
            P("tp", None, None),
            P("tp", None),
            P(None, "tp"),
            P("fs", None, "tp", None),
        ),
        out_specs=(P("fs", ("sp", "tp"), None), P("fs", None, "tp", "sp")),
        check_vma=False,
    )
```

profile of v0, /device:TPU:1, one launch (start us, length us, event | category | flops | bytes accessed | tf_op | source)
XLA Modules:
  0.0 255.2 jit_solution(16286001688518768119)
XLA Ops:
  7.3 0.8 constant_dynamic-update-slice_fusion.5
  8.0 0.7 constant_dynamic-update-slice_fusion.4
  8.8 0.7 constant_dynamic-update-slice_fusion.3
  9.5 0.7 constant_dynamic-update-slice_fusion.2
  10.2 0.7 constant_dynamic-update-slice_fusion.1
  10.9 0.7 constant_dynamic-update-slice_fusion
  12.9 0.8 broadcast_multiply_fusion.1
  15.4 2.9 %sine_bitcast_fusion = (f32[16,16,512]{2,0,1:T(8,128)S(1)}, f32[16,512,16]{1,0,2:T(8,128)}, f32[16,16,512]{2,0,1:T(8,128)S(1)}) fusion(f32[16,512,16]{1,2,0:T(8,128)S(1)} %fusion.59, f32[512]{0:T(512)S(1)} %mul.696, f32[512]{0:T(512)S(1)} %mul.689), kind=kLoop, calls=%fused_computation.50 | loop fusion | flops 262144 | bytes 2101248 | tf_op jit(solution)/shard_map/sin | solution.py:142
  18.3 133.8 %all-gather.3.cloned.1.call-done = bf16[2048,768]{1,0:T(8,128)(2,1)} async-done(((bf16[32,768]{1,0:T(8,128)(2,1)}), bf16[2048,768]{1,0:T(8,128)(2,1)}) %all-gather.3.cloned.1.call-update) | async-done | bytes 3145744 | tf_op jit(solution)/shard_map/all_gather | solution.py:15
  152.1 1.9 convolution_convert_fusion.3
  154.1 0.7 convolution_bitcast_fusion
  154.9 1.3 copy.62
  156.3 1.5 reshape.174
  157.8 1.3 copy.63
  159.1 2.3 reshape.175
  161.4 4.1 %subtract_bitcast_fusion = (f32[1,16,16,512]{3,2,1,0:T(8,128)S(1)}, f32[1,16,16,512]{3,2,1,0:T(8,128)S(1)}, f32[16,16,512]{2,1,0:T(8,128)S(1)}) fusion(f32[16,512,16]{1,0,2:T(8,128)} %get-tuple-element.14, f32[16,512,16]{1,2,0:T(8,128)S(1)} %fusion.59, f32[512]{0:T(512)S(1)} %get-tuple-element.118, f32[16,16,512]{2,0,1:T(8,128)S(1)} %get-tuple-element.13, ...), kind=kLoop, calls=%fused_computation.48 | loop fusion | flops 3932160 | bytes 5251072 | tf_op jit(solution)/shard_map/stack | solution.py:147
  166.8 1.4 multiply_subtract_fusion
  169.0 0.8 slice_bitcast_fusion.4
  171.4 21.3 %all-gather = f32[32768]{0:T(1024)S(1)} all-gather(f32[2048]{0:T(1024)S(1)} %pad_maximum_fusion.12), channel_id=2, replica_groups=mesh['sp'=16,'fs'=4,'tp'=8] {'sp'}, dimensions={0}, use_global_device_ids=true | all-gather | bytes 139264 | tf_op jit(solution)/shard_map/all_gather | solution.py:26
  194.8 1.2 subtract_add_fusion
  197.6 1.2 fusion.28
  198.8 1.3 reshape.177
  200.4 1.6 fusion.8
  202.0 1.5 fusion.7
  203.6 1.9 collective-permute-start
  205.5 1.2 fusion.41
  206.7 1.5 fusion.24
  208.2 3.0 %fusion = bf16[256,2048]{1,0:T(8,128)(2,1)} fusion(f32[256,2048]{1,0:T(8,128)S(1)} %fusion.24, bf16[2048,768]{1,0:T(8,128)(2,1)} %all-gather.3.cloned.1.call-done, f32[258,128]{1,0:T(8,128)S(1)} %maximum_convert_fusion, f32[128]{0:T(128)S(1)} %get-tuple-element.115, f32[128]{0:T(128)S(1)} %get-tuple-element.116, f32[128]{0:T(128)S(1)} %get-tuple-element.114, ...), kind=kOutput, calls=%fused_computation.3 | convolution fusion | flops 271876096 | bytes 5646848 | tf_op jit(solution)/shard_map/rc,dc->rd/dot_general | solution.py:201
  211.3 21.2 %all-to-all-start = ((bf16[8,32,2048]{2,1,0:T(8,128)(2,1)}), bf16[8,32,2048]{2,1,0:T(8,128)(2,1)S(1)}, u32[]{:S(2)}, u32[]{:S(2)}) async-start(bf16[8,32,2048]{2,1,0:T(8,128)(2,1)} %bitcast.114), calls=%async_computation | async-start | bytes 2097152 | tf_op jit(solution)/shard_map/all_to_all | solution.py:47
  232.8 0.7 copy.77
  233.4 14.1 %all-to-all-done = bf16[8,32,2048]{2,1,0:T(8,128)(2,1)S(1)} async-done(((bf16[8,32,2048]{2,1,0:T(8,128)(2,1)}), bf16[8,32,2048]{2,1,0:T(8,128)(2,1)S(1)}, u32[]{:S(2)}, u32[]{:S(2)}) %all-to-all-start) | async-done | bytes 1048608 | tf_op jit(solution)/shard_map/all_to_all | solution.py:47
  247.5 0.8 reduce_sum.22
  (285 shorter events, 10.0 us)
Async XLA Ops:
  7.2 7.1 %copy-start.13 = (f32[8,64]{1,0:T(8,128)S(1)}, f32[8,64]{1,0:T(8,128)}, u32[]{:S(2)}) copy-start(f32[8,64]{1,0:T(8,128)} %param.28) | copy-start | bytes 6148
  7.2 7.2 %copy-start.14 = (f32[8,64]{1,0:T(8,128)S(1)}, f32[8,64]{1,0:T(8,128)}, u32[]{:S(2)}) copy-start(f32[8,64]{1,0:T(8,128)} %param.29) | copy-start | bytes 6148
  7.2 7.3 %copy-start.11 = (f32[1,2,8,64]{3,2,1,0:T(8,128)S(1)}, f32[1,2,8,64]{3,2,1,0:T(8,128)}, u32[]{:S(2)}) copy-start(f32[1,2,8,64]{3,2,1,0:T(8,128)} %param.37) | copy-start | bytes 12292
  7.2 7.4 %copy-start.9 = (f32[8,16,64]{2,1,0:T(8,128)S(1)}, f32[8,16,64]{2,1,0:T(8,128)}, u32[]{:S(2)}) copy-start(f32[8,16,64]{2,1,0:T(8,128)} %param.34) | copy-start | bytes 98308
  7.2 7.4 %copy-start = (bf16[1,256,2048]{2,1,0:T(8,128)(2,1)S(1)}, bf16[1,256,2048]{2,1,0:T(8,128)(2,1)}, u32[]{:S(2)}) copy-start(bf16[1,256,2048]{2,1,0:T(8,128)(2,1)} %param.19) | copy-start | bytes 3145732
  7.2 144.9 %all-gather.3.cloned.1.call-start = ((), (), s32[]{:S(2)}) async-start(), calls=%async_computation.1 | async-start | bytes 3194880 | tf_op jit(solution)/shard_map/all_gather | solution.py:15
  10.9 4.1 %copy-start.15 = (f32[3,128]{1,0:T(4,128)S(1)}, f32[3,128]{1,0:T(4,128)}, u32[]{:S(2)}) copy-start(f32[3,128]{1,0:T(4,128)} %param.36) | copy-start | bytes 4612
  11.6 0.6 copy-start.5
  14.6 137.5 %copy-start.10 = (f32[2048]{0:T(1024)S(1)}, f32[2048]{0:T(1024)}, u32[]{:S(2)}) copy-start(f32[2048]{0:T(1024)} %param.20) | copy-start | bytes 24580
  15.4 138.7 %copy-start.6 = (f32[8,64,16]{1,2,0:T(8,128)S(1)}, f32[8,64,16]{1,2,0:T(8,128)}, u32[]{:S(2)}) copy-start(f32[8,64,16]{1,2,0:T(8,128)} %param.32) | copy-start | bytes 98308
  15.4 138.7 %copy-start.7 = (f32[8,64,16]{1,2,0:T(8,128)S(1)}, f32[8,64,16]{1,2,0:T(8,128)}, u32[]{:S(2)}) copy-start(f32[8,64,16]{1,2,0:T(8,128)} %param.31) | copy-start | bytes 98308
  168.8 24.1 %copy-start.2 = (f32[16,16,512]{2,1,0:T(8,128)}, f32[16,16,512]{2,1,0:T(8,128)S(1)}, u32[]{:S(2)}) copy-start(f32[16,16,512]{2,1,0:T(8,128)S(1)} %copy_add_fusion.1) | copy-start | bytes 1572868
  196.3 1.0 copy-start.3
  196.6 1.1 copy-start.4
  198.8 1.6 copy-start.1
  200.4 5.1 %copy-start.8 = (f32[8,16,64]{2,1,0:T(8,128)S(1)}, f32[8,16,64]{2,1,0:T(8,128)}, u32[]{:S(2)}) copy-start(f32[8,16,64]{2,1,0:T(8,128)} %param.33) | copy-start | bytes 98308
  200.4 5.1 %copy-start.12 = (f32[8,16]{1,0:T(8,128)S(1)}, f32[8,16]{1,0:T(8,128)}, u32[]{:S(2)}) copy-start(f32[8,16]{1,0:T(8,128)} %param.35) | copy-start | bytes 1540
  203.6 4.7 %collective-permute-start = (bf16[2,128]{1,0:T(2,128)(2,1)S(1)}, bf16[2,128]{1,0:T(2,128)(2,1)S(1)}, u32[]{:S(2)}, u32[]{:S(2)}) collective-permute-start(bf16[2,128]{1,0:T(2,128)(2,1)S(1)} %slice.852), channel_id=1, source_target_pairs={{0,32},{32,64},{64,96},{96,128},{128,160},{160,192},{192,224},{224... | collective-permute-start | bytes 1544 | tf_op jit(solution)/shard_map/ppermute | solution.py:37
  211.3 36.2 %all-to-all-start = ((bf16[8,32,2048]{2,1,0:T(8,128)(2,1)}), bf16[8,32,2048]{2,1,0:T(8,128)(2,1)S(1)}, u32[]{:S(2)}, u32[]{:S(2)}) async-start(bf16[8,32,2048]{2,1,0:T(8,128)(2,1)} %bitcast.114), calls=%async_computation | async-start | bytes 2097152 | tf_op jit(solution)/shard_map/all_to_all | solution.py:47
Sparse Core Ops, SparseCore 0:
  12.4 139.7 all-gather.2
where the time goes:
time: 256 us; the launch traced here: 255 us
  waiting for transfers between devices  148 us (58%)
  starting transfers between devices  23.2 us (9%)
  blocking collectives  21.3 us (8%)
  local copies, waits for them, and re-layouts  20.6 us (8%)
  between operations  15.4 us (6%)
  other arithmetic  14.3 us (6%)
  matrix products  12.5 us (5%)
    all_gather x1, waiting for transfers between devices, in_one_piece(): lax.all_gather(both, axis, axis=dim, tiled=True)  134 us
    all_gather x1, blocking collectives, gather_together(): lines, at, done = (lax.all_gather(ravelled, axis), 0, [])  21.3 us
    all_to_all x1, starting transfers between devices, summed_on_arrival(): parts = lax.all_to_all(in_blocks(x, dim, length), axis, 0, 0, tiled=True)  21.2 us
    all_to_all x1, waiting for transfers between devices, summed_on_arrival(): parts = lax.all_to_all(in_blocks(x, dim, length), axis, 0, 0, tiled=True)  14.1 us
    unnamed x45, local copies, waits for them, and re-layouts  5.2 us
  transfers between devices with their start and end apart: 3, of which 2 were waited for; matrix products, arithmetic and copies ran while one was open for 4% of the time, Pallas kernels for 0%

commit v1 on v0

v1 whole, which is shorter than its diff:
```python
import functools

import jax
import jax.numpy as jnp
from jax import lax
from jax.experimental import pallas as pl
from jax.experimental.pallas import tpu as pltpu
from jax.sharding import PartitionSpec as P

F32 = jnp.float32
BF16 = jnp.bfloat16
CHUNKS = 8
HALO = 16


def replicated(x, copies):
    return jnp.broadcast_to(x[None], (copies, *x.shape))


def spread(x, axis):
    copies = lax.axis_size(axis)
    return lax.all_to_all(replicated(x, copies), axis, 0, 0, tiled=True)


def complex_product(left_real, left_imag, right_real, right_imag):
    return (
        left_real * right_real - left_imag * right_imag,
        left_real * right_imag + left_imag * right_real,
    )


def sine_cosine(angle):
    turns = jnp.floor(angle * 0.6366197723675814 + 0.5)
    r = angle - turns * 1.5703125
    r = r - turns * 4.837512969970703e-4
    r = r - turns * 7.549789948768648e-8
    r2 = r * r
    sine = r + r * r2 * (-1.6666654611e-1 + r2 * (8.3321608736e-3 + r2 * -1.9515295891e-4))
    cosine = (
        1.0
        - 0.5 * r2
        + r2 * r2 * (4.166664568298827e-2 + r2 * (-1.388731625493765e-3 + r2 * 2.443315711809948e-5))
    )
    quadrant = turns.astype(jnp.int32)
    odd = (quadrant & 1) == 1
    flip_sine = (quadrant & 2) == 2
    flip_cosine = ((quadrant + 1) & 2) == 2
    base_sine = jnp.where(odd, cosine, sine)
    base_cosine = jnp.where(odd, sine, cosine)
    return (
        jnp.where(flip_sine, -base_sine, base_sine),
        jnp.where(flip_cosine, -base_cosine, base_cosine),
    )


def normed_kernel(x_ref, gain_ref, out_ref):
    x = x_ref[...].astype(F32)
    mean_square = jnp.mean(x * x, axis=-1, keepdims=True)
    out_ref[...] = (x * lax.rsqrt(mean_square + 1e-06) * gain_ref[...]).astype(BF16)


def maps_kernel(rate_ref, scale_ref, decay_ref, freq_ref, bar_ref, hold_ref, cum_ref, total_ref):
    flat = decay_ref.shape[1]
    decay, freq, scale = (decay_ref[...], freq_ref[...], jnp.exp(scale_ref[...]))
    inverse = 1.0 / (decay * decay + freq * freq)
    steps = rate_ref.shape[0] // CHUNKS

    def advance(j, carry):
        cum_real, cum_imag = carry
        rows = pl.ds(pl.multiple_of(j * CHUNKS, CHUNKS), CHUNKS)
        step = rate_ref[rows, :] * scale
        grow = jnp.exp(step * decay)
        sine, cosine = sine_cosine(step * freq)
        bar_real, bar_imag = (grow * cosine, grow * sine)
        less_real = bar_real - 1.0
        bar_ref[0, rows, :] = bar_real
        bar_ref[1, rows, :] = bar_imag
        hold_ref[0, rows, :] = (less_real * decay + bar_imag * freq) * inverse
        hold_ref[1, rows, :] = (bar_imag * decay - less_real * freq) * inverse
        cum_real, cum_imag = complex_product(cum_real, cum_imag, bar_real, bar_imag)
        cum_ref[0, rows, :] = cum_real
        cum_ref[1, rows, :] = cum_imag
        return (cum_real, cum_imag)

    one = jnp.ones((CHUNKS, flat), F32)
    end_real, end_imag = lax.fori_loop(0, steps, advance, (one, jnp.zeros_like(one)))
    real, imag = (end_real[0:1], end_imag[0:1])
    for c in range(1, CHUNKS):
        real, imag = complex_product(real, imag, end_real[c : c + 1], end_imag[c : c + 1])
    total_ref[...] = jnp.concatenate([real, imag], axis=0)


def local_kernel(normed_ref, w_ref, perm_ref, couple_ref, bar_ref, hold_ref, cum_ref, chan_ref, local_ref, end_ref, push_ref):
    fs, sp = w_ref.shape[:2]
    w = jnp.concatenate([w_ref[f, z] for z in range(sp) for f in range(fs)], axis=0)
    state_in = jnp.dot(normed_ref[...], w, preferred_element_type=F32).astype(BF16)
    chan = jnp.dot(perm_ref[...], state_in, preferred_element_type=F32).astype(BF16)
    chan_ref[...] = chan
    flat = bar_ref.shape[2]
    drive = jnp.dot(chan, couple_ref[0], preferred_element_type=F32) + jnp.dot(
        chan, couple_ref[1], preferred_element_type=F32
    )
    push_real, push_imag = complex_product(hold_ref[0], hold_ref[1], drive[:, :flat], drive[:, flat:])
    push_ref[0] = push_real
    push_ref[1] = push_imag
    steps = bar_ref.shape[1] // CHUNKS

    def advance(j, carry):
        rows = pl.ds(pl.multiple_of(j * CHUNKS, CHUNKS), CHUNKS)
        real, imag = complex_product(bar_ref[0, rows, :], bar_ref[1, rows, :], carry[0], carry[1])
        real = real + push_ref[0, rows, :]
        imag = imag + push_ref[1, rows, :]
        local_ref[0, rows, :] = real
        local_ref[1, rows, :] = imag
        return (real, imag)

    zero = jnp.zeros((CHUNKS, flat), F32)
    last_real, last_imag = lax.fori_loop(0, steps, advance, (zero, zero), unroll=4)
    tail = pl.ds((steps - 1) * CHUNKS, CHUNKS)
    end_real, end_imag = (cum_ref[0, tail, :], cum_ref[1, tail, :])
    real, imag = (last_real[0:1], last_imag[0:1])
    for c in range(1, CHUNKS):
        moved_real, moved_imag = complex_product(end_real[c : c + 1], end_imag[c : c + 1], real, imag)
        real = moved_real + last_real[c : c + 1]
        imag = moved_imag + last_imag[c : c + 1]
    end_ref[...] = jnp.concatenate([real, imag], axis=0)


def gelu(v):
    return 0.5 * v * (1.0 + jnp.tanh(0.7978845608 * (v + 0.044715 * v * v * v)))


def halves(x):
    high = x.astype(BF16)
    return high, (x - high.astype(F32)).astype(BF16)


def read_kernel(
    where_ref, maps_ref, ends_ref, initial_ref, local_ref, cum_ref, chan_ref, perm_ref, read_ref, skip_ref, mix_ref, closing_ref
):
    spans = maps_ref.shape[0]
    here = where_ref[0]
    real, imag = (initial_ref[0:1], initial_ref[1:2])
    enter_real, enter_imag = (real, imag)
    for z in range(spans):
        now = here == z
        enter_real = jnp.where(now, real, enter_real)
        enter_imag = jnp.where(now, imag, enter_imag)
        moved_real, moved_imag = complex_product(maps_ref[z, 0:1], maps_ref[z, 1:2], real, imag)
        real = moved_real + ends_ref[z, 0:1]
        imag = moved_imag + ends_ref[z, 1:2]
    closing_ref[...] = jnp.concatenate([real, imag], axis=0)
    rows = local_ref.shape[1]
    flat = local_ref.shape[2]
    steps = rows // CHUNKS
    tail = pl.ds((steps - 1) * CHUNKS, CHUNKS)
    end_real, end_imag = (cum_ref[0, tail, :], cum_ref[1, tail, :])
    last_real, last_imag = (local_ref[0, tail, :], local_ref[1, tail, :])
    in_real, in_imag = ([enter_real], [enter_imag])
    for c in range(CHUNKS - 1):
        moved_real, moved_imag = complex_product(
            end_real[c : c + 1], end_imag[c : c + 1], in_real[-1], in_imag[-1]
        )
        in_real.append(moved_real + last_real[c : c + 1])
        in_imag.append(moved_imag + last_imag[c : c + 1])
    entry_real = jnp.concatenate(in_real, axis=0)[None]
    entry_imag = jnp.concatenate(in_imag, axis=0)[None]
    shape = (steps, CHUNKS, flat)
    moved_real, moved_imag = complex_product(
        cum_ref[0].reshape(shape), cum_ref[1].reshape(shape), entry_real, entry_imag
    )
    hidden_real = local_ref[0] + moved_real.reshape(rows, flat)
    hidden_imag = local_ref[1] + moved_imag.reshape(rows, flat)

    def contract(x, at):
        high, low = halves(x)
        first = jnp.dot(high, read_ref[0, at], preferred_element_type=F32)
        second = jnp.dot(low, read_ref[0, at], preferred_element_type=F32)
        return first + (second + jnp.dot(high, read_ref[1, at], preferred_element_type=F32))

    response = contract(hidden_real, 0) + contract(hidden_imag, 1)
    response = response + skip_ref[...] * chan_ref[...].astype(F32)
    mixed = gelu(response).astype(BF16)
    mix_ref[...] = jnp.dot(perm_ref[...], mixed, preferred_element_type=F32).astype(BF16)


def conv_kernel(normed_ref, halo_ref, w_ref, taps_ref, mix_ref):
    fs, sp = w_ref.shape[:2]
    width = taps_ref.shape[1]
    rows = normed_ref.shape[0]
    w = jnp.concatenate([w_ref[f, z] for z in range(sp) for f in range(fs)], axis=0)
    reach = taps_ref.shape[0] - 1
    here = jnp.dot(normed_ref[...], w, preferred_element_type=F32).astype(BF16).astype(F32)
    before = jnp.dot(halo_ref[...], w[:, : 2 * width], preferred_element_type=F32).astype(BF16).astype(F32)
    gated = (here[:, :width] * here[:, width : 2 * width]).astype(BF16).astype(F32)
    gated_before = (before[:, :width] * before[:, width:]).astype(BF16).astype(F32)
    extended = jnp.concatenate([gated_before, gated], axis=0)
    filtered = taps_ref[reach : reach + 1] * gated
    for tap in range(reach):
        at = HALO - reach + tap
        filtered = filtered + taps_ref[tap : tap + 1] * extended[at : at + rows]
    mix_ref[...] = (here[:, 2 * width :] * filtered).astype(BF16)


def call(kernel, out_shape, flops, *args, scratch=(), smem=0, name=None):
    in_specs = [pl.BlockSpec(memory_space=pltpu.SMEM)] * smem + [
        pl.BlockSpec(memory_space=pltpu.VMEM)
    ] * (len(args) - smem)
    out_specs = jax.tree.map(lambda _: pl.BlockSpec(memory_space=pltpu.VMEM), out_shape)
    return pl.pallas_call(
        kernel,
        out_shape=out_shape,
        in_specs=in_specs,
        out_specs=out_specs,
        scratch_shapes=list(scratch),
        cost_estimate=pl.CostEstimate(flops=flops, bytes_accessed=1 << 20, transcendentals=0),
        name=name,
    )(*args)


def shape(dims, dtype=F32):
    return jax.ShapeDtypeStruct(dims, dtype)


def block_diagonal(blocks):
    groups, rows, columns = blocks.shape
    eye = jnp.eye(groups, dtype=bool)[:, None, :, None]
    return jnp.where(eye, blocks[:, :, None, :], 0.0).reshape(groups * rows, groups * columns)


def body(
    tokens,
    norm_gain,
    w_state_in,
    w_value,
    w_outer,
    w_inner,
    w_state_out,
    w_conv_out,
    log_step,
    decay_real,
    frequency,
    step_rate,
    input_real,
    input_imag,
    read_real,
    read_imag,
    skip_gain,
    conv_taps,
    initial_state,
):
    rows, features = tokens.shape[1:]
    groups, states = decay_real.shape
    group = skip_gain.shape[1]
    flat = groups * states
    width = groups * group
    steps = rows // CHUNKS

    state_shards = spread(w_state_in, "sp")
    conv_shards = spread(jnp.concatenate([w_value, w_inner, w_outer], axis=1), "sp")
    out_shards = spread(jnp.concatenate([w_state_out, w_conv_out], axis=1), "sp")

    count = lax.axis_size("sp")
    edge = lax.ppermute(tokens[0, rows - HALO :], "sp", [(i, i + 1) for i in range(count - 1)])
    gain = norm_gain[None]
    normed = call(normed_kernel, shape((rows, features), BF16), 1 << 22, tokens[0], gain, name="norm")
    halo = call(normed_kernel, shape((HALO, features), BF16), 1 << 18, edge, gain, name="halo")

    rate = step_rate[0].reshape(CHUNKS, steps).T.reshape(rows, 1)
    scale = jnp.repeat(log_step, states)[None]
    bar, hold, cum, total = call(
        maps_kernel,
        (shape((2, rows, flat)), shape((2, rows, flat)), shape((2, rows, flat)), shape((2, flat))),
        1 << 27,
        rate,
        scale,
        decay_real.reshape(1, flat),
        frequency.reshape(1, flat),
        name="maps",
    )
    maps = spread(total, "sp")

    index = jnp.arange(rows)
    source = (index % CHUNKS) * steps + index // CHUNKS
    permute = (source[:, None] == index[None, :]).astype(BF16)
    coupling = jnp.concatenate(
        [
            block_diagonal(jnp.swapaxes(input_real, 1, 2)),
            block_diagonal(jnp.swapaxes(input_imag, 1, 2)),
        ],
        axis=1,
    )
    coupling = jnp.stack(halves(coupling))
    reading = jnp.stack(
        [
            block_diagonal(jnp.swapaxes(read_real, 1, 2)),
            block_diagonal(-jnp.swapaxes(read_imag, 1, 2)),
        ]
    )
    reading = jnp.stack(halves(reading))

    state_weights = spread(state_shards, "fs")
    chan, local, end = call(
        local_kernel,
        (shape((rows, width), BF16), shape((2, rows, flat)), shape((2, flat))),
        1 << 28,
        normed,
        state_weights,
        permute,
        coupling,
        bar,
        hold,
        cum,
        scratch=(pltpu.VMEM((2, rows, flat), F32),),
        name="local",
    )
    ends = spread(end, "sp")
    conv_weights = spread(conv_shards, "fs")
    conv_mix = call(
        conv_kernel,
        shape((rows, width), BF16),
        1 << 29,
        normed,
        halo,
        conv_weights,
        conv_taps,
        name="conv",
    )
    state_mix, closing = call(
        read_kernel,
        (shape((rows, width), BF16), shape((2, flat))),
        1 << 28,
        lax.axis_index("sp").astype(jnp.int32)[None],
        maps,
        ends,
        initial_state[0].reshape(2, flat),
        local,
        cum,
        chan,
        permute.T,
        reading,
        skip_gain.reshape(1, width),
        smem=1,
        name="read",
    )
    out_weights = spread(out_shards, "fs")
    fs, sp = out_weights.shape[:2]
    out_weights = jnp.swapaxes(out_weights, 0, 1).reshape(features, 2 * width)
    mixes = jnp.concatenate([state_mix, conv_mix], axis=1)
    partial = jnp.einsum("rc,dc->rd", mixes, out_weights, preferred_element_type=F32).astype(BF16)
    tp = lax.axis_size("tp")
    parts = lax.all_to_all(partial.reshape(tp, rows // tp, features), "tp", 0, 0, tiled=True)
    mixed = jnp.sum(parts.astype(F32), axis=0).astype(BF16)
    share = states // count
    grid = closing.reshape(2, groups, states)
    own_share = lax.dynamic_slice_in_dim(grid, lax.axis_index("sp") * share, share, 2)
    return (mixed[None], own_share[None])


def solution(mesh):
    return jax.shard_map(
        body,
        mesh=mesh,
        in_specs=(
            P("fs", "sp", None),
            P(),
            P(("sp", "fs"), "tp"),
            P(("sp", "fs"), "tp"),
            P(("sp", "fs"), "tp"),
            P(("sp", "fs"), "tp"),
            P(("sp", "fs"), "tp"),
            P(("sp", "fs"), "tp"),
            P("tp"),
            P("tp", None),
            P("tp", None),
            P("fs", "sp"),
            P("tp", None, None),
            P("tp", None, None),
            P("tp", None, None),
            P("tp", None, None),
            P("tp", None),
            P(None, "tp"),
            P("fs", None, "tp", None),
        ),
        out_specs=(P("fs", ("sp", "tp"), None), P("fs", None, "tp", "sp")),
        check_vma=False,
    )
```

time: 256 us -> 205 us (0.80)
  waiting for transfers between devices: 148 us -> 35.5 us
  blocking collectives: 21.3 us -> 71.7 us
  Pallas kernels: 0 us -> 21.6 us
  starting transfers between devices: 23.2 us -> 41.5 us
  between operations: 15.4 us -> 0.92 us
  matrix products: 12.5 us -> 2.3 us
  other arithmetic: 14.3 us -> 5.95 us
    all_gather x1 -> x0, waiting for transfers between devices: 134 us -> none  [in_one_piece(): lax.all_gather(both, axis, axis=dim, tiled=True)]
    all_to_all x0 -> x4, blocking collectives: none -> 71.7 us  [spread(): return lax.all_to_all(replicated(x, copies), axis, 0, 0, tiled=True)]
    pallas_call x0 -> x6, Pallas kernels: none -> 21.6 us  [call(): pl.pallas_call(kernel, out_shape=out_shape, in_specs=in_specs, out_specs=...]
    all_to_all x1 -> x5, waiting for transfers between devices: 14.1 us -> 35.5 us  [the longest x4 21.4 us: spread(): return lax.all_to_all(replicated(x, copies), axis, 0, 0, tiled=True)]
    all_gather x1 -> x0, blocking collectives: 21.3 us -> none  [gather_together(): lines, at, done = (lax.all_gather(ravelled, axis), 0, [])]
    all_to_all x1 -> x5, starting transfers between devices: 21.2 us -> 33.8 us  [the longest x4 22.5 us: spread(): return lax.all_to_all(replicated(x, copies), axis, 0, 0, tiled=True)]
    dot_general x9 -> x1, matrix products: 12.5 us -> 2.3 us  [body(): jnp.einsum('rc,dc->rd', mixes, out_weights, preferred_element_type=F32)]
    broadcast_in_dim x1 -> x9, local copies, waits for them, and re-layouts: 0.33 us -> 6.68 us  [the longest x8 5.96 us: replicated(): return jnp.broadcast_to(x[None], (copies, *x.shape))]
  transfers between devices with their start and end apart: 3 -> 6, of which waited for: 2 -> 4; matrix products, arithmetic and copies ran while one was open for 4% -> 7% of each run, Pallas kernels for 0% -> 6%
where the time goes in v1:
time: 205 us; the launch traced here: 202 us
  blocking collectives  71.7 us (35%)
  starting transfers between devices  41.5 us (20%)
  waiting for transfers between devices  35.5 us (17%)
  local copies, waits for them, and re-layouts  22.7 us (11%)
  Pallas kernels  21.6 us (11%)
  other arithmetic  5.95 us (3%)
  matrix products  2.3 us (1%)
    all_to_all x4, blocking collectives, spread(): return lax.all_to_all(replicated(x, copies), axis, 0, 0, tiled=True)  71.7 us
    all_to_all x4, starting transfers between devices, spread(): return lax.all_to_all(replicated(x, copies), axis, 0, 0, tiled=True)  22.5 us
    pallas_call x6, Pallas kernels, call(): pl.pallas_call(kernel, out_shape=out_shape, in_specs=in_specs, out_specs=...  21.6 us
    all_to_all x4, waiting for transfers between devices, spread(): return lax.all_to_all(replicated(x, copies), axis, 0, 0, tiled=True)  21.4 us
    all_to_all x1, waiting for transfers between devices, body(): lax.all_to_all(partial.reshape(tp, rows // tp, features), 'tp', 0, 0, til...  14.1 us
    all_to_all x1, starting transfers between devices, body(): lax.all_to_all(partial.reshape(tp, rows // tp, features), 'tp', 0, 0, til...  11.3 us
    ppermute x1, starting transfers between devices, body(): lax.ppermute(tokens[0, rows - HALO:], 'sp', [(i, i + 1) for i in range(co...  7.71 us
    broadcast_in_dim x8, local copies, waits for them, and re-layouts, replicated(): return jnp.broadcast_to(x[None], (copies, *x.shape))  5.96 us
  transfers between devices with their start and end apart: 6, of which 4 were waited for; matrix products, arithmetic and copies ran while one was open for 7% of the time, Pallas kernels for 6%

profile of v1, /device:TPU:1, one launch (start us, length us, event | category | flops | bytes accessed | tf_op | source)
XLA Modules:
  0.0 202.2 jit_solution(10671292803169636742)
XLA Ops:
  1.2 1.3 reduce.4
  4.8 1.3 reshape.291.decay_ref
  6.1 1.3 reshape.292.freq_ref
  7.5 6.0 %maps.1 = (f32[2,256,512]{2,1,0:T(8,128)}, f32[2,256,512]{2,1,0:T(8,128)}, f32[2,256,512]{2,1,0:T(8,128)}, f32[2,512]{1,0:T(2,128)}) custom-call(f32[256,1]{1,0:T(8,128)} %reshape.297.rate_ref, f32[1,512]{1,0:T(1,128)} %broadcast_in_dim_reshape.3.scale_ref, f32[1,512]{1,0:T(1,128)} %reshape.291.decay_ref, f32[1,512]{1,0:T(1,128)} %reshape.292.freq_ref), custom_call_target="tpu_custom_call" | custom-call | flops 134217728 | bytes 1048576 | tf_op jit(solution)/shard_map/maps/pallas_call | solution.py:210
  14.2 27.2 %all_to_all.45.maps_ref = f32[16,2,512]{2,1,0:T(2,128)} all-to-all(f32[16,2,512]{2,1,0:T(2,128)S(1)} %broadcast_in_dim.137), channel_id=1, replica_groups=mesh['sp'=16,'fs'=4,'tp'=8] {'sp'}, dimensions={0} | all-to-all | bytes 131072 | tf_op jit(solution)/shard_map/all_to_all | solution.py:22
  42.2 14.9 %all_to_all.46 = bf16[16,32,128]{2,1,0:T(8,128)(2,1)S(1)} all-to-all(bf16[16,32,128]{2,1,0:T(8,128)(2,1)S(1)} %broadcast_in_dim.139), channel_id=1, replica_groups=mesh['sp'=16,'fs'=4,'tp'=8] {'sp'}, dimensions={0} | all-to-all | bytes 262144 | tf_op jit(solution)/shard_map/all_to_all | solution.py:22
  58.0 4.2 %all-to-all-start.2 = ((bf16[4,16,32,128]{3,2,1,0:T(8,128)(2,1)}), bf16[4,16,32,128]{3,2,1,0:T(8,128)(2,1)S(1)}, u32[]{:S(2)}, u32[]{:S(2)}) async-start(bf16[4,16,32,128]{3,2,1,0:T(8,128)(2,1)} %broadcast_in_dim.140), calls=%async_computation.2 | async-start | bytes 1048576 | tf_op jit(solution)/shard_map/all_to_all | solution.py:22
  62.3 6.8 %all-to-all-done.2.w_ref = bf16[4,16,32,128]{3,2,1,0:T(8,128)(2,1)S(1)} async-done(((bf16[4,16,32,128]{3,2,1,0:T(8,128)(2,1)}), bf16[4,16,32,128]{3,2,1,0:T(8,128)(2,1)S(1)}, u32[]{:S(2)}, u32[]{:S(2)}) %all-to-all-start.2) | async-done | bytes 524320 | tf_op jit(solution)/shard_map/all_to_all | solution.py:22
  69.9 5.5 %all-to-all-start.6 = ((bf16[16,32,256]{2,1,0:T(8,128)(2,1)}), bf16[16,32,256]{2,1,0:T(8,128)(2,1)S(1)}, u32[]{:S(2)}, u32[]{:S(2)}) async-start(bf16[16,32,256]{2,1,0:T(8,128)(2,1)} %broadcast_in_dim.152), calls=%async_computation.6 | async-start | bytes 524288 | tf_op jit(solution)/shard_map/all_to_all | solution.py:22
  75.8 2.6 %norm.1.normed_ref = bf16[256,2048]{1,0:T(8,128)(2,1)} custom-call(bf16[256,2048]{1,0:T(8,128)(2,1)} %bitcast.33, f32[1,2048]{1,0:T(1,128)} %bitcast.39), custom_call_target="tpu_custom_call" | custom-call | flops 4194304 | bytes 1048576 | tf_op jit(solution)/shard_map/norm/pallas_call | solution.py:210
  80.2 4.8 %local.1 = (bf16[256,128]{1,0:T(8,128)(2,1)}, f32[2,256,512]{2,1,0:T(8,128)}, f32[2,512]{1,0:T(2,128)}) custom-call(bf16[256,2048]{1,0:T(8,128)(2,1)} %norm.1.normed_ref, bf16[4,16,32,128]{3,2,1,0:T(8,128)(2,1)} %copy-done.2, bf16[256,256]{1,0:T(8,128)(2,1)} %get-tuple-element.25.perm_ref, bf16[2,128,1024]{2,1,0:T(8,128)(2,1)} %pad_maximum_fusion.couple_ref, ...), custom_call_target="tpu_custom_call" | custom-call | flops 268435456 | bytes 1048576 | tf_op jit(solution)/shard_map/local/pallas_call | solution.py:210
  85.0 3.1 %all-to-all-done.6 = bf16[16,32,256]{2,1,0:T(8,128)(2,1)S(1)} async-done(((bf16[16,32,256]{2,1,0:T(8,128)(2,1)}), bf16[16,32,256]{2,1,0:T(8,128)(2,1)S(1)}, u32[]{:S(2)}, u32[]{:S(2)}) %all-to-all-start.6) | async-done | bytes 262176 | tf_op jit(solution)/shard_map/all_to_all | solution.py:22
  88.0 1.3 broadcast_in_dim.145
  89.4 9.1 %all-to-all-start.3 = ((f32[16,2,512]{2,1,0:T(2,128)}), f32[16,2,512]{2,1,0:T(2,128)S(1)}, u32[]{:S(2)}, u32[]{:S(2)}) async-start(f32[16,2,512]{2,1,0:T(2,128)} %broadcast_in_dim.145), calls=%async_computation.3 | async-start | bytes 131072 | tf_op jit(solution)/shard_map/all_to_all | solution.py:22
  98.6 11.5 %all-to-all-done.3.ends_ref = f32[16,2,512]{2,1,0:T(2,128)S(1)} async-done(((f32[16,2,512]{2,1,0:T(2,128)}), f32[16,2,512]{2,1,0:T(2,128)S(1)}, u32[]{:S(2)}, u32[]{:S(2)}) %all-to-all-start.3) | async-done | bytes 65568 | tf_op jit(solution)/shard_map/all_to_all | solution.py:22
  110.1 17.4 %all_to_all.47 = bf16[16,32,384]{2,1,0:T(8,128)(2,1)S(1)} all-to-all(bf16[16,32,384]{2,1,0:T(8,128)(2,1)S(1)} %broadcast_in_dim.150), channel_id=1, replica_groups=mesh['sp'=16,'fs'=4,'tp'=8] {'sp'}, dimensions={0} | all-to-all | bytes 786432 | tf_op jit(solution)/shard_map/all_to_all | solution.py:22
  127.6 12.2 %all_to_all.48 = bf16[4,16,32,256]{3,2,1,0:T(8,128)(2,1)S(1)} all-to-all(bf16[4,16,32,256]{3,2,1,0:T(8,128)(2,1)S(1)} %broadcast_in_dim.153), channel_id=1, replica_groups=mesh['sp'=16,'fs'=4,'tp'=8] {'fs'}, dimensions={0} | all-to-all | bytes 2097152 | tf_op jit(solution)/shard_map/all_to_all | solution.py:22
  139.8 1.4 broadcast_in_dim.151
  141.2 3.7 %all-to-all-start.5 = ((bf16[4,16,32,384]{3,2,1,0:T(8,128)(2,1)}), bf16[4,16,32,384]{3,2,1,0:T(8,128)(2,1)S(1)}, u32[]{:S(2)}, u32[]{:S(2)}) async-start(bf16[4,16,32,384]{3,2,1,0:T(8,128)(2,1)} %broadcast_in_dim.151), calls=%async_computation.5 | async-start | bytes 3145728 | tf_op jit(solution)/shard_map/all_to_all | solution.py:22
  145.7 7.7 %collective-permute-start = (bf16[16,2048]{1,0:T(8,128)(2,1)S(1)}, bf16[16,2048]{1,0:T(8,128)(2,1)S(1)}, u32[]{:S(2)}, u32[]{:S(2)}) collective-permute-start(bf16[16,2048]{1,0:T(8,128)(2,1)S(1)} %slice_bitcast_fusion), channel_id=1, source_target_pairs={{0,32},{32,64},{64,96},{96,128},{128,160},{160,192},{192,224},{224... | collective-permute-start | bytes 196616 | tf_op jit(solution)/shard_map/ppermute | solution.py:264
  153.5 1.0 broadcast_select_fusion.1
  154.5 1.9 stack.18
  156.5 1.1 copy.38
  158.4 1.1 copy.39
  162.4 1.6 halo.1.halo_ref
  164.0 3.4 %read.1 = (bf16[256,128]{1,0:T(8,128)(2,1)}, f32[2,512]{1,0:T(2,128)}) custom-call(s32[1]{0:T(128)} %bitcast.where_ref, f32[16,2,512]{2,1,0:T(2,128)} %all_to_all.45.maps_ref, f32[16,2,512]{2,1,0:T(2,128)} %copy-done.3, f32[2,512]{1,0:T(2,128)} %reshape_squeeze.7.initial_ref, f32[2,256,512]{2,1,0:T(8,128)} %get-tuple-element.16.local_ref, ...), custom_call_target="tpu_custom_call" | custom-call | flops 268435456 | bytes 1048576 | tf_op jit(solution)/shard_map/read/pallas_call | solution.py:210
  167.3 1.1 copy.40
  168.4 1.2 copy-done
  169.6 3.2 %conv.1 = bf16[256,128]{1,0:T(8,128)(2,1)} custom-call(bf16[256,2048]{1,0:T(8,128)(2,1)} %norm.1.normed_ref, bf16[16,2048]{1,0:T(8,128)(2,1)} %halo.1.halo_ref, bf16[4,16,32,384]{3,2,1,0:T(8,128)(2,1)} %copy-done, f32[3,128]{1,0:T(4,128)} %taps_ref.1), custom_call_target="tpu_custom_call" | custom-call | flops 536870912 | bytes 1048576 | tf_op jit(solution)/shard_map/conv/pallas_call | solution.py:210
  172.9 2.3 %convolution_convert_fusion = bf16[256,2048]{1,0:T(8,128)(2,1)} fusion(bf16[2048,256]{1,0:T(8,128)(2,1)S(1)} %bitcast.32, bf16[256,128]{1,0:T(8,128)(2,1)} %conv.1, bf16[256,128]{1,0:T(8,128)(2,1)S(1)} %copy-done.4), kind=kOutput, calls=%fused_computation | convolution fusion | flops 269221888 | bytes 2228224 | tf_op jit(solution)/shard_map/rc,dc->rd/dot_general | solution.py:350
  175.2 11.3 %all-to-all-start.8 = ((bf16[8,32,2048]{2,1,0:T(8,128)(2,1)}), bf16[8,32,2048]{2,1,0:T(8,128)(2,1)S(1)}, u32[]{:S(2)}, u32[]{:S(2)}) async-start(bf16[8,32,2048]{2,1,0:T(8,128)(2,1)} %bitcast.11), calls=%async_computation.8 | async-start | bytes 2097152 | tf_op jit(solution)/shard_map/all_to_all | solution.py:352
  187.3 14.1 %all-to-all-done.8 = bf16[8,32,2048]{2,1,0:T(8,128)(2,1)S(1)} async-done(((bf16[8,32,2048]{2,1,0:T(8,128)(2,1)}), bf16[8,32,2048]{2,1,0:T(8,128)(2,1)S(1)}, u32[]{:S(2)}, u32[]{:S(2)}) %all-to-all-start.8) | async-done | bytes 1048608 | tf_op jit(solution)/shard_map/all_to_all | solution.py:352
  (76 shorter events, 14.7 us)
Async XLA Ops:
  0.6 61.6 %copy-start.12 = (bf16[32,128]{1,0:T(8,128)(2,1)S(1)}, bf16[32,128]{1,0:T(8,128)(2,1)}, u32[]{:S(2)}) copy-start(bf16[32,128]{1,0:T(8,128)(2,1)} %param.25) | copy-start | bytes 24580
  0.6 61.6 %copy-start.11 = (bf16[32,128]{1,0:T(8,128)(2,1)S(1)}, bf16[32,128]{1,0:T(8,128)(2,1)}, u32[]{:S(2)}) copy-start(bf16[32,128]{1,0:T(8,128)(2,1)} %param.26) | copy-start | bytes 24580
  13.5 61.8 %copy-start.8 = (f32[8,64,16]{1,2,0:T(8,128)S(1)}, f32[8,64,16]{1,2,0:T(8,128)}, u32[]{:S(2)}) copy-start(f32[8,64,16]{1,2,0:T(8,128)} %param.32) | copy-start | bytes 98308
  13.5 61.8 %copy-start.9 = (f32[8,64,16]{1,2,0:T(8,128)S(1)}, f32[8,64,16]{1,2,0:T(8,128)}, u32[]{:S(2)}) copy-start(f32[8,64,16]{1,2,0:T(8,128)} %param.31) | copy-start | bytes 98308
  58.0 11.1 %all-to-all-start.2 = ((bf16[4,16,32,128]{3,2,1,0:T(8,128)(2,1)}), bf16[4,16,32,128]{3,2,1,0:T(8,128)(2,1)S(1)}, u32[]{:S(2)}, u32[]{:S(2)}) async-start(bf16[4,16,32,128]{3,2,1,0:T(8,128)(2,1)} %broadcast_in_dim.140), calls=%async_computation.2 | async-start | bytes 1048576 | tf_op jit(solution)/shard_map/all_to_all | solution.py:22
  69.1 6.7 %copy-start.2 = (bf16[4,16,32,128]{3,2,1,0:T(8,128)(2,1)}, bf16[4,16,32,128]{3,2,1,0:T(8,128)(2,1)S(1)}, u32[]{:S(2)}) copy-start(bf16[4,16,32,128]{3,2,1,0:T(8,128)(2,1)S(1)} %all-to-all-done.2.w_ref) | copy-start | bytes 1572868
  69.9 18.2 %all-to-all-start.6 = ((bf16[16,32,256]{2,1,0:T(8,128)(2,1)}), bf16[16,32,256]{2,1,0:T(8,128)(2,1)S(1)}, u32[]{:S(2)}, u32[]{:S(2)}) async-start(bf16[16,32,256]{2,1,0:T(8,128)(2,1)} %broadcast_in_dim.152), calls=%async_computation.6 | async-start | bytes 524288 | tf_op jit(solution)/shard_map/all_to_all | solution.py:22
  80.2 18.3 %copy-start.13 = (bf16[32,128]{1,0:T(8,128)(2,1)S(1)}, bf16[32,128]{1,0:T(8,128)(2,1)}, u32[]{:S(2)}) copy-start(bf16[32,128]{1,0:T(8,128)(2,1)} %param.23) | copy-start | bytes 24580
  80.2 18.4 %copy-start.14 = (bf16[32,128]{1,0:T(8,128)(2,1)S(1)}, bf16[32,128]{1,0:T(8,128)(2,1)}, u32[]{:S(2)}) copy-start(bf16[32,128]{1,0:T(8,128)(2,1)} %param.24) | copy-start | bytes 24580
  80.2 18.4 %copy-start.15 = (bf16[32,128]{1,0:T(8,128)(2,1)S(1)}, bf16[32,128]{1,0:T(8,128)(2,1)}, u32[]{:S(2)}) copy-start(bf16[32,128]{1,0:T(8,128)(2,1)} %param.22) | copy-start | bytes 24580
  89.4 20.7 %all-to-all-start.3 = ((f32[16,2,512]{2,1,0:T(2,128)}), f32[16,2,512]{2,1,0:T(2,128)S(1)}, u32[]{:S(2)}, u32[]{:S(2)}) async-start(f32[16,2,512]{2,1,0:T(2,128)} %broadcast_in_dim.145), calls=%async_computation.3 | async-start | bytes 131072 | tf_op jit(solution)/shard_map/all_to_all | solution.py:22
  110.1 29.7 %copy-start.3 = (f32[16,2,512]{2,1,0:T(2,128)}, f32[16,2,512]{2,1,0:T(2,128)S(1)}, u32[]{:S(2)}) copy-start(f32[16,2,512]{2,1,0:T(2,128)S(1)} %all-to-all-done.3.ends_ref) | copy-start | bytes 196612
  141.2 12.3 %copy-start.5 = (f32[8,16,64]{2,1,0:T(8,128)S(1)}, f32[8,16,64]{2,1,0:T(8,128)}, u32[]{:S(2)}) copy-start(f32[8,16,64]{2,1,0:T(8,128)} %param.34) | copy-start | bytes 98308
  141.2 12.3 %copy-start.6 = (f32[8,16,64]{2,1,0:T(8,128)S(1)}, f32[8,16,64]{2,1,0:T(8,128)}, u32[]{:S(2)}) copy-start(f32[8,16,64]{2,1,0:T(8,128)} %param.33) | copy-start | bytes 98308
  141.2 27.3 %all-to-all-start.5 = ((bf16[4,16,32,384]{3,2,1,0:T(8,128)(2,1)}), bf16[4,16,32,384]{3,2,1,0:T(8,128)(2,1)S(1)}, u32[]{:S(2)}, u32[]{:S(2)}) async-start(bf16[4,16,32,384]{3,2,1,0:T(8,128)(2,1)} %broadcast_in_dim.151), calls=%async_computation.5 | async-start | bytes 3145728 | tf_op jit(solution)/shard_map/all_to_all | solution.py:22
  145.7 16.0 %collective-permute-start = (bf16[16,2048]{1,0:T(8,128)(2,1)S(1)}, bf16[16,2048]{1,0:T(8,128)(2,1)S(1)}, u32[]{:S(2)}, u32[]{:S(2)}) collective-permute-start(bf16[16,2048]{1,0:T(8,128)(2,1)S(1)} %slice_bitcast_fusion), channel_id=1, source_target_pairs={{0,32},{32,64},{64,96},{96,128},{128,160},{160,192},{192,224},{224... | collective-permute-start | bytes 196616 | tf_op jit(solution)/shard_map/ppermute | solution.py:264
  154.5 5.0 %copy-start.10 = (f32[1,2,8,64]{3,2,1,0:T(8,128)S(1)}, f32[1,2,8,64]{3,2,1,0:T(8,128)}, u32[]{:S(2)}) copy-start(f32[1,2,8,64]{3,2,1,0:T(8,128)} %param.37) | copy-start | bytes 12292
  154.5 5.7 %copy-start.17 = (f32[8,16]{1,0:T(8,128)S(1)}, f32[8,16]{1,0:T(8,128)}, u32[]{:S(2)}) copy-start(f32[8,16]{1,0:T(8,128)} %param.35) | copy-start | bytes 1540
  161.8 0.6 copy-start.7
  168.4 4.4 %copy-start.1 = (bf16[4,16,32,256]{3,2,0,1:T(8,128)(2,1)S(1)}, bf16[4,16,32,256]{3,2,0,1:T(8,128)(2,1)}, u32[]{:S(2)}) copy-start(bf16[4,16,32,256]{3,2,0,1:T(8,128)(2,1)} %copy.40) | copy-start | bytes 3145732
  168.4 4.4 %copy-start.4 = (bf16[256,128]{1,0:T(8,128)(2,1)S(1)}, bf16[256,128]{1,0:T(8,128)(2,1)}, u32[]{:S(2)}) copy-start(bf16[256,128]{1,0:T(8,128)(2,1)} %get-tuple-element.18) | copy-start | bytes 196612
  168.4 1.2 copy-start
  175.2 11.3 %copy-start.16 = (f32[2,512]{1,0:T(2,128)S(1)}, f32[2,512]{1,0:T(2,128)}, u32[]{:S(2)}) copy-start(f32[2,512]{1,0:T(2,128)} %get-tuple-element.19) | copy-start | bytes 12292
  175.2 26.3 %all-to-all-start.8 = ((bf16[8,32,2048]{2,1,0:T(8,128)(2,1)}), bf16[8,32,2048]{2,1,0:T(8,128)(2,1)S(1)}, u32[]{:S(2)}, u32[]{:S(2)}) async-start(bf16[8,32,2048]{2,1,0:T(8,128)(2,1)} %bitcast.11), calls=%async_computation.8 | async-start | bytes 2097152 | tf_op jit(solution)/shard_map/all_to_all | solution.py:352

commit v2 on v1

v2 whole, which is shorter than its diff:
```python
import jax
import jax.numpy as jnp
from jax import lax
from jax.experimental import pallas as pl
from jax.experimental.pallas import tpu as pltpu
from jax.sharding import PartitionSpec as P


F32 = jnp.float32
BF16 = jnp.bfloat16
CHUNKS = 8
HALO = 16
NT = (((1,), (1,)), ((), ()))


def spread(x, axis):
    copies = lax.axis_size(axis)
    many = jnp.broadcast_to(x[None], (copies, *x.shape))
    return lax.all_to_all(many, axis, 0, 0, tiled=True)


def complex_product(left_real, left_imag, right_real, right_imag):
    return (
        left_real * right_real - left_imag * right_imag,
        left_real * right_imag + left_imag * right_real,
    )


def sine_cosine(angle):
    turns = jnp.floor(angle * 0.6366197723675814 + 0.5)
    r = angle - turns * 1.5703125
    r = r - turns * 4.837512969970703e-4
    r = r - turns * 7.549789948768648e-8
    r2 = r * r
    sine = r + r * r2 * (-1.6666654611e-1 + r2 * (8.3321608736e-3 + r2 * -1.9515295891e-4))
    cosine = (
        1.0
        - 0.5 * r2
        + r2 * r2 * (4.166664568298827e-2 + r2 * (-1.388731625493765e-3 + r2 * 2.443315711809948e-5))
    )
    quadrant = turns.astype(jnp.int32)
    odd = (quadrant & 1) == 1
    flip_sine = (quadrant & 2) == 2
    flip_cosine = ((quadrant + 1) & 2) == 2
    base_sine = jnp.where(odd, cosine, sine)
    base_cosine = jnp.where(odd, sine, cosine)
    return (
        jnp.where(flip_sine, -base_sine, base_sine),
        jnp.where(flip_cosine, -base_cosine, base_cosine),
    )


def iota(dims, axis):
    return lax.broadcasted_iota(jnp.int32, dims, axis)


def pieces(x, count):
    found = []
    for _ in range(count):
        part = x.astype(BF16)
        found.append(part)
        x = x - part.astype(F32)
    return found


def picked(x, selector, count=3):
    total = None
    for part in pieces(x, count):
        term = jnp.dot(part, selector, preferred_element_type=F32)
        total = term if total is None else total + term
    return total


def repeat_selector(narrow, wide):
    return (iota((narrow, wide), 1) % narrow == iota((narrow, wide), 0)).astype(BF16)


def flattened(x, groups):
    rows, narrow = x.shape
    wide = groups * narrow
    tiled = picked(x, repeat_selector(narrow, wide))
    own = iota((rows, wide), 1) // narrow == iota((rows, wide), 0) % groups
    tiled = jnp.where(own, tiled, 0.0)
    return [jnp.sum(tiled[at : at + groups], axis=0, keepdims=True) for at in range(0, rows, groups)]


def block_diagonal(x, groups):
    rows, narrow = x.shape
    wide = groups * narrow
    selector = repeat_selector(narrow, wide)
    own = iota((rows, wide), 1) // narrow == iota((rows, wide), 0) // (rows // groups)
    return [
        jnp.where(own, jnp.dot(part, selector, preferred_element_type=F32), 0.0).astype(BF16)
        for part in pieces(x, 2)
    ]


def spread_steps(log_ref, groups, states):
    lane = iota((1, groups * states), 1) // states
    out = jnp.zeros((1, groups * states), F32)
    for g in range(groups):
        out = jnp.where(lane == g, log_ref[g], out)
    return jnp.exp(out)


def chunk_order(rows, flip):
    r, c = (iota((rows, rows), 1 if flip else 0), iota((rows, rows), 0 if flip else 1))
    steps = rows // CHUNKS
    return (c == (r % CHUNKS) * steps + r // CHUNKS).astype(BF16)


def normalized(x, gain):
    x = x.astype(F32)
    mean_square = jnp.mean(x * x, axis=-1, keepdims=True)
    return (x * lax.rsqrt(mean_square + 1e-06) * gain).astype(BF16)


def prep_kernel(
    log_ref, tokens_ref, gain_ref, rate_ref, decay_ref, freq_ref, in_real_ref, in_imag_ref, out_real_ref, out_imag_ref,
    normed_ref, bar_ref, hold_ref, cum_ref, couple_ref, read_ref, column_ref,
):
    groups, states = decay_ref.shape
    flat = groups * states
    rows = tokens_ref.shape[0]
    part = 64

    def norm(i, _):
        at = pl.ds(pl.multiple_of(i * part, part), part)
        normed_ref[at, :] = normalized(tokens_ref[at, :], gain_ref[...])
        return 0

    lax.fori_loop(0, rows // part, norm, 0)
    order = chunk_order(rows, False)
    column = None
    for piece in pieces(jnp.broadcast_to(rate_ref[...], (16, rows)), 3):
        term = lax.dot_general(order, piece, NT, preferred_element_type=F32)
        column = term if column is None else column + term
    column_ref[...] = column
    (decay,) = flattened(decay_ref[...], groups)
    (freq,) = flattened(freq_ref[...], groups)
    scale = spread_steps(log_ref, groups, states)
    inverse = 1.0 / (decay * decay + freq * freq)
    steps = rows // CHUNKS

    def advance(j, carry):
        cum_real, cum_imag = carry
        at = pl.ds(pl.multiple_of(j * CHUNKS, CHUNKS), CHUNKS)
        step = column_ref[at, 0:1] * scale
        grow = jnp.exp(step * decay)
        sine, cosine = sine_cosine(step * freq)
        bar_real, bar_imag = (grow * cosine, grow * sine)
        less_real = bar_real - 1.0
        bar_ref[0, at, :] = bar_real
        bar_ref[1, at, :] = bar_imag
        hold_ref[0, at, :] = (less_real * decay + bar_imag * freq) * inverse
        hold_ref[1, at, :] = (bar_imag * decay - less_real * freq) * inverse
        cum_real, cum_imag = complex_product(cum_real, cum_imag, bar_real, bar_imag)
        cum_ref[0, at, :] = cum_real
        cum_ref[1, at, :] = cum_imag
        return (cum_real, cum_imag)

    one = jnp.ones((CHUNKS, flat), F32)
    lax.fori_loop(0, steps, advance, (one, jnp.zeros_like(one)))
    for at, ref in enumerate((in_real_ref, in_imag_ref)):
        high, low = block_diagonal(ref[...], groups)
        couple_ref[0, :, at * flat : (at + 1) * flat] = high
        couple_ref[1, :, at * flat : (at + 1) * flat] = low
    for at, (ref, sign) in enumerate(((out_real_ref, 1.0), (out_imag_ref, -1.0))):
        high, low = block_diagonal(ref[...] * sign, groups)
        read_ref[0, :, at * flat : (at + 1) * flat] = high
        read_ref[1, :, at * flat : (at + 1) * flat] = low


def gathered_rows(ref):
    fs, sp = ref.shape[:2]
    return jnp.concatenate([ref[f, z] for z in range(sp) for f in range(fs)], axis=0)


def local_kernel(normed_ref, w_ref, couple_ref, bar_ref, hold_ref, cum_ref, rate_ref, chan_ref, local_ref, end_ref, push_ref):
    rows = normed_ref.shape[0]
    w = gathered_rows(w_ref)
    state_in = jnp.dot(normed_ref[...], w, preferred_element_type=F32).astype(BF16)
    chan = jnp.dot(chunk_order(rows, False), state_in, preferred_element_type=F32).astype(BF16)
    chan_ref[...] = chan
    flat = bar_ref.shape[2]
    drive = jnp.dot(chan, couple_ref[0], preferred_element_type=F32) + jnp.dot(
        chan, couple_ref[1], preferred_element_type=F32
    )
    push_real, push_imag = complex_product(hold_ref[0], hold_ref[1], drive[:, :flat], drive[:, flat:])
    push_ref[0] = push_real
    push_ref[1] = push_imag
    steps = rows // CHUNKS

    def advance(j, carry):
        at = pl.ds(pl.multiple_of(j * CHUNKS, CHUNKS), CHUNKS)
        real, imag = complex_product(bar_ref[0, at, :], bar_ref[1, at, :], carry[0], carry[1])
        real = real + push_ref[0, at, :]
        imag = imag + push_ref[1, at, :]
        local_ref[0, at, :] = real
        local_ref[1, at, :] = imag
        return (real, imag)

    zero = jnp.zeros((CHUNKS, flat), F32)
    last_real, last_imag = lax.fori_loop(0, steps, advance, (zero, zero), unroll=4)
    tail = pl.ds((steps - 1) * CHUNKS, CHUNKS)
    end_real, end_imag = (cum_ref[0, tail, :], cum_ref[1, tail, :])
    real, imag = (last_real[0:1], last_imag[0:1])
    for c in range(1, CHUNKS):
        moved_real, moved_imag = complex_product(end_real[c : c + 1], end_imag[c : c + 1], real, imag)
        real = moved_real + last_real[c : c + 1]
        imag = moved_imag + last_imag[c : c + 1]
    end_ref[:, :flat] = jnp.concatenate([real, imag], axis=0)
    whole = jnp.sum(rate_ref[...], axis=1, keepdims=True)
    end_ref[:, flat:] = jnp.broadcast_to(whole, (2, end_ref.shape[1] - flat))


def gelu(v):
    return 0.5 * v * (1.0 + jnp.tanh(0.7978845608 * (v + 0.044715 * v * v * v)))


def read_kernel(
    where_ref, log_ref, ends_ref, decay_ref, freq_ref, initial_ref, local_ref, cum_ref, chan_ref, read_ref, skip_ref,
    mix_ref, closing_ref,
):
    groups, states = decay_ref.shape
    flat = groups * states
    spans = ends_ref.shape[0]
    here = where_ref[0]
    scale = spread_steps(log_ref, groups, states)
    (decay,) = flattened(decay_ref[...], groups)
    (freq,) = flattened(freq_ref[...], groups)
    enter_real, enter_imag = flattened(initial_ref[...], groups)
    real, imag = (enter_real, enter_imag)
    elapsed = jnp.concatenate([ends_ref[z, 0:1, flat:] for z in range(spans)], axis=0)[:, 0:1] * scale
    grow = jnp.exp(elapsed * decay)
    sine, cosine = sine_cosine(elapsed * freq)
    map_real, map_imag = (grow * cosine, grow * sine)
    for z in range(spans):
        now = here == z
        enter_real = jnp.where(now, real, enter_real)
        enter_imag = jnp.where(now, imag, enter_imag)
        moved_real, moved_imag = complex_product(map_real[z : z + 1], map_imag[z : z + 1], real, imag)
        real = moved_real + ends_ref[z, 0:1, :flat]
        imag = moved_imag + ends_ref[z, 1:2, :flat]
    share = states // spans
    lane = iota((flat, share), 0) % states
    wanted = (lane == here * share + iota((flat, share), 1)).astype(BF16)
    own = iota((groups, flat), 1) // states == iota((groups, flat), 0)
    for at, row in enumerate((real, imag)):
        closing_ref[at] = picked(jnp.where(own, jnp.broadcast_to(row, (groups, flat)), 0.0), wanted)
    rows = local_ref.shape[1]
    steps = rows // CHUNKS
    tail = pl.ds((steps - 1) * CHUNKS, CHUNKS)
    end_real, end_imag = (cum_ref[0, tail, :], cum_ref[1, tail, :])
    last_real, last_imag = (local_ref[0, tail, :], local_ref[1, tail, :])
    in_real, in_imag = ([enter_real], [enter_imag])
    for c in range(CHUNKS - 1):
        moved_real, moved_imag = complex_product(
            end_real[c : c + 1], end_imag[c : c + 1], in_real[-1], in_imag[-1]
        )
        in_real.append(moved_real + last_real[c : c + 1])
        in_imag.append(moved_imag + last_imag[c : c + 1])
    entry_real = jnp.concatenate(in_real, axis=0)[None]
    entry_imag = jnp.concatenate(in_imag, axis=0)[None]
    shape = (steps, CHUNKS, flat)
    moved_real, moved_imag = complex_product(
        cum_ref[0].reshape(shape), cum_ref[1].reshape(shape), entry_real, entry_imag
    )
    hidden_real = local_ref[0] + moved_real.reshape(rows, flat)
    hidden_imag = local_ref[1] + moved_imag.reshape(rows, flat)
    response = None
    for at, hidden in enumerate((hidden_real, hidden_imag)):
        high, low = pieces(hidden, 2)
        lanes = pl.ds(at * flat, flat)
        for left, right in ((high, 0), (low, 0), (high, 1)):
            term = lax.dot_general(left, read_ref[right, :, lanes], NT, preferred_element_type=F32)
            response = term if response is None else response + term
    (skip,) = flattened(skip_ref[...], groups)
    mixed = gelu(response + skip * chan_ref[...].astype(F32)).astype(BF16)
    mix_ref[...] = jnp.dot(chunk_order(rows, True), mixed, preferred_element_type=F32).astype(BF16)


def conv_kernel(
    place_ref, normed_ref, halo_ref, gain_ref, own_ref, up_ref, down_ref, left_ref, right_ref, taps_ref,
    mix_ref, weights_ref, w_ref,
):
    width = taps_ref.shape[1]
    rows = normed_ref.shape[0]
    spans, tall, wide = own_ref.shape
    half = left_ref.shape[2]
    split = w_ref.shape[1]
    z, y = (place_ref[0], place_ref[1])

    def placed(dz, turn):
        at_z = (z + dz) & (spans - 1)
        at_y = (y + 2 * dz + turn) & 3
        return pl.ds(pl.multiple_of((at_z * 4 + at_y) * tall, tall), tall)

    def put(at, lanes, piece):
        start, stop = lanes
        if start < split:
            w_ref[at, start : min(stop, split)] = piece[:, : min(stop, split) - start]
        if stop > split:
            begin = max(start, split)
            weights_ref[at, begin - split : stop - split] = piece[:, begin - start :]

    for dz in range(spans):
        put(placed(dz, 0), (0, wide), own_ref[dz])
        put(placed(dz, 1), (0, wide), up_ref[dz])
        put(placed(dz, 3), (0, wide), down_ref[dz])
        put(placed(dz + 1, 2), (0, half), left_ref[dz])
        put(placed(dz - 1, 2), (half, wide), right_ref[dz])
    w = w_ref[...]
    reach = taps_ref.shape[0] - 1
    here = jnp.dot(normed_ref[...], w, preferred_element_type=F32).astype(BF16).astype(F32)
    halo = normalized(halo_ref[...], gain_ref[...])
    before = jnp.dot(halo, w[:, : 2 * width], preferred_element_type=F32).astype(BF16).astype(F32)
    gated = (here[:, :width] * here[:, width : 2 * width]).astype(BF16).astype(F32)
    gated_before = (before[:, :width] * before[:, width:]).astype(BF16).astype(F32)
    extended = jnp.concatenate([gated_before, gated], axis=0)
    filtered = taps_ref[reach : reach + 1] * gated
    for tap in range(reach):
        at = HALO - reach + tap
        filtered = filtered + taps_ref[tap : tap + 1] * extended[at : at + rows]
    mix_ref[...] = (here[:, 2 * width :] * filtered).astype(BF16)


def out_kernel(state_ref, conv_ref, w_ref, out_ref):
    mixes = jnp.concatenate([state_ref[...], conv_ref[...]], axis=1)
    per = 512
    for at in range(0, w_ref.shape[0], per):
        product = lax.dot_general(mixes, w_ref[at : at + per], NT, preferred_element_type=F32)
        out_ref[:, at : at + per] = product.astype(BF16)


def moved(x, dz, dy):
    sp, fs = (lax.axis_size("sp"), lax.axis_size("fs"))
    pairs = [
        (z * fs + y, ((z - dz) % sp) * fs + (y - dy) % fs) for z in range(sp) for y in range(fs)
    ]
    return lax.ppermute(x, ("sp", "fs"), pairs)


def all_shards(x):
    far = [x] + [moved(x, dz, 0) for dz in (4, 8, 12)]
    far = jnp.stack(far)
    near = [far] + [moved(far, dz, dy) for dz, dy in ((1, 2), (2, 0), (-1, 2))]
    near[3] = jnp.roll(near[3], -1, axis=0)
    near = jnp.stack(near, axis=1)
    own = near.reshape(-1, *x.shape)
    half = x.shape[1] // 2 // 128 * 128
    return (
        own,
        moved(own, 0, 1),
        moved(own, 0, -1),
        moved(own[:, :, :half], 1, 0),
        moved(own[:, :, half:], -1, 0),
    )


def call(kernel, out_shape, flops, *args, scratch=(), smem=0):
    in_specs = [pl.BlockSpec(memory_space=pltpu.SMEM)] * smem + [
        pl.BlockSpec(memory_space=pltpu.VMEM)
    ] * (len(args) - smem)
    out_specs = jax.tree.map(lambda _: pl.BlockSpec(memory_space=pltpu.VMEM), out_shape)
    return pl.pallas_call(
        kernel,
        out_shape=out_shape,
        in_specs=in_specs,
        out_specs=out_specs,
        scratch_shapes=list(scratch),
        cost_estimate=pl.CostEstimate(flops=flops, bytes_accessed=1 << 20, transcendentals=0),
        compiler_params=pltpu.CompilerParams(vmem_limit_bytes=20 << 20),
    )(*args)


def shape(dims, dtype=F32):
    return jax.ShapeDtypeStruct(dims, dtype)


def body(
    tokens,
    norm_gain,
    w_state_in,
    w_value,
    w_outer,
    w_inner,
    w_state_out,
    w_conv_out,
    log_step,
    decay_real,
    frequency,
    step_rate,
    input_real,
    input_imag,
    read_real,
    read_imag,
    skip_gain,
    conv_taps,
    initial_state,
):
    rows, features = tokens.shape[1:]
    groups, states = decay_real.shape
    group = skip_gain.shape[1]
    flat = groups * states
    width = groups * group
    count = lax.axis_size("sp")

    state_shards = spread(w_state_in, "sp")
    own, up, down, left, right = all_shards(
        jnp.concatenate([w_value, w_inner, w_outer, w_state_out, w_conv_out], axis=1)
    )
    edge = lax.ppermute(tokens[0, rows - HALO :], "sp", [(i, i + 1) for i in range(count - 1)])
    gain = norm_gain[None]
    normed, bar, hold, cum, coupling, reading, _ = call(
        prep_kernel,
        (
            shape((rows, features), BF16),
            shape((2, rows, flat)),
            shape((2, rows, flat)),
            shape((2, rows, flat)),
            shape((2, width, 2 * flat), BF16),
            shape((2, width, 2 * flat), BF16),
            shape((rows, 16)),
        ),
        1 << 30,
        log_step,
        tokens[0],
        gain,
        step_rate,
        decay_real,
        frequency,
        jnp.swapaxes(input_real, 1, 2).reshape(width, states),
        jnp.swapaxes(input_imag, 1, 2).reshape(width, states),
        read_real.reshape(width, states),
        read_imag.reshape(width, states),
        smem=1,
    )
    state_weights = spread(state_shards, "fs")
    chan, local, end = call(
        local_kernel,
        (shape((rows, width), BF16), shape((2, rows, flat)), shape((2, flat + 128))),
        1 << 29,
        normed,
        state_weights,
        coupling,
        bar,
        hold,
        cum,
        step_rate,
        scratch=(pltpu.VMEM((2, rows, flat), F32),),
    )
    ends = spread(end, "sp")
    place = jnp.stack([lax.axis_index("sp"), lax.axis_index("fs")]).astype(jnp.int32)
    conv_mix, out_weights = call(
        conv_kernel,
        (shape((rows, width), BF16), shape((features, 2 * width), BF16)),
        1 << 29,
        place,
        normed,
        edge,
        gain,
        own,
        up,
        down,
        left,
        right,
        conv_taps,
        scratch=(pltpu.VMEM((features, 3 * width), BF16),),
        smem=1,
    )
    state_mix, closing = call(
        read_kernel,
        (shape((rows, width), BF16), shape((2, groups, states // count))),
        1 << 29,
        lax.axis_index("sp").astype(jnp.int32)[None],
        log_step,
        ends,
        decay_real,
        frequency,
        initial_state[0].reshape(2 * groups, states),
        local,
        cum,
        chan,
        reading,
        skip_gain,
        smem=2,
    )
    partial = call(
        out_kernel, shape((rows, features), BF16), 1 << 29, state_mix, conv_mix, out_weights
    )
    tp = lax.axis_size("tp")
    parts = lax.all_to_all(partial.reshape(tp, rows // tp, features), "tp", 0, 0, tiled=True)
    mixed = jnp.sum(parts.astype(F32), axis=0).astype(BF16)
    return (mixed[None], closing[None])


def solution(mesh):
    return jax.shard_map(
        body,
        mesh=mesh,
        in_specs=(
            P("fs", "sp", None),
            P(),
            P(("sp", "fs"), "tp"),
            P(("sp", "fs"), "tp"),
            P(("sp", "fs"), "tp"),
            P(("sp", "fs"), "tp"),
            P(("sp", "fs"), "tp"),
            P(("sp", "fs"), "tp"),
            P("tp"),
            P("tp", None),
            P("tp", None),
            P("fs", "sp"),
            P("tp", None, None),
            P("tp", None, None),
            P("tp", None, None),
            P("tp", None, None),
            P("tp", None),
            P(None, "tp"),
            P("fs", None, "tp", None),
        ),
        out_specs=(P("fs", ("sp", "tp"), None), P("fs", None, "tp", "sp")),
        check_vma=False,
    )
```

time: 205 us -> 149 us (0.73)
  blocking collectives: 71.7 us -> 0 us
  starting transfers between devices: 41.5 us -> 85.3 us
  waiting for transfers between devices: 35.5 us -> 24.6 us
  Pallas kernels: 21.6 us -> 13.3 us
  other arithmetic: 5.95 us -> 1.05 us
  matrix products: 2.3 us -> 0 us
    all_to_all x4 -> x0, blocking collectives: 71.7 us -> none  [spread(): return lax.all_to_all(replicated(x, copies), axis, 0, 0, tiled=True)]
    ppermute x0 -> x10, starting transfers between devices: none -> 45.4 us  [moved(): return lax.ppermute(x, ('sp', 'fs'), pairs)]
    all_to_all x4 -> x3, waiting for transfers between devices: 21.4 us -> 2.19 us  [spread(): return lax.all_to_all(many, axis, 0, 0, tiled=True)]
    unnamed x39 -> x72, local copies, waits for them, and re-layouts: 3.1 us -> 16.1 us
    pallas_call x6 -> x5, Pallas kernels: 21.6 us -> 13.3 us  [call(): pl.pallas_call(kernel, out_shape=out_shape, in_specs=in_specs, out_specs=...]
    ppermute x0 -> x10, waiting for transfers between devices: none -> 6.84 us  [moved(): return lax.ppermute(x, ('sp', 'fs'), pairs)]
    another operation x8 -> x1, local copies, waits for them, and re-layouts: 6.44 us -> 0.07 us  [all_shards(): near = jnp.stack(near, axis=1)]
    all_to_all x4 -> x3, starting transfers between devices: 22.5 us -> 28.2 us  [spread(): return lax.all_to_all(many, axis, 0, 0, tiled=True)]
  transfers between devices with their start and end apart: 6 -> 15, of which waited for: 4 -> 5; matrix products, arithmetic and copies ran while one was open for 7% -> 3% of each run, Pallas kernels for 6% -> 7%
where the time goes in v2:
time: 149 us; the launch traced here: 148 us
  starting transfers between devices  85.3 us (57%)
  waiting for transfers between devices  24.6 us (17%)
  local copies, waits for them, and re-layouts  22.3 us (15%)
  Pallas kernels  13.3 us (9%)
    ppermute x10, starting transfers between devices, moved(): return lax.ppermute(x, ('sp', 'fs'), pairs)  45.4 us
    all_to_all x3, starting transfers between devices, spread(): return lax.all_to_all(many, axis, 0, 0, tiled=True)  28.2 us
    unnamed x72, local copies, waits for them, and re-layouts  16.1 us
    all_to_all x1, waiting for transfers between devices, body(): lax.all_to_all(partial.reshape(tp, rows // tp, features), 'tp', 0, 0, til...  14.3 us
    pallas_call x5, Pallas kernels, call(): pl.pallas_call(kernel, out_shape=out_shape, in_specs=in_specs, out_specs=...  13.3 us
    all_to_all x1, starting transfers between devices, body(): lax.all_to_all(partial.reshape(tp, rows // tp, features), 'tp', 0, 0, til...  8.48 us
    ppermute x10, waiting for transfers between devices, moved(): return lax.ppermute(x, ('sp', 'fs'), pairs)  6.84 us
    ppermute x1, starting transfers between devices, body(): lax.ppermute(tokens[0, rows - HALO:], 'sp', [(i, i + 1) for i in range(co...  3.26 us
  transfers between devices with their start and end apart: 15, of which 5 were waited for; matrix products, arithmetic and copies ran while one was open for 3% of the time, Pallas kernels for 7%

profile of v2, /device:TPU:1, one launch (start us, length us, event | category | flops | bytes accessed | tf_op | source)
XLA Modules:
  0.0 147.7 jit_solution(12015880777190163701)
XLA Ops:
  0.6 1.4 broadcast_in_dim.32
  2.0 15.9 %all-to-all-start = ((bf16[16,32,128]{2,1,0:T(8,128)(2,1)}), bf16[16,32,128]{2,1,0:T(8,128)(2,1)S(1)}, u32[]{:S(2)}, u32[]{:S(2)}) async-start(bf16[16,32,128]{2,1,0:T(8,128)(2,1)} %broadcast_in_dim.32), calls=%async_computation | async-start | bytes 262144 | tf_op jit(solution)/shard_map/all_to_all | solution.py:19
  20.7 7.2 %collective-permute-start.3 = (bf16[32,640]{1,0:T(8,128)(2,1)S(1)}, bf16[32,640]{1,0:T(8,128)(2,1)S(1)}, u32[]{:S(2)}, u32[]{:S(2)}) collective-permute-start(bf16[32,640]{1,0:T(8,128)(2,1)S(1)} %constant_dynamic-update-slice_fusion), channel_id=1, source_target_pairs={{0,128},{8,136},{16,144},{24,152},{32,160},{40,168},{48,176},{56,1... | collective-permute-start | bytes 122888 | tf_op jit(solution)/shard_map/ppermute | solution.py:341
  27.9 7.0 %collective-permute-start.2 = (bf16[32,640]{1,0:T(8,128)(2,1)S(1)}, bf16[32,640]{1,0:T(8,128)(2,1)S(1)}, u32[]{:S(2)}, u32[]{:S(2)}) collective-permute-start(bf16[32,640]{1,0:T(8,128)(2,1)S(1)} %constant_dynamic-update-slice_fusion), channel_id=1, source_target_pairs={{0,256},{8,264},{16,272},{24,280},{32,288},{40,296},{48,304},{56,3... | collective-permute-start | bytes 122888 | tf_op jit(solution)/shard_map/ppermute | solution.py:341
  34.9 7.0 %collective-permute-start.1 = (bf16[32,640]{1,0:T(8,128)(2,1)S(1)}, bf16[32,640]{1,0:T(8,128)(2,1)S(1)}, u32[]{:S(2)}, u32[]{:S(2)}) collective-permute-start(bf16[32,640]{1,0:T(8,128)(2,1)S(1)} %constant_dynamic-update-slice_fusion), channel_id=1, source_target_pairs={{0,384},{8,392},{16,400},{24,408},{32,416},{40,424},{48,432},{56,4... | collective-permute-start | bytes 122888 | tf_op jit(solution)/shard_map/ppermute | solution.py:341
  41.9 4.5 %collective-permute-done.1 = bf16[32,640]{1,0:T(8,128)(2,1)S(1)} collective-permute-done((bf16[32,640]{1,0:T(8,128)(2,1)S(1)}, bf16[32,640]{1,0:T(8,128)(2,1)S(1)}, u32[]{:S(2)}, u32[]{:S(2)}) %collective-permute-start.1) | collective-permute-done | bytes 40992 | tf_op jit(solution)/shard_map/ppermute | solution.py:341
  46.4 3.6 %collective-permute-start.6 = (bf16[4,32,640]{2,1,0:T(8,128)(2,1)S(1)}, bf16[4,32,640]{2,1,0:T(8,128)(2,1)S(1)}, u32[]{:S(2)}, u32[]{:S(2)}) collective-permute-start(bf16[4,32,640]{2,1,0:T(8,128)(2,1)S(1)} %get-tuple-element.29), channel_id=1, source_target_pairs={{0,48},{8,56},{16,32},{24,40},{32,80},{40,88},{48,64},{56,72},{64,... | collective-permute-start | bytes 491528 | tf_op jit(solution)/shard_map/ppermute | solution.py:341
  50.0 4.0 %collective-permute-start.5 = (bf16[4,32,640]{2,1,0:T(8,128)(2,1)S(1)}, bf16[4,32,640]{2,1,0:T(8,128)(2,1)S(1)}, u32[]{:S(2)}, u32[]{:S(2)}) collective-permute-start(bf16[4,32,640]{2,1,0:T(8,128)(2,1)S(1)} %get-tuple-element.29), channel_id=1, source_target_pairs={{0,448},{8,456},{16,464},{24,472},{32,480},{40,488},{48,496},{56,5... | collective-permute-start | bytes 491528 | tf_op jit(solution)/shard_map/ppermute | solution.py:341
  54.1 4.0 %collective-permute-start.4 = (bf16[4,32,640]{2,1,0:T(8,128)(2,1)S(1)}, bf16[4,32,640]{2,1,0:T(8,128)(2,1)S(1)}, u32[]{:S(2)}, u32[]{:S(2)}) collective-permute-start(bf16[4,32,640]{2,1,0:T(8,128)(2,1)S(1)} %get-tuple-element.29), channel_id=1, source_target_pairs={{0,496},{8,504},{16,480},{24,488},{32,16},{40,24},{48,0},{56,8},{6... | collective-permute-start | bytes 491528 | tf_op jit(solution)/shard_map/ppermute | solution.py:341
  59.0 4.2 %all-to-all-start.1 = ((bf16[4,16,32,128]{3,2,1,0:T(8,128)(2,1)}), bf16[4,16,32,128]{3,2,1,0:T(8,128)(2,1)S(1)}, u32[]{:S(2)}, u32[]{:S(2)}) async-start(bf16[4,16,32,128]{3,2,1,0:T(8,128)(2,1)} %broadcast_in_dim.33), calls=%async_computation.1 | async-start | bytes 1048576 | tf_op jit(solution)/shard_map/all_to_all | solution.py:19
  63.2 2.3 %collective-permute-done.4 = bf16[4,32,640]{2,1,0:T(8,128)(2,1)S(1)} collective-permute-done((bf16[4,32,640]{2,1,0:T(8,128)(2,1)S(1)}, bf16[4,32,640]{2,1,0:T(8,128)(2,1)S(1)}, u32[]{:S(2)}, u32[]{:S(2)}) %collective-permute-start.4) | collective-permute-done | bytes 163872 | tf_op jit(solution)/shard_map/ppermute | solution.py:341
  65.8 3.6 %collective-permute-start.7 = (bf16[16,32,640]{2,1,0:T(8,128)(2,1)S(1)}, bf16[16,32,640]{2,1,0:T(8,128)(2,1)}, u32[]{:S(2)}, u32[]{:S(2)}) collective-permute-start(bf16[16,32,640]{2,1,0:T(8,128)(2,1)S(1)} %bitcast.29), channel_id=1, source_target_pairs={{0,24},{8,0},{16,8},{24,16},{32,56},{40,32},{48,40},{56,48},{64,88... | collective-permute-start | bytes 1966088 | tf_op jit(solution)/shard_map/ppermute | solution.py:341
  69.4 1.9 %collective-permute-start.8 = (bf16[16,32,640]{2,1,0:T(8,128)(2,1)S(1)}, bf16[16,32,640]{2,1,0:T(8,128)(2,1)}, u32[]{:S(2)}, u32[]{:S(2)}) collective-permute-start(bf16[16,32,640]{2,1,0:T(8,128)(2,1)S(1)} %bitcast.30), channel_id=1, source_target_pairs={{0,8},{8,16},{16,24},{24,0},{32,40},{40,48},{48,56},{56,32},{64,72... | collective-permute-start | bytes 1966088 | tf_op jit(solution)/shard_map/ppermute | solution.py:341
  72.1 6.0 %shard_map.194 = (bf16[256,2048]{1,0:T(8,128)(2,1)S(1)}, f32[2,256,512]{2,1,0:T(8,128)S(1)}, f32[2,256,512]{2,1,0:T(8,128)S(1)}, f32[2,256,512]{2,1,0:T(8,128)S(...) custom-call(f32[8]{0:T(128)S(1)} %copy-done.23, ...), custom_call_target="tpu_custom_call" | custom-call | flops 1073741824 | bytes 1048576 | tf_op jit(solution)/shard_map/pallas_call | solution.py:366
  78.0 1.0 copy-done.6
  82.3 5.1 %collective-permute-start.9 = (bf16[16,32,256]{2,1,0:T(8,128)(2,1)}, bf16[16,32,256]{2,1,0:T(8,128)(2,1)}, u32[]{:S(2)}, u32[]{:S(2)}) collective-permute-start(bf16[16,32,256]{2,1,0:T(8,128)(2,1)} %slice.24), channel_id=1, source_target_pairs={{0,480},{8,488},{16,496},{24,504},{32,0},{40,8},{48,16},{56,24},{6... | collective-permute-start | bytes 786440 | tf_op jit(solution)/shard_map/ppermute | solution.py:341
  87.4 1.9 %collective-permute-start.10 = (bf16[16,32,384]{2,1,0:T(8,128)(2,1)}, bf16[16,32,384]{2,1,0:T(8,128)(2,1)}, u32[]{:S(2)}, u32[]{:S(2)}) collective-permute-start(bf16[16,32,384]{2,1,0:T(8,128)(2,1)} %slice.25), channel_id=1, source_target_pairs={{0,32},{8,40},{16,48},{24,56},{32,64},{40,72},{48,80},{56,88},{64,... | collective-permute-start | bytes 1179656 | tf_op jit(solution)/shard_map/ppermute | solution.py:341
  89.4 1.2 copy-done.5
  90.6 1.2 copy-done.7
  91.8 1.0 copy-done.11
  92.8 1.4 shard_map.195
  94.2 1.0 copy-done
  95.9 8.2 %all-to-all-start.2 = ((f32[16,2,640]{2,1,0:T(2,128)}), f32[16,2,640]{2,1,0:T(2,128)S(1)}, u32[]{:S(2)}, u32[]{:S(2)}) async-start(f32[16,2,640]{2,1,0:T(2,128)} %broadcast_in_dim.34), calls=%async_computation.2 | async-start | bytes 163840 | tf_op jit(solution)/shard_map/all_to_all | solution.py:19
  104.9 3.3 %collective-permute-start = (bf16[16,2048]{1,0:T(8,128)(2,1)S(1)}, bf16[16,2048]{1,0:T(8,128)(2,1)S(1)}, u32[]{:S(2)}, u32[]{:S(2)}) collective-permute-start(bf16[16,2048]{1,0:T(8,128)(2,1)S(1)} %slice_bitcast_fusion), channel_id=1, source_target_pairs={{0,32},{32,64},{64,96},{96,128},{128,160},{160,192},{192,224},{224... | collective-permute-start | bytes 196616 | tf_op jit(solution)/shard_map/ppermute | solution.py:413
  108.3 1.3 collective-permute-done.halo_ref
  110.3 2.6 %shard_map.197 = (bf16[256,128]{1,0:T(8,128)(2,1)S(1)}, bf16[2048,256]{1,0:T(8,128)(2,1)S(1)}) custom-call(s32[2]{0:T(128)S(1)} %pad_add_fusion.place_ref, bf16[256,2048]{1,0:T(8,128)(2,1)S(1)} %get-tuple-element.15.normed_ref, bf16[16,2048]{1,0:T(8,128)(2,1)S(1)} %collective-permute-done.halo_ref, f32[1,2048]{1,0:T(1,128)S(1)} %bitcast.35, ...), custom_call_target="tpu_custom_call" | custom-call | flops 536870912 | bytes 1048576 | tf_op jit(solution)/shard_map/pallas_call | solution.py:366
  113.9 2.2 %all-to-all-done.2.ends_ref = f32[16,2,640]{2,1,0:T(2,128)S(1)} async-done(((f32[16,2,640]{2,1,0:T(2,128)}), f32[16,2,640]{2,1,0:T(2,128)S(1)}, u32[]{:S(2)}, u32[]{:S(2)}) %all-to-all-start.2) | async-done | bytes 81952 | tf_op jit(solution)/shard_map/all_to_all | solution.py:19
  116.7 1.2 copy-done.1
  120.0 2.0 %shard_map.196 = (bf16[256,128]{1,0:T(8,128)(2,1)S(1)}, f32[2,8,4]{2,1,0:T(8,128)S(1)}) custom-call(s32[1]{0:T(128)} %bitcast.where_ref, f32[8]{0:T(128)S(1)} %copy-done.24, f32[16,2,640]{2,1,0:T(2,128)S(1)} %all-to-all-done.2.ends_ref, f32[8,64]{1,0:T(8,128)S(1)} %copy-done.16, f32[8,64]{1,0:T(8,128)S(1)} %copy-done.18, f32[16,64]{1,0:T(8,128)S(1)} %bitcast.36, ...), custom_call_target="tpu_custom_call" | custom-call | flops 536870912 | bytes 1048576 | tf_op jit(solution)/shard_map/pallas_call | solution.py:366
  122.0 1.5 %shard_map.198 = bf16[256,2048]{1,0:T(8,128)(2,1)} custom-call(bf16[256,128]{1,0:T(8,128)(2,1)S(1)} %get-tuple-element.24.state_ref, bf16[256,128]{1,0:T(8,128)(2,1)S(1)} %get-tuple-element.25.conv_ref, bf16[2048,256]{1,0:T(8,128)(2,1)S(1)} %copy-done.3), custom_call_target="tpu_custom_call" | custom-call | flops 536870912 | bytes 1048576 | tf_op jit(solution)/shard_map/pallas_call | solution.py:366
  123.5 8.5 %all-to-all-start.3 = ((bf16[8,32,2048]{2,1,0:T(8,128)(2,1)}), bf16[8,32,2048]{2,1,0:T(8,128)(2,1)S(1)}, u32[]{:S(2)}, u32[]{:S(2)}) async-start(bf16[8,32,2048]{2,1,0:T(8,128)(2,1)} %bitcast.21), calls=%async_computation.3 | async-start | bytes 2097152 | tf_op jit(solution)/shard_map/all_to_all | solution.py:493
  132.6 14.3 %all-to-all-done.3 = bf16[8,32,2048]{2,1,0:T(8,128)(2,1)S(1)} async-done(((bf16[8,32,2048]{2,1,0:T(8,128)(2,1)}), bf16[8,32,2048]{2,1,0:T(8,128)(2,1)S(1)}, u32[]{:S(2)}, u32[]{:S(2)}) %all-to-all-start.3) | async-done | bytes 1048608 | tf_op jit(solution)/shard_map/all_to_all | solution.py:493
  (91 shorter events, 15.3 us)
Async XLA Ops:
  2.0 15.9 %copy-start.29 = (bf16[32,128]{1,0:T(8,128)(2,1)S(1)}, bf16[32,128]{1,0:T(8,128)(2,1)}, u32[]{:S(2)}) copy-start(bf16[32,128]{1,0:T(8,128)(2,1)} %param.22) | copy-start | bytes 24580
  2.0 56.1 %all-to-all-start = ((bf16[16,32,128]{2,1,0:T(8,128)(2,1)}), bf16[16,32,128]{2,1,0:T(8,128)(2,1)S(1)}, u32[]{:S(2)}, u32[]{:S(2)}) async-start(bf16[16,32,128]{2,1,0:T(8,128)(2,1)} %broadcast_in_dim.32), calls=%async_computation | async-start | bytes 262144 | tf_op jit(solution)/shard_map/all_to_all | solution.py:19
  20.7 21.2 %collective-permute-start.3 = (bf16[32,640]{1,0:T(8,128)(2,1)S(1)}, bf16[32,640]{1,0:T(8,128)(2,1)S(1)}, u32[]{:S(2)}, u32[]{:S(2)}) collective-permute-start(bf16[32,640]{1,0:T(8,128)(2,1)S(1)} %constant_dynamic-update-slice_fusion), channel_id=1, source_target_pairs={{0,128},{8,136},{16,144},{24,152},{32,160},{40,168},{48,176},{56,1... | collective-permute-start | bytes 122888 | tf_op jit(solution)/shard_map/ppermute | solution.py:341
  27.9 14.0 %collective-permute-start.2 = (bf16[32,640]{1,0:T(8,128)(2,1)S(1)}, bf16[32,640]{1,0:T(8,128)(2,1)S(1)}, u32[]{:S(2)}, u32[]{:S(2)}) collective-permute-start(bf16[32,640]{1,0:T(8,128)(2,1)S(1)} %constant_dynamic-update-slice_fusion), channel_id=1, source_target_pairs={{0,256},{8,264},{16,272},{24,280},{32,288},{40,296},{48,304},{56,3... | collective-permute-start | bytes 122888 | tf_op jit(solution)/shard_map/ppermute | solution.py:341
  34.9 11.5 %collective-permute-start.1 = (bf16[32,640]{1,0:T(8,128)(2,1)S(1)}, bf16[32,640]{1,0:T(8,128)(2,1)S(1)}, u32[]{:S(2)}, u32[]{:S(2)}) collective-permute-start(bf16[32,640]{1,0:T(8,128)(2,1)S(1)} %constant_dynamic-update-slice_fusion), channel_id=1, source_target_pairs={{0,384},{8,392},{16,400},{24,408},{32,416},{40,424},{48,432},{56,4... | collective-permute-start | bytes 122888 | tf_op jit(solution)/shard_map/ppermute | solution.py:341
  46.4 16.7 %collective-permute-start.6 = (bf16[4,32,640]{2,1,0:T(8,128)(2,1)S(1)}, bf16[4,32,640]{2,1,0:T(8,128)(2,1)S(1)}, u32[]{:S(2)}, u32[]{:S(2)}) collective-permute-start(bf16[4,32,640]{2,1,0:T(8,128)(2,1)S(1)} %get-tuple-element.29), channel_id=1, source_target_pairs={{0,48},{8,56},{16,32},{24,40},{32,80},{40,88},{48,64},{56,72},{64,... | collective-permute-start | bytes 491528 | tf_op jit(solution)/shard_map/ppermute | solution.py:341
  50.0 13.2 %collective-permute-start.5 = (bf16[4,32,640]{2,1,0:T(8,128)(2,1)S(1)}, bf16[4,32,640]{2,1,0:T(8,128)(2,1)S(1)}, u32[]{:S(2)}, u32[]{:S(2)}) collective-permute-start(bf16[4,32,640]{2,1,0:T(8,128)(2,1)S(1)} %get-tuple-element.29), channel_id=1, source_target_pairs={{0,448},{8,456},{16,464},{24,472},{32,480},{40,488},{48,496},{56,5... | collective-permute-start | bytes 491528 | tf_op jit(solution)/shard_map/ppermute | solution.py:341
  54.1 11.4 %collective-permute-start.4 = (bf16[4,32,640]{2,1,0:T(8,128)(2,1)S(1)}, bf16[4,32,640]{2,1,0:T(8,128)(2,1)S(1)}, u32[]{:S(2)}, u32[]{:S(2)}) collective-permute-start(bf16[4,32,640]{2,1,0:T(8,128)(2,1)S(1)} %get-tuple-element.29), channel_id=1, source_target_pairs={{0,496},{8,504},{16,480},{24,488},{32,16},{40,24},{48,0},{56,8},{6... | collective-permute-start | bytes 491528 | tf_op jit(solution)/shard_map/ppermute | solution.py:341
  59.0 30.4 %all-to-all-start.1 = ((bf16[4,16,32,128]{3,2,1,0:T(8,128)(2,1)}), bf16[4,16,32,128]{3,2,1,0:T(8,128)(2,1)S(1)}, u32[]{:S(2)}, u32[]{:S(2)}) async-start(bf16[4,16,32,128]{3,2,1,0:T(8,128)(2,1)} %broadcast_in_dim.33), calls=%async_computation.1 | async-start | bytes 1048576 | tf_op jit(solution)/shard_map/all_to_all | solution.py:19
  65.5 5.9 %copy-start.20 = (bf16[1,256,2048]{2,1,0:T(8,128)(2,1)S(1)}, bf16[1,256,2048]{2,1,0:T(8,128)(2,1)}, u32[]{:S(2)}) copy-start(bf16[1,256,2048]{2,1,0:T(8,128)(2,1)} %param.19) | copy-start | bytes 3145732
  65.6 5.8 %copy-start.17 = (f32[8,64]{1,0:T(8,128)S(1)}, f32[8,64]{1,0:T(8,128)}, u32[]{:S(2)}) copy-start(f32[8,64]{1,0:T(8,128)} %freq_ref.3) | copy-start | bytes 6148
  65.6 5.8 %copy-start.23 = (f32[8]{0:T(128)S(1)}, f32[8]{0:T(128)}, u32[]{:S(2)}) copy-start(f32[8]{0:T(128)} %log_ref.3) | copy-start | bytes 100
  65.6 5.8 %copy-start.25 = (f32[8,64,16]{1,2,0:T(8,128)S(1)}, f32[8,64,16]{1,2,0:T(8,128)}, u32[]{:S(2)}) copy-start(f32[8,64,16]{1,2,0:T(8,128)} %param.31) | copy-start | bytes 98308
  65.7 5.8 %copy-start.26 = (f32[8,64,16]{1,2,0:T(8,128)S(1)}, f32[8,64,16]{1,2,0:T(8,128)}, u32[]{:S(2)}) copy-start(f32[8,64,16]{1,2,0:T(8,128)} %param.32) | copy-start | bytes 98308
  65.7 5.8 %copy-start.27 = (f32[8,16,64]{2,1,0:T(8,128)S(1)}, f32[8,16,64]{2,1,0:T(8,128)}, u32[]{:S(2)}) copy-start(f32[8,16,64]{2,1,0:T(8,128)} %param.33) | copy-start | bytes 98308
  65.7 5.8 %copy-start.28 = (f32[8,16,64]{2,1,0:T(8,128)S(1)}, f32[8,16,64]{2,1,0:T(8,128)}, u32[]{:S(2)}) copy-start(f32[8,16,64]{2,1,0:T(8,128)} %param.34) | copy-start | bytes 98308
  65.8 5.7 %copy-start.12 = (f32[2048]{0:T(1024)S(1)}, f32[2048]{0:T(1024)}, u32[]{:S(2)}) copy-start(f32[2048]{0:T(1024)} %param.20) | copy-start | bytes 24580
  65.8 43.8 %collective-permute-start.7 = (bf16[16,32,640]{2,1,0:T(8,128)(2,1)S(1)}, bf16[16,32,640]{2,1,0:T(8,128)(2,1)}, u32[]{:S(2)}, u32[]{:S(2)}) collective-permute-start(bf16[16,32,640]{2,1,0:T(8,128)(2,1)S(1)} %bitcast.29), channel_id=1, source_target_pairs={{0,24},{8,0},{16,8},{24,16},{32,56},{40,32},{48,40},{56,48},{64,88... | collective-permute-start | bytes 1966088 | tf_op jit(solution)/shard_map/ppermute | solution.py:341
  69.4 40.2 %collective-permute-start.8 = (bf16[16,32,640]{2,1,0:T(8,128)(2,1)S(1)}, bf16[16,32,640]{2,1,0:T(8,128)(2,1)}, u32[]{:S(2)}, u32[]{:S(2)}) collective-permute-start(bf16[16,32,640]{2,1,0:T(8,128)(2,1)S(1)} %bitcast.30), channel_id=1, source_target_pairs={{0,8},{8,16},{16,24},{24,0},{32,40},{40,48},{48,56},{56,32},{64,72... | collective-permute-start | bytes 1966088 | tf_op jit(solution)/shard_map/ppermute | solution.py:341
  80.6 6.8 %copy-start.4 = (f32[2,256,512]{2,1,0:T(8,128)}, f32[2,256,512]{2,1,0:T(8,128)S(1)}, u32[]{:S(2)}) copy-start(f32[2,256,512]{2,1,0:T(8,128)S(1)} %get-tuple-element.17.bar_ref) | copy-start | bytes 3145732
  82.3 27.3 %collective-permute-start.9 = (bf16[16,32,256]{2,1,0:T(8,128)(2,1)}, bf16[16,32,256]{2,1,0:T(8,128)(2,1)}, u32[]{:S(2)}, u32[]{:S(2)}) collective-permute-start(bf16[16,32,256]{2,1,0:T(8,128)(2,1)} %slice.24), channel_id=1, source_target_pairs={{0,480},{8,488},{16,496},{24,504},{32,0},{40,8},{48,16},{56,24},{6... | collective-permute-start | bytes 786440 | tf_op jit(solution)/shard_map/ppermute | solution.py:341
  87.4 22.2 %collective-permute-start.10 = (bf16[16,32,384]{2,1,0:T(8,128)(2,1)}, bf16[16,32,384]{2,1,0:T(8,128)(2,1)}, u32[]{:S(2)}, u32[]{:S(2)}) collective-permute-start(bf16[16,32,384]{2,1,0:T(8,128)(2,1)} %slice.25), channel_id=1, source_target_pairs={{0,32},{8,40},{16,48},{24,56},{32,64},{40,72},{48,80},{56,88},{64,... | collective-permute-start | bytes 1179656 | tf_op jit(solution)/shard_map/ppermute | solution.py:341
  89.3 1.2 copy-start.5
  90.6 1.2 copy-start.7
  95.9 20.2 %all-to-all-start.2 = ((f32[16,2,640]{2,1,0:T(2,128)}), f32[16,2,640]{2,1,0:T(2,128)S(1)}, u32[]{:S(2)}, u32[]{:S(2)}) async-start(f32[16,2,640]{2,1,0:T(2,128)} %broadcast_in_dim.34), calls=%async_computation.2 | async-start | bytes 163840 | tf_op jit(solution)/shard_map/all_to_all | solution.py:19
  104.9 4.7 %collective-permute-start = (bf16[16,2048]{1,0:T(8,128)(2,1)S(1)}, bf16[16,2048]{1,0:T(8,128)(2,1)S(1)}, u32[]{:S(2)}, u32[]{:S(2)}) collective-permute-start(bf16[16,2048]{1,0:T(8,128)(2,1)S(1)} %slice_bitcast_fusion), channel_id=1, source_target_pairs={{0,32},{32,64},{64,96},{96,128},{128,160},{160,192},{192,224},{224... | collective-permute-start | bytes 196616 | tf_op jit(solution)/shard_map/ppermute | solution.py:413
  108.2 1.4 copy-start.21
  108.3 7.8 %copy-start.9 = (bf16[2,128,1024]{2,1,0:T(8,128)(2,1)S(1)}, bf16[2,128,1024]{2,1,0:T(8,128)(2,1)}, u32[]{:S(2)}) copy-start(bf16[2,128,1024]{2,1,0:T(8,128)(2,1)} %copy-done.8) | copy-start | bytes 1572868
  113.9 2.2 %copy-start.16 = (f32[8,64]{1,0:T(8,128)S(1)}, f32[8,64]{1,0:T(8,128)}, u32[]{:S(2)}) copy-start(f32[8,64]{1,0:T(8,128)} %decay_ref.3) | copy-start | bytes 6148
  116.7 1.2 copy-start.1
  120.0 2.0 %copy-start.3 = (bf16[2048,256]{1,0:T(8,128)(2,1)S(1)}, bf16[2048,256]{1,0:T(8,128)(2,1)}, u32[]{:S(2)}) copy-start(bf16[2048,256]{1,0:T(8,128)(2,1)} %copy-done.2) | copy-start | bytes 3145732
  123.5 23.5 %all-to-all-start.3 = ((bf16[8,32,2048]{2,1,0:T(8,128)(2,1)}), bf16[8,32,2048]{2,1,0:T(8,128)(2,1)S(1)}, u32[]{:S(2)}, u32[]{:S(2)}) async-start(bf16[8,32,2048]{2,1,0:T(8,128)(2,1)} %bitcast.21), calls=%async_computation.3 | async-start | bytes 2097152 | tf_op jit(solution)/shard_map/all_to_all | solution.py:493
  (17 other events, 13.2 us)

commit v3 on v2

v3 whole, which is shorter than its diff:
```python
import functools

import jax
import jax.numpy as jnp
from jax import lax
from jax.experimental import pallas as pl
from jax.experimental.pallas import tpu as pltpu
from jax.sharding import PartitionSpec as P


F32 = jnp.float32
BF16 = jnp.bfloat16
CHUNKS = 8
HALO = 16
PACKED = 16
NT = (((1,), (1,)), ((), ()))


def spread(x, axis, groups=None):
    copies = lax.axis_size(axis) if groups is None else len(groups[0])
    many = jnp.broadcast_to(x[None], (copies, *x.shape))
    return lax.all_to_all(many, axis, 0, 0, tiled=True, axis_index_groups=groups)


def complex_product(left_real, left_imag, right_real, right_imag):
    return (
        left_real * right_real - left_imag * right_imag,
        left_real * right_imag + left_imag * right_real,
    )


def sine_cosine(angle):
    turns = jnp.floor(angle * 0.6366197723675814 + 0.5)
    r = angle - turns * 1.5703125
    r = r - turns * 4.837512969970703e-4
    r = r - turns * 7.549789948768648e-8
    r2 = r * r
    sine = r + r * r2 * (-1.6666654611e-1 + r2 * (8.3321608736e-3 + r2 * -1.9515295891e-4))
    cosine = (
        1.0
        - 0.5 * r2
        + r2 * r2 * (4.166664568298827e-2 + r2 * (-1.388731625493765e-3 + r2 * 2.443315711809948e-5))
    )
    quadrant = turns.astype(jnp.int32)
    odd = (quadrant & 1) == 1
    flip_sine = (quadrant & 2) == 2
    flip_cosine = ((quadrant + 1) & 2) == 2
    base_sine = jnp.where(odd, cosine, sine)
    base_cosine = jnp.where(odd, sine, cosine)
    return (
        jnp.where(flip_sine, -base_sine, base_sine),
        jnp.where(flip_cosine, -base_cosine, base_cosine),
    )


def iota(dims, axis):
    return lax.broadcasted_iota(jnp.int32, dims, axis)


def pieces(x, count):
    found = []
    for _ in range(count):
        part = x.astype(BF16)
        found.append(part)
        x = x - part.astype(F32)
    return found


def picked(x, selector, count=3):
    total = None
    for part in pieces(x, count):
        term = jnp.dot(part, selector, preferred_element_type=F32)
        total = term if total is None else total + term
    return total


def repeat_selector(narrow, wide):
    return (iota((narrow, wide), 1) % narrow == iota((narrow, wide), 0)).astype(BF16)


def flattened(x, groups):
    rows, narrow = x.shape
    wide = groups * narrow
    tiled = picked(x, repeat_selector(narrow, wide))
    own = iota((rows, wide), 1) // narrow == iota((rows, wide), 0) % groups
    tiled = jnp.where(own, tiled, 0.0)
    return [jnp.sum(tiled[at : at + groups], axis=0, keepdims=True) for at in range(0, rows, groups)]


def block_diagonal(x, groups):
    rows, narrow = x.shape
    wide = groups * narrow
    selector = repeat_selector(narrow, wide)
    own = iota((rows, wide), 1) // narrow == iota((rows, wide), 0) // (rows // groups)
    return [
        jnp.where(own, jnp.dot(part, selector, preferred_element_type=F32), 0.0).astype(BF16)
        for part in pieces(x, 2)
    ]


def spread_steps(log_ref, groups, states):
    lane = iota((1, groups * states), 1) // states
    out = jnp.zeros((1, groups * states), F32)
    for g in range(groups):
        out = jnp.where(lane == g, log_ref[g], out)
    return jnp.exp(out)


def chunk_order(rows, flip):
    r, c = (iota((rows, rows), 1 if flip else 0), iota((rows, rows), 0 if flip else 1))
    steps = rows // CHUNKS
    return (c == (r % CHUNKS) * steps + r // CHUNKS).astype(BF16)


def normalized(x, gain):
    x = x.astype(F32)
    mean_square = jnp.mean(x * x, axis=-1, keepdims=True)
    return (x * lax.rsqrt(mean_square + 1e-06) * gain).astype(BF16)


def prep_kernel(
    log_ref, tokens_ref, gain_ref, rate_ref, decay_ref, freq_ref, initial_ref, in_real_ref, in_imag_ref,
    out_real_ref, out_imag_ref, skip_ref, taps_ref, normed_ref, bar_ref, pack_ref, column_ref,
):
    groups, states = decay_ref.shape
    flat = groups * states
    rows = tokens_ref.shape[0]
    part = 64

    def norm(i, _):
        at = pl.ds(pl.multiple_of(i * part, part), part)
        normed_ref[at, :] = normalized(tokens_ref[at, :], gain_ref[...])
        return 0

    lax.fori_loop(0, rows // part, norm, 0)
    order = chunk_order(rows, False)
    column = None
    for piece in pieces(jnp.broadcast_to(rate_ref[...], (16, rows)), 3):
        term = lax.dot_general(order, piece, NT, preferred_element_type=F32)
        column = term if column is None else column + term
    column_ref[...] = column
    (decay,) = flattened(decay_ref[...], groups)
    (freq,) = flattened(freq_ref[...], groups)
    scale = spread_steps(log_ref, groups, states)
    for at, ref in enumerate((in_real_ref, in_imag_ref, out_real_ref, out_imag_ref)):
        pack_ref[: ref.shape[0], at * states : (at + 1) * states] = ref[...]
    width = taps_ref.shape[1]
    (skip,) = flattened(skip_ref[...], groups)
    gain_rows = gain_ref.shape[1] // flat
    for at, row in enumerate(
        (
            decay,
            freq,
            scale,
            *flattened(initial_ref[...], groups),
            *(gain_ref[:, i * flat : (i + 1) * flat] for i in range(gain_rows)),
            skip,
            *(taps_ref[i : i + 1] for i in range(taps_ref.shape[0])),
        )
    ):
        pack_ref[width + at : width + at + 1, : row.shape[1]] = row
    steps = rows // CHUNKS

    def advance(j, carry):
        at = pl.ds(pl.multiple_of(j * CHUNKS, CHUNKS), CHUNKS)
        step = column_ref[at, 0:1] * scale
        grow = jnp.exp(step * decay)
        sine, cosine = sine_cosine(step * freq)
        bar_real, bar_imag = (grow * cosine, grow * sine)
        bar_ref[0, at, :] = bar_real
        bar_ref[1, at, :] = bar_imag
        return 0

    lax.fori_loop(0, steps, advance, 0)


def packed(pack_ref, at, wide=None):
    top = pack_ref.shape[0] - PACKED
    return pack_ref[top + at : top + at + 1, : pack_ref.shape[1] if wide is None else wide]


def matrix(pack_ref, at, states):
    return pack_ref[: pack_ref.shape[0] - PACKED, at * states : (at + 1) * states]


def driven(chan, pack_ref, bar_ref, groups, push_ref):
    flat = bar_ref.shape[2]
    drives = []
    for at in range(2):
        high, low = block_diagonal(matrix(pack_ref, at, flat // groups), groups)
        drives.append(
            jnp.dot(chan, high, preferred_element_type=F32) + jnp.dot(chan, low, preferred_element_type=F32)
        )
    decay, freq = (packed(pack_ref, 0), packed(pack_ref, 1))
    inverse = 1.0 / (decay * decay + freq * freq)
    bar_imag = bar_ref[1]
    less_real = bar_ref[0] - 1.0
    push_ref[0], push_ref[1] = complex_product(
        (less_real * decay + bar_imag * freq) * inverse,
        (bar_imag * decay - less_real * freq) * inverse,
        drives[0],
        drives[1],
    )


def scanned(bar_ref, push_ref, start):
    steps = bar_ref.shape[1] // CHUNKS

    def advance(j, carry):
        at = pl.ds(pl.multiple_of(j * CHUNKS, CHUNKS), CHUNKS)
        real, imag = complex_product(bar_ref[0, at, :], bar_ref[1, at, :], carry[0], carry[1])
        real = real + push_ref[0, at, :]
        imag = imag + push_ref[1, at, :]
        push_ref[0, at, :] = real
        push_ref[1, at, :] = imag
        return (real, imag)

    lax.fori_loop(0, steps, advance, start, unroll=4)


def chunk_maps(bar_ref, push_ref):
    steps, flat = (bar_ref.shape[1] // CHUNKS, bar_ref.shape[2])

    def advance(j, carry):
        at = pl.ds(pl.multiple_of(j * CHUNKS, CHUNKS), CHUNKS)
        bar = (bar_ref[0, at, :], bar_ref[1, at, :])
        product = complex_product(*bar, carry[0], carry[1])
        real, imag = complex_product(*bar, carry[2], carry[3])
        return (*product, real + push_ref[0, at, :], imag + push_ref[1, at, :])

    one, zero = (jnp.ones((CHUNKS, flat), F32), jnp.zeros((CHUNKS, flat), F32))
    return lax.fori_loop(0, steps, advance, (one, zero, zero, zero), unroll=4)


def local_kernel(
    groups, normed_ref, w_ref, bar_ref, pack_ref, rate_ref, chan_ref, end_ref, push_ref
):
    rows = normed_ref.shape[0]
    near, fs, far = w_ref.shape[:3]
    w = jnp.concatenate(
        [w_ref[zb, y, za] for za in range(far) for zb in range(near) for y in range(fs)], axis=0
    )
    state_in = jnp.dot(normed_ref[...], w, preferred_element_type=F32).astype(BF16)
    chan = jnp.dot(chunk_order(rows, False), state_in, preferred_element_type=F32).astype(BF16)
    chan_ref[...] = chan
    flat = bar_ref.shape[2]
    driven(chan, pack_ref, bar_ref, groups, push_ref)
    end_real, end_imag, last_real, last_imag = chunk_maps(bar_ref, push_ref)
    real, imag = (last_real[0:1], last_imag[0:1])
    for c in range(1, CHUNKS):
        moved_real, moved_imag = complex_product(end_real[c : c + 1], end_imag[c : c + 1], real, imag)
        real = moved_real + last_real[c : c + 1]
        imag = moved_imag + last_imag[c : c + 1]
    end_ref[:, :flat] = jnp.concatenate([real, imag], axis=0)
    whole = jnp.sum(rate_ref[...], axis=1, keepdims=True)
    end_ref[:, flat:] = jnp.broadcast_to(whole, (2, end_ref.shape[1] - flat))


def gelu(v):
    return 0.5 * v * (1.0 + jnp.tanh(0.7978845608 * (v + 0.044715 * v * v * v)))


def read_kernel(
    groups, ends_ref, bar_ref, chan_ref, pack_ref, mix_ref, closing_ref, push_ref
):
    flat = bar_ref.shape[2]
    states = flat // groups
    spans = ends_ref.shape[0]
    here = lax.axis_index("sp")
    decay, freq, scale, enter_real, enter_imag = (packed(pack_ref, at) for at in range(5))
    real, imag = (enter_real, enter_imag)
    elapsed = jnp.concatenate([ends_ref[z, 0:1, flat:] for z in range(spans)], axis=0)[:, 0:1] * scale
    grow = jnp.exp(elapsed * decay)
    sine, cosine = sine_cosine(elapsed * freq)
    map_real, map_imag = (grow * cosine, grow * sine)
    for z in range(spans):
        now = here == z
        enter_real = jnp.where(now, real, enter_real)
        enter_imag = jnp.where(now, imag, enter_imag)
        moved_real, moved_imag = complex_product(map_real[z : z + 1], map_imag[z : z + 1], real, imag)
        real = moved_real + ends_ref[z, 0:1, :flat]
        imag = moved_imag + ends_ref[z, 1:2, :flat]
    share = states // spans
    lane = iota((flat, share), 0) % states
    wanted = (lane == here * share + iota((flat, share), 1)).astype(BF16)
    own = iota((groups, flat), 1) // states == iota((groups, flat), 0)
    for at, row in enumerate((real, imag)):
        closing_ref[at] = picked(jnp.where(own, jnp.broadcast_to(row, (groups, flat)), 0.0), wanted)
    rows = bar_ref.shape[1]
    chan = chan_ref[...]
    driven(chan, pack_ref, bar_ref, groups, push_ref)
    end_real, end_imag, last_real, last_imag = chunk_maps(bar_ref, push_ref)
    in_real, in_imag = ([enter_real], [enter_imag])
    for c in range(CHUNKS - 1):
        moved_real, moved_imag = complex_product(
            end_real[c : c + 1], end_imag[c : c + 1], in_real[-1], in_imag[-1]
        )
        in_real.append(moved_real + last_real[c : c + 1])
        in_imag.append(moved_imag + last_imag[c : c + 1])
    scanned(bar_ref, push_ref, (jnp.concatenate(in_real, axis=0), jnp.concatenate(in_imag, axis=0)))
    response = None
    for at, sign in enumerate((1.0, -1.0)):
        weights = block_diagonal(matrix(pack_ref, 2 + at, states) * sign, groups)
        high, low = pieces(push_ref[at], 2)
        for left, right in ((high, 0), (low, 0), (high, 1)):
            term = lax.dot_general(left, weights[right], NT, preferred_element_type=F32)
            response = term if response is None else response + term
    skip = packed(pack_ref, 9, mix_ref.shape[1])
    mixed = gelu(response + skip * chan.astype(F32)).astype(BF16)
    mix_ref[...] = jnp.dot(chunk_order(rows, True), mixed, preferred_element_type=F32).astype(BF16)


def conv_kernel(
    normed_ref, halo_ref, own_ref, up_ref, down_ref, left_ref, right_ref, pack_ref, mix_ref, weights_ref, w_ref
):
    width = mix_ref.shape[1]
    rows = normed_ref.shape[0]
    near, far, tall, _ = own_ref.shape
    split = w_ref.shape[1]
    z, y = (lax.axis_index("sp"), lax.axis_index("fs"))

    def put(j, turn, ref, at_j):
        for k in range(far):
            at_z = 4 * k + ((z + j) & 3)
            at_y = (y + 2 * j + turn) & 3
            at = pl.ds(pl.multiple_of((at_z * 4 + at_y) * tall, tall), tall)
            w_ref[at, :] = ref[at_j, k, :, :split]
            weights_ref[at, :] = ref[at_j, k, :, split:]

    for j in range(near):
        put(j, 0, own_ref, j)
        put(j, 1, up_ref, j)
        put(j, 3, down_ref, j)
    for j in range(near // 2):
        put(j + 1, 2, left_ref, j)
        put(j - 1, 2, right_ref, j)
    w = w_ref[...]
    taps = [packed(pack_ref, 10 + at, width) for at in range(3)]
    gain = jnp.concatenate([packed(pack_ref, 5 + at) for at in range(4)], axis=1)
    reach = len(taps) - 1
    here = jnp.dot(normed_ref[...], w, preferred_element_type=F32).astype(BF16).astype(F32)
    halo = normalized(halo_ref[...], gain)
    before = jnp.dot(halo, w[:, : 2 * width], preferred_element_type=F32).astype(BF16).astype(F32)
    gated = (here[:, :width] * here[:, width : 2 * width]).astype(BF16).astype(F32)
    gated_before = (before[:, :width] * before[:, width:]).astype(BF16).astype(F32)
    extended = jnp.concatenate([gated_before, gated], axis=0)
    filtered = taps[reach] * gated
    for tap in range(reach):
        at = HALO - reach + tap
        filtered = filtered + taps[tap] * extended[at : at + rows]
    mix_ref[...] = (here[:, 2 * width :] * filtered).astype(BF16)


def out_kernel(state_ref, conv_ref, w_ref, out_ref):
    mixes = jnp.concatenate([state_ref[...], conv_ref[...]], axis=1)
    per = 512
    for at in range(0, w_ref.shape[0], per):
        product = lax.dot_general(mixes, w_ref[at : at + per], NT, preferred_element_type=F32)
        out_ref[:, at : at + per] = product.astype(BF16)


def moved(x, dz, dy):
    sp, fs = (lax.axis_size("sp"), lax.axis_size("fs"))
    pairs = [
        (z * fs + y, ((z - dz) % sp) * fs + (y - dy) % fs) for z in range(sp) for y in range(fs)
    ]
    return lax.ppermute(x, ("sp", "fs"), pairs)


def all_shards(far):
    near = [far] + [moved(far, dz, dy) for dz, dy in ((1, 2), (2, 0), (-1, 2))]
    own = jnp.stack(near)
    half = own[:2]
    return (own, moved(own, 0, 1), moved(own, 0, -1), moved(half, 1, 0), moved(half, -1, 0))


def call(kernel, out_shape, flops, *args, smem=0, scratch=()):
    vmem = pl.BlockSpec(memory_space=pltpu.VMEM)
    return pl.pallas_call(
        kernel,
        out_shape=out_shape,
        in_specs=[pl.BlockSpec(memory_space=pltpu.SMEM)] * smem + [vmem] * (len(args) - smem),
        out_specs=jax.tree.map(lambda _: vmem, out_shape),
        scratch_shapes=list(scratch),
        cost_estimate=pl.CostEstimate(flops=flops, bytes_accessed=1 << 20, transcendentals=0),
        compiler_params=pltpu.CompilerParams(vmem_limit_bytes=20 << 20),
    )(*args)


def shape(dims, dtype=F32):
    return jax.ShapeDtypeStruct(dims, dtype)


def body(
    tokens,
    norm_gain,
    w_state_in,
    w_value,
    w_outer,
    w_inner,
    w_state_out,
    w_conv_out,
    log_step,
    decay_real,
    frequency,
    step_rate,
    input_real,
    input_imag,
    read_real,
    read_imag,
    skip_gain,
    conv_taps,
    initial_state,
):
    rows, features = tokens.shape[1:]
    groups, states = decay_real.shape
    group = skip_gain.shape[1]
    flat = groups * states
    width = groups * group
    count = lax.axis_size("sp")

    fs = lax.axis_size("fs")
    shards = jnp.concatenate([w_state_in, w_value, w_inner, w_outer, w_state_out, w_conv_out], axis=1)
    apart = [[zb + 4 * za for za in range(count // 4)] for zb in range(4)]
    far = spread(shards, "sp", apart)
    block = 4 * fs
    blocks = [[at + i for i in range(block)] for at in range(0, count * fs, block)]
    state_weights = spread(far[:, :, :width], ("sp", "fs"), blocks)
    state_weights = state_weights.reshape(4, fs, *state_weights.shape[1:])
    own, up, down, left, right = all_shards(far[:, :, width:])
    edge = lax.ppermute(tokens[0, rows - HALO :], "sp", [(i, i + 1) for i in range(count - 1)])
    gain = norm_gain[None]
    into = [jnp.swapaxes(x, 1, 2).reshape(width, states) for x in (input_real, input_imag)]
    normed, bar, pack = call(
        prep_kernel,
        (shape((rows, features), BF16), shape((2, rows, flat)), shape((width + PACKED, flat))),
        1 << 30,
        log_step,
        tokens[0],
        gain,
        step_rate,
        decay_real,
        frequency,
        initial_state[0].reshape(2 * groups, states),
        *into,
        read_real.reshape(width, states),
        read_imag.reshape(width, states),
        skip_gain,
        conv_taps,
        smem=1,
        scratch=(pltpu.VMEM((rows, 16), F32),),
    )
    chan, end = call(
        functools.partial(local_kernel, groups),
        (shape((rows, width), BF16), shape((2, flat + 128))),
        1 << 29,
        normed,
        state_weights,
        bar,
        pack,
        step_rate,
        scratch=(pltpu.VMEM((2, rows, flat), F32),),
    )
    ends = spread(end, "sp")
    conv_mix, out_weights = call(
        conv_kernel,
        (shape((rows, width), BF16), shape((features, 2 * width), BF16)),
        1 << 29,
        normed,
        edge,
        own,
        up,
        down,
        left,
        right,
        pack,
        scratch=(pltpu.VMEM((features, 3 * width), BF16),),
    )
    state_mix, closing = call(
        functools.partial(read_kernel, groups),
        (shape((rows, width), BF16), shape((2, groups, states // count))),
        1 << 29,
        ends,
        bar,
        chan,
        pack,
        scratch=(pltpu.VMEM((2, rows, flat), F32),),
    )
    partial = call(
        out_kernel, shape((rows, features), BF16), 1 << 29, state_mix, conv_mix, out_weights
    )
    tp = lax.axis_size("tp")
    parts = lax.all_to_all(partial.reshape(tp, rows // tp, features), "tp", 0, 0, tiled=True)
    mixed = jnp.sum(parts.astype(F32), axis=0).astype(BF16)
    return (mixed[None], closing[None])


def solution(mesh):
    return jax.shard_map(
        body,
        mesh=mesh,
        in_specs=(
            P("fs", "sp", None),
            P(),
            P(("sp", "fs"), "tp"),
            P(("sp", "fs"), "tp"),
            P(("sp", "fs"), "tp"),
            P(("sp", "fs"), "tp"),
            P(("sp", "fs"), "tp"),
            P(("sp", "fs"), "tp"),
            P("tp"),
            P("tp", None),
            P("tp", None),
            P("fs", "sp"),
            P("tp", None, None),
            P("tp", None, None),
            P("tp", None, None),
            P("tp", None, None),
            P("tp", None),
            P(None, "tp"),
            P("fs", None, "tp", None),
        ),
        out_specs=(P("fs", ("sp", "tp"), None), P("fs", None, "tp", "sp")),
        check_vma=False,
    )
```

time: 149 us -> 132 us (0.89)
  starting transfers between devices: 85.3 us -> 50.9 us
  blocking collectives: 0 us -> 28.5 us
  local copies, waits for them, and re-layouts: 22.3 us -> 11.3 us
    all_to_all x0 -> x1, blocking collectives: none -> 28.5 us  [spread(): lax.all_to_all(many, axis, 0, 0, tiled=True, axis_index_groups=groups)]
    ppermute x10 -> x7, starting transfers between devices: 45.4 us -> 24.4 us  [moved(): return lax.ppermute(x, ('sp', 'fs'), pairs)]
    all_to_all x3 -> x2, starting transfers between devices: 28.2 us -> 14.3 us  [spread(): lax.all_to_all(many, axis, 0, 0, tiled=True, axis_index_groups=groups)]
    unnamed x72 -> x55, local copies, waits for them, and re-layouts: 16.1 us -> 8.18 us
    slice x4 -> x1, local copies, waits for them, and re-layouts: 1.63 us -> 0.01 us  [body(): state_weights = spread(far[:, :, :width], ('sp', 'fs'), blocks)]
    ppermute x10 -> x7, waiting for transfers between devices: 6.84 us -> 5.66 us  [moved(): return lax.ppermute(x, ('sp', 'fs'), pairs)]
  transfers between devices with their start and end apart: 15 -> 11, of which waited for: 5 -> 5; matrix products, arithmetic and copies ran while one was open for 3% -> 2% of each run, Pallas kernels for 7% -> 7%
where the time goes in v3:
time: 132 us; the launch traced here: 131 us
  starting transfers between devices  50.9 us (39%)
  blocking collectives  28.5 us (22%)
  waiting for transfers between devices  24.3 us (18%)
  Pallas kernels  12.9 us (10%)
  local copies, waits for them, and re-layouts  11.3 us (9%)
  other arithmetic  1.68 us (1%)
    all_to_all x1, blocking collectives, spread(): lax.all_to_all(many, axis, 0, 0, tiled=True, axis_index_groups=groups)  28.5 us
    ppermute x7, starting transfers between devices, moved(): return lax.ppermute(x, ('sp', 'fs'), pairs)  24.4 us
    all_to_all x1, waiting for transfers between devices, body(): lax.all_to_all(partial.reshape(tp, rows // tp, features), 'tp', 0, 0, til...  14.3 us
    all_to_all x2, starting transfers between devices, spread(): lax.all_to_all(many, axis, 0, 0, tiled=True, axis_index_groups=groups)  14.3 us
    pallas_call x5, Pallas kernels, call(): pl.pallas_call(kernel, out_shape=out_shape, in_specs=[pl.BlockSpec(memory...  12.9 us
    all_to_all x1, starting transfers between devices, body(): lax.all_to_all(partial.reshape(tp, rows // tp, features), 'tp', 0, 0, til...  8.86 us
    unnamed x55, local copies, waits for them, and re-layouts  8.18 us
    ppermute x7, waiting for transfers between devices, moved(): return lax.ppermute(x, ('sp', 'fs'), pairs)  5.66 us
  transfers between devices with their start and end apart: 11, of which 5 were waited for; matrix products, arithmetic and copies ran while one was open for 2% of the time, Pallas kernels for 7%

profile of v3, /device:TPU:1, one launch (start us, length us, event | category | flops | bytes accessed | tf_op | source)
XLA Modules:
  0.0 130.6 jit_solution(7133981376388828036)
XLA Ops:
  0.6 0.7 constant_dynamic-update-slice_fusion.5
  1.4 0.7 copy-done.21
  2.8 0.7 copy-done.23
  4.2 28.5 %all_to_all.20 = bf16[4,32,768]{2,1,0:T(8,128)(2,1)S(1)} all-to-all(bf16[4,32,768]{2,1,0:T(8,128)(2,1)S(1)} %broadcast_in_dim.13), channel_id=1, replica_groups={{0,128,256,384},{32,160,288,416},{64,192,320,448},{96,224,352,480},{1,1..., dimensions={0} | all-to-all | bytes 393216 | tf_op jit(solution)/shard_map/all_to_all | solution.py:22
  32.7 0.9 broadcast_in_dim.14
  33.6 9.6 %all-to-all-start.1 = ((bf16[16,4,32,128]{3,2,1,0:T(8,128)(2,1)}), bf16[16,4,32,128]{3,2,1,0:T(8,128)(2,1)S(1)}, u32[]{:S(2)}, u32[]{:S(2)}) async-start(bf16[16,4,32,128]{3,2,1,0:T(8,128)(2,1)} %broadcast_in_dim.14), calls=%async_computation.1 | async-start | bytes 1048576 | tf_op jit(solution)/shard_map/all_to_all | solution.py:22
  43.3 5.8 %collective-permute-start.3 = (bf16[4,32,640]{2,1,0:T(8,128)(2,1)S(1)}, bf16[4,32,640]{2,1,0:T(8,128)(2,1)S(1)}, u32[]{:S(2)}, u32[]{:S(2)}) collective-permute-start(bf16[4,32,640]{2,1,0:T(8,128)(2,1)S(1)} %get-tuple-element.21), channel_id=1, source_target_pairs={{0,48},{8,56},{16,32},{24,40},{32,80},{40,88},{48,64},{56,72},{64,... | collective-permute-start | bytes 491528 | tf_op jit(solution)/shard_map/ppermute | solution.py:367
  49.2 3.8 %collective-permute-start.2 = (bf16[4,32,640]{2,1,0:T(8,128)(2,1)S(1)}, bf16[4,32,640]{2,1,0:T(8,128)(2,1)S(1)}, u32[]{:S(2)}, u32[]{:S(2)}) collective-permute-start(bf16[4,32,640]{2,1,0:T(8,128)(2,1)S(1)} %get-tuple-element.21), channel_id=1, source_target_pairs={{0,448},{8,456},{16,464},{24,472},{32,480},{40,488},{48,496},{56,5... | collective-permute-start | bytes 491528 | tf_op jit(solution)/shard_map/ppermute | solution.py:367
  53.0 2.2 %collective-permute-start.1 = (bf16[4,32,640]{2,1,0:T(8,128)(2,1)S(1)}, bf16[4,32,640]{2,1,0:T(8,128)(2,1)S(1)}, u32[]{:S(2)}, u32[]{:S(2)}) collective-permute-start(bf16[4,32,640]{2,1,0:T(8,128)(2,1)S(1)} %get-tuple-element.21), channel_id=1, source_target_pairs={{0,496},{8,504},{16,480},{24,488},{32,16},{40,24},{48,0},{56,8},{6... | collective-permute-start | bytes 491528 | tf_op jit(solution)/shard_map/ppermute | solution.py:367
  55.9 4.6 %shard_map.194 = (bf16[256,2048]{1,0:T(8,128)(2,1)S(1)}, f32[2,256,512]{2,1,0:T(8,128)S(1)}, f32[144,512]{1,0:T(8,128)S(1)}) custom-call(f32[8]{0:T(128)S(1)} %copy-done.19, bf16[256,2048]{1,0:T(8,128)(2,1)S(1)} %bitcast.23, f32[1,2048]{1,0:T(1,128)S(1)} %bitcast.28, f32[1,256]{1,0:T(1,128)S(1)} %copy-done.6, f32[8,64]{1,0:T(8,128)S(1)} %copy-done.15, ...), custom_call_target="tpu_custom_call" | custom-call | flops 1073741824 | bytes 1048576 | tf_op jit(solution)/shard_map/pallas_call | solution.py:379
  60.6 2.0 %collective-permute-done.2 = bf16[4,32,640]{2,1,0:T(8,128)(2,1)S(1)} collective-permute-done((bf16[4,32,640]{2,1,0:T(8,128)(2,1)S(1)}, bf16[4,32,640]{2,1,0:T(8,128)(2,1)S(1)}, u32[]{:S(2)}, u32[]{:S(2)}) %collective-permute-start.2) | collective-permute-done | bytes 163872 | tf_op jit(solution)/shard_map/ppermute | solution.py:367
  62.6 3.6 %collective-permute-done.1 = bf16[4,32,640]{2,1,0:T(8,128)(2,1)S(1)} collective-permute-done((bf16[4,32,640]{2,1,0:T(8,128)(2,1)S(1)}, bf16[4,32,640]{2,1,0:T(8,128)(2,1)S(1)}, u32[]{:S(2)}, u32[]{:S(2)}) %collective-permute-start.1) | collective-permute-done | bytes 163872 | tf_op jit(solution)/shard_map/ppermute | solution.py:367
  66.3 2.7 %collective-permute-start.4 = (bf16[4,4,32,640]{3,2,1,0:T(8,128)(2,1)S(1)}, bf16[4,4,32,640]{3,2,1,0:T(8,128)(2,1)S(1)}, u32[]{:S(2)}, u32[]{:S(2)}) collective-permute-start(bf16[4,4,32,640]{3,2,1,0:T(8,128)(2,1)S(1)} %pad_maximum_fusion.own_ref), channel_id=1, source_target_pairs={{0,24},{8,0},{16,8},{24,16},{32,56},{40,32},{48,40},{56,48},{64,88... | collective-permute-start | bytes 1966088 | tf_op jit(solution)/shard_map/ppermute | solution.py:367
  69.0 2.6 %collective-permute-start.5 = (bf16[4,4,32,640]{3,2,1,0:T(8,128)(2,1)S(1)}, bf16[4,4,32,640]{3,2,1,0:T(8,128)(2,1)}, u32[]{:S(2)}, u32[]{:S(2)}) collective-permute-start(bf16[4,4,32,640]{3,2,1,0:T(8,128)(2,1)S(1)} %pad_maximum_fusion.own_ref), channel_id=1, source_target_pairs={{0,8},{8,16},{16,24},{24,0},{32,40},{40,48},{48,56},{56,32},{64,72... | collective-permute-start | bytes 1966088 | tf_op jit(solution)/shard_map/ppermute | solution.py:367
  71.6 0.8 pad_maximum_fusion.1
  72.4 2.1 %collective-permute-start.6 = (bf16[2,4,32,640]{3,2,1,0:T(8,128)(2,1)}, bf16[2,4,32,640]{3,2,1,0:T(8,128)(2,1)S(1)}, u32[]{:S(2)}, u32[]{:S(2)}) collective-permute-start(bf16[2,4,32,640]{3,2,1,0:T(8,128)(2,1)} %pad_maximum_fusion.1), channel_id=1, source_target_pairs={{0,480},{8,488},{16,496},{24,504},{32,0},{40,8},{48,16},{56,24},{6... | collective-permute-start | bytes 983048 | tf_op jit(solution)/shard_map/ppermute | solution.py:367
  74.5 5.2 %collective-permute-start.7 = (bf16[2,4,32,640]{3,2,1,0:T(8,128)(2,1)}, bf16[2,4,32,640]{3,2,1,0:T(8,128)(2,1)}, u32[]{:S(2)}, u32[]{:S(2)}) collective-permute-start(bf16[2,4,32,640]{3,2,1,0:T(8,128)(2,1)} %pad_maximum_fusion.1), channel_id=1, source_target_pairs={{0,32},{8,40},{16,48},{24,56},{32,64},{40,72},{48,80},{56,88},{64,... | collective-permute-start | bytes 983048 | tf_op jit(solution)/shard_map/ppermute | solution.py:367
  79.7 1.2 copy-done.1
  80.9 1.7 %shard_map.195 = (bf16[256,128]{1,0:T(8,128)(2,1)S(1)}, f32[2,640]{1,0:T(2,128)S(1)}) custom-call(bf16[256,2048]{1,0:T(8,128)(2,1)S(1)} %get-tuple-element.11.normed_ref, bf16[4,4,4,32,128]{4,3,2,1,0:T(8,128)(2,1)S(1)} %bitcast.22, f32[2,256,512]{2,1,0:T(8,128)S(1)} %copy-done.1, f32[144,512]{1,0:T(8,128)S(1)} %get-tuple-element.13.pack_ref, ...), custom_call_target="tpu_custom_call" | custom-call | flops 536870912 | bytes 1048576 | tf_op jit(solution)/shard_map/pallas_call | solution.py:379
  83.9 4.7 %all-to-all-start.2 = ((f32[16,2,640]{2,1,0:T(2,128)}), f32[16,2,640]{2,1,0:T(2,128)S(1)}, u32[]{:S(2)}, u32[]{:S(2)}) async-start(f32[16,2,640]{2,1,0:T(2,128)} %broadcast_in_dim.30), calls=%async_computation.2 | async-start | bytes 163840 | tf_op jit(solution)/shard_map/all_to_all | solution.py:22
  88.6 0.8 slice_bitcast_fusion
  89.4 3.4 %collective-permute-start = (bf16[16,2048]{1,0:T(8,128)(2,1)S(1)}, bf16[16,2048]{1,0:T(8,128)(2,1)S(1)}, u32[]{:S(2)}, u32[]{:S(2)}) collective-permute-start(bf16[16,2048]{1,0:T(8,128)(2,1)S(1)} %slice_bitcast_fusion), channel_id=1, source_target_pairs={{0,32},{32,64},{64,96},{96,128},{128,160},{160,192},{192,224},{224... | collective-permute-start | bytes 196616 | tf_op jit(solution)/shard_map/ppermute | solution.py:431
  92.8 1.4 %collective-permute-done.halo_ref = bf16[16,2048]{1,0:T(8,128)(2,1)S(1)} collective-permute-done((bf16[16,2048]{1,0:T(8,128)(2,1)S(1)}, bf16[16,2048]{1,0:T(8,128)(2,1)S(1)}, u32[]{:S(2)}, u32[]{:S(2)}) %collective-permute-start) | collective-permute-done | bytes 65568 | tf_op jit(solution)/shard_map/ppermute | solution.py:431
  94.2 2.2 %shard_map.197 = (bf16[256,128]{1,0:T(8,128)(2,1)S(1)}, bf16[2048,256]{1,0:T(8,128)(2,1)S(1)}) custom-call(bf16[256,2048]{1,0:T(8,128)(2,1)S(1)} %get-tuple-element.11.normed_ref, bf16[16,2048]{1,0:T(8,128)(2,1)S(1)} %collective-permute-done.halo_ref, bf16[4,4,32,640]{3,2,1,0:T(8,128)(2,1)S(1)} %pad_maximum_fusion.own_ref, ...), custom_call_target="tpu_custom_call" | custom-call | flops 536870912 | bytes 1048576 | tf_op jit(solution)/shard_map/pallas_call | solution.py:379
  96.5 1.0 copy-done.3
  97.5 2.9 %all-to-all-done.2.ends_ref = f32[16,2,640]{2,1,0:T(2,128)S(1)} async-done(((f32[16,2,640]{2,1,0:T(2,128)}), f32[16,2,640]{2,1,0:T(2,128)S(1)}, u32[]{:S(2)}, u32[]{:S(2)}) %all-to-all-start.2) | async-done | bytes 81952 | tf_op jit(solution)/shard_map/all_to_all | solution.py:22
  100.4 1.2 copy-done.2
  101.6 2.9 %shard_map.196 = (bf16[256,128]{1,0:T(8,128)(2,1)S(1)}, f32[2,8,4]{2,1,0:T(8,128)S(1)}) custom-call(f32[16,2,640]{2,1,0:T(2,128)S(1)} %all-to-all-done.2.ends_ref, f32[2,256,512]{2,1,0:T(8,128)S(1)} %copy-done.2, bf16[256,128]{1,0:T(8,128)(2,1)S(1)} %copy-done.12, f32[144,512]{1,0:T(8,128)S(1)} %get-tuple-element.13.pack_ref), custom_call_target="tpu_custom_call" | custom-call | flops 536870912 | bytes 1048576 | tf_op jit(solution)/shard_map/pallas_call | solution.py:379
  104.5 1.5 %shard_map.198 = bf16[256,2048]{1,0:T(8,128)(2,1)} custom-call(bf16[256,128]{1,0:T(8,128)(2,1)S(1)} %get-tuple-element.16.state_ref, bf16[256,128]{1,0:T(8,128)(2,1)S(1)} %get-tuple-element.17.conv_ref, bf16[2048,256]{1,0:T(8,128)(2,1)S(1)} %copy-done.4), custom_call_target="tpu_custom_call" | custom-call | flops 536870912 | bytes 1048576 | tf_op jit(solution)/shard_map/pallas_call | solution.py:379
  106.0 8.9 %all-to-all-start.3 = ((bf16[8,32,2048]{2,1,0:T(8,128)(2,1)}), bf16[8,32,2048]{2,1,0:T(8,128)(2,1)S(1)}, u32[]{:S(2)}, u32[]{:S(2)}) async-start(bf16[8,32,2048]{2,1,0:T(8,128)(2,1)} %bitcast.15), calls=%async_computation.3 | async-start | bytes 2097152 | tf_op jit(solution)/shard_map/all_to_all | solution.py:493
  115.5 14.3 %all-to-all-done.3 = bf16[8,32,2048]{2,1,0:T(8,128)(2,1)S(1)} async-done(((bf16[8,32,2048]{2,1,0:T(8,128)(2,1)}), bf16[8,32,2048]{2,1,0:T(8,128)(2,1)S(1)}, u32[]{:S(2)}, u32[]{:S(2)}) %all-to-all-start.3) | async-done | bytes 1048608 | tf_op jit(solution)/shard_map/all_to_all | solution.py:493
  129.8 0.8 reduce_sum.12
  (62 shorter events, 4.2 us)
Async XLA Ops:
  0.6 0.7 copy-start.20
  1.3 0.7 copy-start.21
  2.0 0.7 copy-start.22
  2.7 0.7 copy-start.23
  3.4 0.7 copy-start.24
  32.7 22.5 %copy-start.5 = (bf16[1,256,2048]{2,1,0:T(8,128)(2,1)S(1)}, bf16[1,256,2048]{2,1,0:T(8,128)(2,1)}, u32[]{:S(2)}) copy-start(bf16[1,256,2048]{2,1,0:T(8,128)(2,1)} %param.19) | copy-start | bytes 3145732
  33.6 46.0 %all-to-all-start.1 = ((bf16[16,4,32,128]{3,2,1,0:T(8,128)(2,1)}), bf16[16,4,32,128]{3,2,1,0:T(8,128)(2,1)S(1)}, u32[]{:S(2)}, u32[]{:S(2)}) async-start(bf16[16,4,32,128]{3,2,1,0:T(8,128)(2,1)} %broadcast_in_dim.14), calls=%async_computation.1 | async-start | bytes 1048576 | tf_op jit(solution)/shard_map/all_to_all | solution.py:22
  43.2 12.0 %copy-start.7 = (f32[8,64,16]{1,2,0:T(8,128)S(1)}, f32[8,64,16]{1,2,0:T(8,128)}, u32[]{:S(2)}) copy-start(f32[8,64,16]{1,2,0:T(8,128)} %param.31) | copy-start | bytes 98308
  43.2 12.0 %copy-start.8 = (f32[8,64,16]{1,2,0:T(8,128)S(1)}, f32[8,64,16]{1,2,0:T(8,128)}, u32[]{:S(2)}) copy-start(f32[8,64,16]{1,2,0:T(8,128)} %param.32) | copy-start | bytes 98308
  43.2 12.0 %copy-start.9 = (f32[8,16,64]{2,1,0:T(8,128)S(1)}, f32[8,16,64]{2,1,0:T(8,128)}, u32[]{:S(2)}) copy-start(f32[8,16,64]{2,1,0:T(8,128)} %param.33) | copy-start | bytes 98308
  43.2 12.0 %copy-start.10 = (f32[8,16,64]{2,1,0:T(8,128)S(1)}, f32[8,16,64]{2,1,0:T(8,128)}, u32[]{:S(2)}) copy-start(f32[8,16,64]{2,1,0:T(8,128)} %param.34) | copy-start | bytes 98308
  43.2 12.0 %copy-start.14 = (f32[1,2,8,64]{3,2,1,0:T(8,128)S(1)}, f32[1,2,8,64]{3,2,1,0:T(8,128)}, u32[]{:S(2)}) copy-start(f32[1,2,8,64]{3,2,1,0:T(8,128)} %param.37) | copy-start | bytes 12292
  43.3 12.0 %copy-start.16 = (f32[8,64]{1,0:T(8,128)S(1)}, f32[8,64]{1,0:T(8,128)}, u32[]{:S(2)}) copy-start(f32[8,64]{1,0:T(8,128)} %freq_ref.1) | copy-start | bytes 6148
  43.3 12.0 %copy-start.17 = (f32[8,16]{1,0:T(8,128)S(1)}, f32[8,16]{1,0:T(8,128)}, u32[]{:S(2)}) copy-start(f32[8,16]{1,0:T(8,128)} %skip_ref.1) | copy-start | bytes 1540
  43.3 12.0 %copy-start.19 = (f32[8]{0:T(128)S(1)}, f32[8]{0:T(128)}, u32[]{:S(2)}) copy-start(f32[8]{0:T(128)} %log_ref.1) | copy-start | bytes 100
  43.3 12.0 %copy-start.13 = (f32[2048]{0:T(1024)S(1)}, f32[2048]{0:T(1024)}, u32[]{:S(2)}) copy-start(f32[2048]{0:T(1024)} %param.20) | copy-start | bytes 24580
  43.3 17.2 %collective-permute-start.3 = (bf16[4,32,640]{2,1,0:T(8,128)(2,1)S(1)}, bf16[4,32,640]{2,1,0:T(8,128)(2,1)S(1)}, u32[]{:S(2)}, u32[]{:S(2)}) collective-permute-start(bf16[4,32,640]{2,1,0:T(8,128)(2,1)S(1)} %get-tuple-element.21), channel_id=1, source_target_pairs={{0,48},{8,56},{16,32},{24,40},{32,80},{40,88},{48,64},{56,72},{64,... | collective-permute-start | bytes 491528 | tf_op jit(solution)/shard_map/ppermute | solution.py:367
  49.2 13.5 %collective-permute-start.2 = (bf16[4,32,640]{2,1,0:T(8,128)(2,1)S(1)}, bf16[4,32,640]{2,1,0:T(8,128)(2,1)S(1)}, u32[]{:S(2)}, u32[]{:S(2)}) collective-permute-start(bf16[4,32,640]{2,1,0:T(8,128)(2,1)S(1)} %get-tuple-element.21), channel_id=1, source_target_pairs={{0,448},{8,456},{16,464},{24,472},{32,480},{40,488},{48,496},{56,5... | collective-permute-start | bytes 491528 | tf_op jit(solution)/shard_map/ppermute | solution.py:367
  53.0 13.2 %collective-permute-start.1 = (bf16[4,32,640]{2,1,0:T(8,128)(2,1)S(1)}, bf16[4,32,640]{2,1,0:T(8,128)(2,1)S(1)}, u32[]{:S(2)}, u32[]{:S(2)}) collective-permute-start(bf16[4,32,640]{2,1,0:T(8,128)(2,1)S(1)} %get-tuple-element.21), channel_id=1, source_target_pairs={{0,496},{8,504},{16,480},{24,488},{32,16},{40,24},{48,0},{56,8},{6... | collective-permute-start | bytes 491528 | tf_op jit(solution)/shard_map/ppermute | solution.py:367
  60.6 13.9 %copy-start = (f32[2,256,512]{2,1,0:T(8,128)}, f32[2,256,512]{2,1,0:T(8,128)S(1)}, u32[]{:S(2)}) copy-start(f32[2,256,512]{2,1,0:T(8,128)S(1)} %get-tuple-element.12.bar_ref) | copy-start | bytes 3145732
  66.3 27.9 %collective-permute-start.4 = (bf16[4,4,32,640]{3,2,1,0:T(8,128)(2,1)S(1)}, bf16[4,4,32,640]{3,2,1,0:T(8,128)(2,1)S(1)}, u32[]{:S(2)}, u32[]{:S(2)}) collective-permute-start(bf16[4,4,32,640]{3,2,1,0:T(8,128)(2,1)S(1)} %pad_maximum_fusion.own_ref), channel_id=1, source_target_pairs={{0,24},{8,0},{16,8},{24,16},{32,56},{40,32},{48,40},{56,48},{64,88... | collective-permute-start | bytes 1966088 | tf_op jit(solution)/shard_map/ppermute | solution.py:367
  69.0 25.2 %collective-permute-start.5 = (bf16[4,4,32,640]{3,2,1,0:T(8,128)(2,1)S(1)}, bf16[4,4,32,640]{3,2,1,0:T(8,128)(2,1)}, u32[]{:S(2)}, u32[]{:S(2)}) collective-permute-start(bf16[4,4,32,640]{3,2,1,0:T(8,128)(2,1)S(1)} %pad_maximum_fusion.own_ref), channel_id=1, source_target_pairs={{0,8},{8,16},{16,24},{24,0},{32,40},{40,48},{48,56},{56,32},{64,72... | collective-permute-start | bytes 1966088 | tf_op jit(solution)/shard_map/ppermute | solution.py:367
  72.4 21.8 %collective-permute-start.6 = (bf16[2,4,32,640]{3,2,1,0:T(8,128)(2,1)}, bf16[2,4,32,640]{3,2,1,0:T(8,128)(2,1)S(1)}, u32[]{:S(2)}, u32[]{:S(2)}) collective-permute-start(bf16[2,4,32,640]{3,2,1,0:T(8,128)(2,1)} %pad_maximum_fusion.1), channel_id=1, source_target_pairs={{0,480},{8,488},{16,496},{24,504},{32,0},{40,8},{48,16},{56,24},{6... | collective-permute-start | bytes 983048 | tf_op jit(solution)/shard_map/ppermute | solution.py:367
  74.5 19.8 %collective-permute-start.7 = (bf16[2,4,32,640]{3,2,1,0:T(8,128)(2,1)}, bf16[2,4,32,640]{3,2,1,0:T(8,128)(2,1)}, u32[]{:S(2)}, u32[]{:S(2)}) collective-permute-start(bf16[2,4,32,640]{3,2,1,0:T(8,128)(2,1)} %pad_maximum_fusion.1), channel_id=1, source_target_pairs={{0,32},{8,40},{16,48},{24,56},{32,64},{40,72},{48,80},{56,88},{64,... | collective-permute-start | bytes 983048 | tf_op jit(solution)/shard_map/ppermute | solution.py:367
  79.7 1.2 copy-start.1
  83.9 16.5 %all-to-all-start.2 = ((f32[16,2,640]{2,1,0:T(2,128)}), f32[16,2,640]{2,1,0:T(2,128)S(1)}, u32[]{:S(2)}, u32[]{:S(2)}) async-start(f32[16,2,640]{2,1,0:T(2,128)} %broadcast_in_dim.30), calls=%async_computation.2 | async-start | bytes 163840 | tf_op jit(solution)/shard_map/all_to_all | solution.py:22
  89.4 11.0 %copy-start.12 = (bf16[256,128]{1,0:T(8,128)(2,1)S(1)}, bf16[256,128]{1,0:T(8,128)(2,1)}, u32[]{:S(2)}) copy-start(bf16[256,128]{1,0:T(8,128)(2,1)} %copy-done.11) | copy-start | bytes 196612
  89.4 4.8 %collective-permute-start = (bf16[16,2048]{1,0:T(8,128)(2,1)S(1)}, bf16[16,2048]{1,0:T(8,128)(2,1)S(1)}, u32[]{:S(2)}, u32[]{:S(2)}) collective-permute-start(bf16[16,2048]{1,0:T(8,128)(2,1)S(1)} %slice_bitcast_fusion), channel_id=1, source_target_pairs={{0,32},{32,64},{64,96},{96,128},{128,160},{160,192},{192,224},{224... | collective-permute-start | bytes 196616 | tf_op jit(solution)/shard_map/ppermute | solution.py:431
  96.5 1.0 copy-start.3
  100.4 1.2 copy-start.2
  101.6 2.9 %copy-start.4 = (bf16[2048,256]{1,0:T(8,128)(2,1)S(1)}, bf16[2048,256]{1,0:T(8,128)(2,1)}, u32[]{:S(2)}) copy-start(bf16[2048,256]{1,0:T(8,128)(2,1)} %copy-done.3) | copy-start | bytes 3145732
  106.0 23.8 %all-to-all-start.3 = ((bf16[8,32,2048]{2,1,0:T(8,128)(2,1)}), bf16[8,32,2048]{2,1,0:T(8,128)(2,1)S(1)}, u32[]{:S(2)}, u32[]{:S(2)}) async-start(bf16[8,32,2048]{2,1,0:T(8,128)(2,1)} %bitcast.15), calls=%async_computation.3 | async-start | bytes 2097152 | tf_op jit(solution)/shard_map/all_to_all | solution.py:493
  (4 other events, 2.7 us)

commit v4 on v3

--- a/solution.py
+++ b/solution.py
@@ -16,10 +16,10 @@
 NT = (((1,), (1,)), ((), ()))
 
 
-def spread(x, axis, groups=None):
-    copies = lax.axis_size(axis) if groups is None else len(groups[0])
+def spread(x, axis):
+    copies = lax.axis_size(axis)
     many = jnp.broadcast_to(x[None], (copies, *x.shape))
-    return lax.all_to_all(many, axis, 0, 0, tiled=True, axis_index_groups=groups)
+    return lax.all_to_all(many, axis, 0, 0, tiled=True)
 
 
 def complex_product(left_real, left_imag, right_real, right_imag):
@@ -116,6 +116,26 @@
     x = x.astype(F32)
     mean_square = jnp.mean(x * x, axis=-1, keepdims=True)
     return (x * lax.rsqrt(mean_square + 1e-06) * gain).astype(BF16)
+
+
+def pack_kernel(*refs):
+    count = 6
+    sources, out_ref, landed, sems = (refs[:count], refs[count], refs[count + 1], refs[count + 2])
+    copies = [
+        pltpu.make_async_copy(source, landed.at[i], sems.at[i]) for i, source in enumerate(sources)
+    ]
+    for copy in copies:
+        copy.start()
+    for copy in copies:
+        copy.wait()
+    tall = landed.shape[1]
+    part = tall // 4
+    for z in range(out_ref.shape[0]):
+        out_ref[z, :tall] = landed[0]
+        q = z % 4
+        for i in range(1, count):
+            at = tall + (i - 1) * part
+            out_ref[z, at : at + part] = landed[i, q * part : (q + 1) * part]
 
 
 def prep_kernel(
@@ -236,10 +256,8 @@
     groups, normed_ref, w_ref, bar_ref, pack_ref, rate_ref, chan_ref, end_ref, push_ref
 ):
     rows = normed_ref.shape[0]
-    near, fs, far = w_ref.shape[:3]
-    w = jnp.concatenate(
-        [w_ref[zb, y, za] for za in range(far) for zb in range(near) for y in range(fs)], axis=0
-    )
+    fs, sp = w_ref.shape[:2]
+    w = jnp.concatenate([w_ref[f, z] for z in range(sp) for f in range(fs)], axis=0)
     state_in = jnp.dot(normed_ref[...], w, preferred_element_type=F32).astype(BF16)
     chan = jnp.dot(chunk_order(rows, False), state_in, preferred_element_type=F32).astype(BF16)
     chan_ref[...] = chan
@@ -315,17 +333,21 @@
 ):
     width = mix_ref.shape[1]
     rows = normed_ref.shape[0]
-    near, far, tall, _ = own_ref.shape
-    split = w_ref.shape[1]
+    near, far = own_ref.shape[:2]
+    part = w_ref.shape[1]
     z, y = (lax.axis_index("sp"), lax.axis_index("fs"))
 
     def put(j, turn, ref, at_j):
+        at_q = (z + j) & 3
+        at_y = (y + 2 * j + turn) & 3
         for k in range(far):
-            at_z = 4 * k + ((z + j) & 3)
-            at_y = (y + 2 * j + turn) & 3
-            at = pl.ds(pl.multiple_of((at_z * 4 + at_y) * tall, tall), tall)
-            w_ref[at, :] = ref[at_j, k, :, :split]
-            weights_ref[at, :] = ref[at_j, k, :, split:]
+            at = (k * 4 + at_y) * 4 + at_q
+            for i in range(5):
+                piece = ref[at_j, k, i * part : (i + 1) * part]
+                if i < 3:
+                    w_ref[at, :, i * width : (i + 1) * width] = piece
+                else:
+                    weights_ref[at, :, (i - 3) * width : (i - 2) * width] = piece
 
     for j in range(near):
         put(j, 0, own_ref, j)
@@ -334,7 +356,7 @@
     for j in range(near // 2):
         put(j + 1, 2, left_ref, j)
         put(j - 1, 2, right_ref, j)
-    w = w_ref[...]
+    w = w_ref[...].reshape(normed_ref.shape[1], 3 * width)
     taps = [packed(pack_ref, 10 + at, width) for at in range(3)]
     gain = jnp.concatenate([packed(pack_ref, 5 + at) for at in range(4)], axis=1)
     reach = len(taps) - 1
@@ -354,8 +376,10 @@
 def out_kernel(state_ref, conv_ref, w_ref, out_ref):
     mixes = jnp.concatenate([state_ref[...], conv_ref[...]], axis=1)
     per = 512
-    for at in range(0, w_ref.shape[0], per):
-        product = lax.dot_general(mixes, w_ref[at : at + per], NT, preferred_element_type=F32)
+    tall, part, wide = w_ref.shape
+    for at in range(0, tall * part, per):
+        w = w_ref[at // part : (at + per) // part].reshape(per, wide)
+        product = lax.dot_general(mixes, w, NT, preferred_element_type=F32)
         out_ref[:, at : at + per] = product.astype(BF16)
 
 
@@ -374,16 +398,17 @@
     return (own, moved(own, 0, 1), moved(own, 0, -1), moved(half, 1, 0), moved(half, -1, 0))
 
 
-def call(kernel, out_shape, flops, *args, smem=0, scratch=()):
+def call(kernel, out_shape, flops, *args, smem=0, anywhere=0, scratch=(), limit=20 << 20):
     vmem = pl.BlockSpec(memory_space=pltpu.VMEM)
+    first = [pl.BlockSpec(memory_space=pltpu.SMEM)] * smem + [pl.BlockSpec(memory_space=pl.ANY)] * anywhere
     return pl.pallas_call(
         kernel,
         out_shape=out_shape,
-        in_specs=[pl.BlockSpec(memory_space=pltpu.SMEM)] * smem + [vmem] * (len(args) - smem),
+        in_specs=first + [vmem] * (len(args) - len(first)),
         out_specs=jax.tree.map(lambda _: vmem, out_shape),
         scratch_shapes=list(scratch),
         cost_estimate=pl.CostEstimate(flops=flops, bytes_accessed=1 << 20, transcendentals=0),
-        compiler_params=pltpu.CompilerParams(vmem_limit_bytes=20 << 20),
+        compiler_params=pltpu.CompilerParams(vmem_limit_bytes=limit),
     )(*args)
 
 
@@ -419,15 +444,23 @@
     width = groups * group
     count = lax.axis_size("sp")
 
-    fs = lax.axis_size("fs")
-    shards = jnp.concatenate([w_state_in, w_value, w_inner, w_outer, w_state_out, w_conv_out], axis=1)
-    apart = [[zb + 4 * za for za in range(count // 4)] for zb in range(4)]
-    far = spread(shards, "sp", apart)
-    block = 4 * fs
-    blocks = [[at + i for i in range(block)] for at in range(0, count * fs, block)]
-    state_weights = spread(far[:, :, :width], ("sp", "fs"), blocks)
-    state_weights = state_weights.reshape(4, fs, *state_weights.shape[1:])
-    own, up, down, left, right = all_shards(far[:, :, width:])
+    part = w_state_in.shape[0] // 4
+    weights = (w_state_in, w_value, w_inner, w_outer, w_state_out, w_conv_out)
+    shards = call(
+        pack_kernel,
+        shape((count, w_state_in.shape[0] + 5 * part, width), BF16),
+        1 << 20,
+        *weights,
+        anywhere=len(weights),
+        scratch=(
+            pltpu.VMEM((len(weights), *w_state_in.shape), BF16),
+            pltpu.SemaphoreType.DMA((len(weights),)),
+        ),
+        limit=None,
+    )
+    far = lax.all_to_all(shards, "sp", 0, 0, tiled=True)
+    state_weights = spread(far[:, : 4 * part], "fs")
+    own, up, down, left, right = all_shards(far[:, 4 * part :])
     edge = lax.ppermute(tokens[0, rows - HALO :], "sp", [(i, i + 1) for i in range(count - 1)])
     gain = norm_gain[None]
     into = [jnp.swapaxes(x, 1, 2).reshape(width, states) for x in (input_real, input_imag)]
@@ -464,7 +497,7 @@
     ends = spread(end, "sp")
     conv_mix, out_weights = call(
         conv_kernel,
-        (shape((rows, width), BF16), shape((features, 2 * width), BF16)),
+        (shape((rows, width), BF16), shape((features // part, part, 2 * width), BF16)),
         1 << 29,
         normed,
         edge,
@@ -474,7 +507,7 @@
         left,
         right,
         pack,
-        scratch=(pltpu.VMEM((features, 3 * width), BF16),),
+        scratch=(pltpu.VMEM((features // part, part, 3 * width), BF16),),
     )
     state_mix, closing = call(
         functools.partial(read_kernel, groups),

time: 132 us -> 130 us (0.985)
  local copies, waits for them, and re-layouts: 11.3 us -> 8.1 us
  waiting for transfers between devices: 24.3 us -> 22 us
  Pallas kernels: 12.9 us -> 14.5 us
  blocking collectives: 28.5 us -> 29.9 us
    ppermute x7, waiting for transfers between devices: 5.66 us -> 0.02 us  [moved(): return lax.ppermute(x, ('sp', 'fs'), pairs)]
    all_to_all x2, waiting for transfers between devices: 2.94 us -> 7.72 us  [spread(): return lax.all_to_all(many, axis, 0, 0, tiled=True)]
    ppermute x7, starting transfers between devices: 24.4 us -> 28.9 us  [moved(): return lax.ppermute(x, ('sp', 'fs'), pairs)]
    all_to_all x2, starting transfers between devices: 14.3 us -> 10.5 us  [spread(): return lax.all_to_all(many, axis, 0, 0, tiled=True)]
    unnamed x55 -> x36, local copies, waits for them, and re-layouts: 8.18 us -> 4.96 us
    pallas_call x5 -> x6, Pallas kernels: 12.9 us -> 14.5 us  [call(): pl.pallas_call(kernel, out_shape=out_shape, in_specs=first + [vmem] * (le...]
    ppermute x1, waiting for transfers between devices: 1.41 us -> 0.01 us  [body(): lax.ppermute(tokens[0, rows - HALO:], 'sp', [(i, i + 1) for i in range(co...]
    all_to_all x1, blocking collectives: 28.5 us -> 29.9 us  [body(): far = lax.all_to_all(shards, 'sp', 0, 0, tiled=True)]
  transfers between devices with their start and end apart: 11 -> 11, of which waited for: 5 -> 2; matrix products, arithmetic and copies ran while one was open for 2% -> 3% of each run, Pallas kernels for 7% -> 7%
where the time goes in v4:
time: 130 us; the launch traced here: 129 us
  starting transfers between devices  52 us (40%)
  blocking collectives  29.9 us (23%)
  waiting for transfers between devices  22 us (17%)
  Pallas kernels  14.5 us (11%)
  local copies, waits for them, and re-layouts  8.1 us (6%)
  other arithmetic  1.67 us (1%)
    all_to_all x1, blocking collectives, body(): far = lax.all_to_all(shards, 'sp', 0, 0, tiled=True)  29.9 us
    ppermute x7, starting transfers between devices, moved(): return lax.ppermute(x, ('sp', 'fs'), pairs)  28.9 us
    pallas_call x6, Pallas kernels, call(): pl.pallas_call(kernel, out_shape=out_shape, in_specs=first + [vmem] * (le...  14.5 us
    all_to_all x1, waiting for transfers between devices, body(): lax.all_to_all(partial.reshape(tp, rows // tp, features), 'tp', 0, 0, til...  14.3 us
    all_to_all x2, starting transfers between devices, spread(): return lax.all_to_all(many, axis, 0, 0, tiled=True)  10.5 us
    all_to_all x1, starting transfers between devices, body(): lax.all_to_all(partial.reshape(tp, rows // tp, features), 'tp', 0, 0, til...  9.35 us
    all_to_all x2, waiting for transfers between devices, spread(): return lax.all_to_all(many, axis, 0, 0, tiled=True)  7.72 us
    unnamed x36, local copies, waits for them, and re-layouts  4.96 us
  transfers between devices with their start and end apart: 11, of which 2 were waited for; matrix products, arithmetic and copies ran while one was open for 3% of the time, Pallas kernels for 7%

profile of v4, /device:TPU:1, one launch (start us, length us, event | category | flops | bytes accessed | tf_op | source)
XLA Modules:
  0.0 129.2 jit_solution(18054047962595148146)
XLA Ops:
  0.6 1.6 %shard_map.195 = bf16[16,72,128]{2,1,0:T(8,128)(2,1)} custom-call(bf16[32,128]{1,0:T(8,128)(2,1)} %refs_0_.1, bf16[32,128]{1,0:T(8,128)(2,1)} %refs_1_.1, bf16[32,128]{1,0:T(8,128)(2,1)} %refs_2_.1, bf16[32,128]{1,0:T(8,128)(2,1)} %refs_3_.1, bf16[32,128]{1,0:T(8,128)(2,1)} %refs_4_.1, bf16[32,128]{1,0:T(8,128)(2,1)} %refs_5_.1), custom_call_target="tpu_custom_call" | custom-call | flops 1048576 | bytes 1048576 | tf_op jit(solution)/shard_map/pallas_call | solution.py:404
  2.2 29.9 %all_to_all.20 = bf16[16,72,128]{2,1,0:T(8,128)(2,1)S(1)} all-to-all(bf16[16,72,128]{2,1,0:T(8,128)(2,1)} %shard_map.195), channel_id=1, replica_groups=mesh['sp'=16,'fs'=4,'tp'=8] {'sp'}, dimensions={0} | all-to-all | bytes 589824 | tf_op jit(solution)/shard_map/all_to_all | solution.py:461
  32.2 10.4 %collective-permute-start.3 = (bf16[16,40,128]{2,1,0:T(8,128)(2,1)S(1)}, bf16[16,40,128]{2,1,0:T(8,128)(2,1)S(1)}, u32[]{:S(2)}, u32[]{:S(2)}) collective-permute-start(bf16[16,40,128]{2,1,0:T(8,128)(2,1)S(1)} %get-tuple-element.21), channel_id=1, source_target_pairs={{0,48},{8,56},{16,32},{24,40},{32,80},{40,88},{48,64},{56,72},{64,... | collective-permute-start | bytes 491528 | tf_op jit(solution)/shard_map/ppermute | solution.py:391
  42.6 3.7 %collective-permute-start.2 = (bf16[16,40,128]{2,1,0:T(8,128)(2,1)S(1)}, bf16[16,40,128]{2,1,0:T(8,128)(2,1)S(1)}, u32[]{:S(2)}, u32[]{:S(2)}) collective-permute-start(bf16[16,40,128]{2,1,0:T(8,128)(2,1)S(1)} %get-tuple-element.21), channel_id=1, source_target_pairs={{0,448},{8,456},{16,464},{24,472},{32,480},{40,488},{48,496},{56,5... | collective-permute-start | bytes 491528 | tf_op jit(solution)/shard_map/ppermute | solution.py:391
  46.3 2.4 %collective-permute-start.1 = (bf16[16,40,128]{2,1,0:T(8,128)(2,1)S(1)}, bf16[16,40,128]{2,1,0:T(8,128)(2,1)S(1)}, u32[]{:S(2)}, u32[]{:S(2)}) collective-permute-start(bf16[16,40,128]{2,1,0:T(8,128)(2,1)S(1)} %get-tuple-element.21), channel_id=1, source_target_pairs={{0,496},{8,504},{16,480},{24,488},{32,16},{40,24},{48,0},{56,8},{6... | collective-permute-start | bytes 491528 | tf_op jit(solution)/shard_map/ppermute | solution.py:391
  48.8 0.9 broadcast_in_dim.22
  49.8 3.6 %all-to-all-start.1 = ((bf16[4,16,32,128]{3,2,1,0:T(8,128)(2,1)}), bf16[4,16,32,128]{3,2,1,0:T(8,128)(2,1)S(1)}, u32[]{:S(2)}, u32[]{:S(2)}) async-start(bf16[4,16,32,128]{3,2,1,0:T(8,128)(2,1)} %broadcast_in_dim.22), calls=%async_computation.1 | async-start | bytes 1048576 | tf_op jit(solution)/shard_map/all_to_all | solution.py:22
  53.5 0.6 copy-done.11
  54.1 1.2 copy-done.3
  55.3 4.6 %shard_map.194 = (bf16[256,2048]{1,0:T(8,128)(2,1)S(1)}, f32[2,256,512]{2,1,0:T(8,128)S(1)}, f32[144,512]{1,0:T(8,128)S(1)}) custom-call(f32[8]{0:T(128)S(1)} %copy-done.17, bf16[256,2048]{1,0:T(8,128)(2,1)S(1)} %bitcast.21, f32[1,2048]{1,0:T(1,128)S(1)} %bitcast.26, f32[1,256]{1,0:T(1,128)S(1)} %copy-done.4, f32[8,64]{1,0:T(8,128)S(1)} %copy-done.13, ...), custom_call_target="tpu_custom_call" | custom-call | flops 1073741824 | bytes 1048576 | tf_op jit(solution)/shard_map/pallas_call | solution.py:404
  60.0 0.1 pad_maximum_fusion.own_ref
  60.1 4.5 %collective-permute-start.4 = (bf16[4,16,40,128]{3,2,1,0:T(8,128)(2,1)S(1)}, bf16[4,16,40,128]{3,2,1,0:T(8,128)(2,1)S(1)}, u32[]{:S(2)}, u32[]{:S(2)}) collective-permute-start(bf16[4,16,40,128]{3,2,1,0:T(8,128)(2,1)S(1)} %pad_maximum_fusion.own_ref), channel_id=1, source_target_pairs={{0,24},{8,0},{16,8},{24,16},{32,56},{40,32},{48,40},{56,48},{64,88... | collective-permute-start | bytes 1966088 | tf_op jit(solution)/shard_map/ppermute | solution.py:391
  64.7 1.9 %collective-permute-start.5 = (bf16[4,16,40,128]{3,2,1,0:T(8,128)(2,1)S(1)}, bf16[4,16,40,128]{3,2,1,0:T(8,128)(2,1)}, u32[]{:S(2)}, u32[]{:S(2)}) collective-permute-start(bf16[4,16,40,128]{3,2,1,0:T(8,128)(2,1)S(1)} %pad_maximum_fusion.own_ref), channel_id=1, source_target_pairs={{0,8},{8,16},{16,24},{24,0},{32,40},{40,48},{48,56},{56,32},{64,72... | collective-permute-start | bytes 1966088 | tf_op jit(solution)/shard_map/ppermute | solution.py:391
  66.6 0.8 pad_maximum_fusion.1
  67.4 3.9 %collective-permute-start.6 = (bf16[2,16,40,128]{3,2,1,0:T(8,128)(2,1)}, bf16[2,16,40,128]{3,2,1,0:T(8,128)(2,1)S(1)}, u32[]{:S(2)}, u32[]{:S(2)}) collective-permute-start(bf16[2,16,40,128]{3,2,1,0:T(8,128)(2,1)} %pad_maximum_fusion.1), channel_id=1, source_target_pairs={{0,480},{8,488},{16,496},{24,504},{32,0},{40,8},{48,16},{56,24},{6... | collective-permute-start | bytes 983048 | tf_op jit(solution)/shard_map/ppermute | solution.py:391
  71.3 1.9 %collective-permute-start.7 = (bf16[2,16,40,128]{3,2,1,0:T(8,128)(2,1)}, bf16[2,16,40,128]{3,2,1,0:T(8,128)(2,1)}, u32[]{:S(2)}, u32[]{:S(2)}) collective-permute-start(bf16[2,16,40,128]{3,2,1,0:T(8,128)(2,1)} %pad_maximum_fusion.1), channel_id=1, source_target_pairs={{0,32},{8,40},{16,48},{24,56},{32,64},{40,72},{48,80},{56,88},{64,... | collective-permute-start | bytes 983048 | tf_op jit(solution)/shard_map/ppermute | solution.py:391
  73.2 1.2 copy-done.1
  74.4 1.7 %shard_map.196 = (bf16[256,128]{1,0:T(8,128)(2,1)S(1)}, f32[2,640]{1,0:T(2,128)S(1)}) custom-call(bf16[256,2048]{1,0:T(8,128)(2,1)S(1)} %get-tuple-element.11.normed_ref, bf16[4,16,32,128]{3,2,1,0:T(8,128)(2,1)S(1)} %all-to-all-done.1.w_ref, f32[2,256,512]{2,1,0:T(8,128)S(1)} %copy-done.1, f32[144,512]{1,0:T(8,128)S(1)} %get-tuple-element.13.pack_ref, ...), custom_call_target="tpu_custom_call" | custom-call | flops 536870912 | bytes 1048576 | tf_op jit(solution)/shard_map/pallas_call | solution.py:404
  76.1 0.6 copy-done.9
  76.7 0.7 broadcast_in_dim.23
  77.4 6.9 %all-to-all-start.2 = ((f32[16,2,640]{2,1,0:T(2,128)}), f32[16,2,640]{2,1,0:T(2,128)S(1)}, u32[]{:S(2)}, u32[]{:S(2)}) async-start(f32[16,2,640]{2,1,0:T(2,128)} %broadcast_in_dim.23), calls=%async_computation.2 | async-start | bytes 163840 | tf_op jit(solution)/shard_map/all_to_all | solution.py:22
  84.3 0.9 slice_bitcast_fusion
  85.2 3.3 %collective-permute-start = (bf16[16,2048]{1,0:T(8,128)(2,1)S(1)}, bf16[16,2048]{1,0:T(8,128)(2,1)S(1)}, u32[]{:S(2)}, u32[]{:S(2)}) collective-permute-start(bf16[16,2048]{1,0:T(8,128)(2,1)S(1)} %slice_bitcast_fusion), channel_id=1, source_target_pairs={{0,32},{32,64},{64,96},{96,128},{128,160},{160,192},{192,224},{224... | collective-permute-start | bytes 196616 | tf_op jit(solution)/shard_map/ppermute | solution.py:464
  88.4 7.7 %all-to-all-done.2.ends_ref = f32[16,2,640]{2,1,0:T(2,128)S(1)} async-done(((f32[16,2,640]{2,1,0:T(2,128)}), f32[16,2,640]{2,1,0:T(2,128)S(1)}, u32[]{:S(2)}, u32[]{:S(2)}) %all-to-all-start.2) | async-done | bytes 81952 | tf_op jit(solution)/shard_map/all_to_all | solution.py:22
  96.2 1.2 copy-done.2
  97.4 2.9 %shard_map.197 = (bf16[256,128]{1,0:T(8,128)(2,1)S(1)}, f32[2,8,4]{2,1,0:T(8,128)S(1)}) custom-call(f32[16,2,640]{2,1,0:T(2,128)S(1)} %all-to-all-done.2.ends_ref, f32[2,256,512]{2,1,0:T(8,128)S(1)} %copy-done.2, bf16[256,128]{1,0:T(8,128)(2,1)S(1)} %copy-done.10, f32[144,512]{1,0:T(8,128)S(1)} %get-tuple-element.13.pack_ref), custom_call_target="tpu_custom_call" | custom-call | flops 536870912 | bytes 1048576 | tf_op jit(solution)/shard_map/pallas_call | solution.py:404
  100.3 2.3 %shard_map.198 = (bf16[256,128]{1,0:T(8,128)(2,1)S(1)}, bf16[256,8,256]{2,1,0:T(8,128)(2,1)S(1)}) custom-call(bf16[256,2048]{1,0:T(8,128)(2,1)S(1)} %get-tuple-element.11.normed_ref, bf16[16,2048]{1,0:T(8,128)(2,1)S(1)} %collective-permute-done.halo_ref, bf16[4,16,40,128]{3,2,1,0:T(8,128)(2,1)S(1)} %pad_maximum_fusion.own_ref, ...), custom_call_target="tpu_custom_call" | custom-call | flops 536870912 | bytes 1048576 | tf_op jit(solution)/shard_map/pallas_call | solution.py:404
  102.6 1.5 %shard_map.199 = bf16[256,2048]{1,0:T(8,128)(2,1)} custom-call(bf16[256,128]{1,0:T(8,128)(2,1)S(1)} %get-tuple-element.16.state_ref, bf16[256,128]{1,0:T(8,128)(2,1)S(1)} %get-tuple-element.17.conv_ref, bf16[256,8,256]{2,1,0:T(8,128)(2,1)S(1)} %get-tuple-element.18.w_ref), custom_call_target="tpu_custom_call" | custom-call | flops 536870912 | bytes 1048576 | tf_op jit(solution)/shard_map/pallas_call | solution.py:404
  104.1 9.3 %all-to-all-start.3 = ((bf16[8,32,2048]{2,1,0:T(8,128)(2,1)}), bf16[8,32,2048]{2,1,0:T(8,128)(2,1)S(1)}, u32[]{:S(2)}, u32[]{:S(2)}) async-start(bf16[8,32,2048]{2,1,0:T(8,128)(2,1)} %bitcast.14), calls=%async_computation.3 | async-start | bytes 2097152 | tf_op jit(solution)/shard_map/all_to_all | solution.py:526
  113.4 0.7 copy.21
  114.1 14.3 %all-to-all-done.3 = bf16[8,32,2048]{2,1,0:T(8,128)(2,1)S(1)} async-done(((bf16[8,32,2048]{2,1,0:T(8,128)(2,1)}), bf16[8,32,2048]{2,1,0:T(8,128)(2,1)S(1)}, u32[]{:S(2)}, u32[]{:S(2)}) %all-to-all-start.3) | async-done | bytes 1048608 | tf_op jit(solution)/shard_map/all_to_all | solution.py:526
  128.4 0.8 reduce_sum.12
  (42 shorter events, 0.2 us)
Async XLA Ops:
  32.2 27.8 %collective-permute-start.3 = (bf16[16,40,128]{2,1,0:T(8,128)(2,1)S(1)}, bf16[16,40,128]{2,1,0:T(8,128)(2,1)S(1)}, u32[]{:S(2)}, u32[]{:S(2)}) collective-permute-start(bf16[16,40,128]{2,1,0:T(8,128)(2,1)S(1)} %get-tuple-element.21), channel_id=1, source_target_pairs={{0,48},{8,56},{16,32},{24,40},{32,80},{40,88},{48,64},{56,72},{64,... | collective-permute-start | bytes 491528 | tf_op jit(solution)/shard_map/ppermute | solution.py:391
  42.6 17.4 %collective-permute-start.2 = (bf16[16,40,128]{2,1,0:T(8,128)(2,1)S(1)}, bf16[16,40,128]{2,1,0:T(8,128)(2,1)S(1)}, u32[]{:S(2)}, u32[]{:S(2)}) collective-permute-start(bf16[16,40,128]{2,1,0:T(8,128)(2,1)S(1)} %get-tuple-element.21), channel_id=1, source_target_pairs={{0,448},{8,456},{16,464},{24,472},{32,480},{40,488},{48,496},{56,5... | collective-permute-start | bytes 491528 | tf_op jit(solution)/shard_map/ppermute | solution.py:391
  46.3 13.7 %collective-permute-start.1 = (bf16[16,40,128]{2,1,0:T(8,128)(2,1)S(1)}, bf16[16,40,128]{2,1,0:T(8,128)(2,1)S(1)}, u32[]{:S(2)}, u32[]{:S(2)}) collective-permute-start(bf16[16,40,128]{2,1,0:T(8,128)(2,1)S(1)} %get-tuple-element.21), channel_id=1, source_target_pairs={{0,496},{8,504},{16,480},{24,488},{32,16},{40,24},{48,0},{56,8},{6... | collective-permute-start | bytes 491528 | tf_op jit(solution)/shard_map/ppermute | solution.py:391
  49.7 3.7 %copy-start.5 = (f32[8,64,16]{1,2,0:T(8,128)S(1)}, f32[8,64,16]{1,2,0:T(8,128)}, u32[]{:S(2)}) copy-start(f32[8,64,16]{1,2,0:T(8,128)} %param.31) | copy-start | bytes 98308
  49.7 3.7 %copy-start.6 = (f32[8,64,16]{1,2,0:T(8,128)S(1)}, f32[8,64,16]{1,2,0:T(8,128)}, u32[]{:S(2)}) copy-start(f32[8,64,16]{1,2,0:T(8,128)} %param.32) | copy-start | bytes 98308
  49.7 3.7 %copy-start.7 = (f32[8,16,64]{2,1,0:T(8,128)S(1)}, f32[8,16,64]{2,1,0:T(8,128)}, u32[]{:S(2)}) copy-start(f32[8,16,64]{2,1,0:T(8,128)} %param.33) | copy-start | bytes 98308
  49.7 3.8 %copy-start.8 = (f32[8,16,64]{2,1,0:T(8,128)S(1)}, f32[8,16,64]{2,1,0:T(8,128)}, u32[]{:S(2)}) copy-start(f32[8,16,64]{2,1,0:T(8,128)} %param.34) | copy-start | bytes 98308
  49.7 3.8 %copy-start.12 = (f32[1,2,8,64]{3,2,1,0:T(8,128)S(1)}, f32[1,2,8,64]{3,2,1,0:T(8,128)}, u32[]{:S(2)}) copy-start(f32[1,2,8,64]{3,2,1,0:T(8,128)} %param.37) | copy-start | bytes 12292
  49.7 3.8 %copy-start.14 = (f32[8,64]{1,0:T(8,128)S(1)}, f32[8,64]{1,0:T(8,128)}, u32[]{:S(2)}) copy-start(f32[8,64]{1,0:T(8,128)} %freq_ref.1) | copy-start | bytes 6148
  49.7 3.8 %copy-start.15 = (f32[8,16]{1,0:T(8,128)S(1)}, f32[8,16]{1,0:T(8,128)}, u32[]{:S(2)}) copy-start(f32[8,16]{1,0:T(8,128)} %skip_ref.1) | copy-start | bytes 1540
  49.8 3.8 %copy-start.16 = (f32[3,128]{1,0:T(4,128)S(1)}, f32[3,128]{1,0:T(4,128)}, u32[]{:S(2)}) copy-start(f32[3,128]{1,0:T(4,128)} %taps_ref.1) | copy-start | bytes 4612
  49.8 3.8 %copy-start.17 = (f32[8]{0:T(128)S(1)}, f32[8]{0:T(128)}, u32[]{:S(2)}) copy-start(f32[8]{0:T(128)} %log_ref.1) | copy-start | bytes 100
  49.8 23.4 %all-to-all-start.1 = ((bf16[4,16,32,128]{3,2,1,0:T(8,128)(2,1)}), bf16[4,16,32,128]{3,2,1,0:T(8,128)(2,1)S(1)}, u32[]{:S(2)}, u32[]{:S(2)}) async-start(bf16[4,16,32,128]{3,2,1,0:T(8,128)(2,1)} %broadcast_in_dim.22), calls=%async_computation.1 | async-start | bytes 1048576 | tf_op jit(solution)/shard_map/all_to_all | solution.py:22
  53.4 0.7 copy-start.11
  53.4 0.7 copy-start.13
  53.4 0.7 copy-start.4
  54.1 1.2 copy-start.3
  60.0 11.3 %copy-start = (f32[2,256,512]{2,1,0:T(8,128)}, f32[2,256,512]{2,1,0:T(8,128)S(1)}, u32[]{:S(2)}) copy-start(f32[2,256,512]{2,1,0:T(8,128)S(1)} %get-tuple-element.12.bar_ref) | copy-start | bytes 3145732
  60.1 40.2 %collective-permute-start.4 = (bf16[4,16,40,128]{3,2,1,0:T(8,128)(2,1)S(1)}, bf16[4,16,40,128]{3,2,1,0:T(8,128)(2,1)S(1)}, u32[]{:S(2)}, u32[]{:S(2)}) collective-permute-start(bf16[4,16,40,128]{3,2,1,0:T(8,128)(2,1)S(1)} %pad_maximum_fusion.own_ref), channel_id=1, source_target_pairs={{0,24},{8,0},{16,8},{24,16},{32,56},{40,32},{48,40},{56,48},{64,88... | collective-permute-start | bytes 1966088 | tf_op jit(solution)/shard_map/ppermute | solution.py:391
  64.7 35.6 %collective-permute-start.5 = (bf16[4,16,40,128]{3,2,1,0:T(8,128)(2,1)S(1)}, bf16[4,16,40,128]{3,2,1,0:T(8,128)(2,1)}, u32[]{:S(2)}, u32[]{:S(2)}) collective-permute-start(bf16[4,16,40,128]{3,2,1,0:T(8,128)(2,1)S(1)} %pad_maximum_fusion.own_ref), channel_id=1, source_target_pairs={{0,8},{8,16},{16,24},{24,0},{32,40},{40,48},{48,56},{56,32},{64,72... | collective-permute-start | bytes 1966088 | tf_op jit(solution)/shard_map/ppermute | solution.py:391
  67.4 32.9 %collective-permute-start.6 = (bf16[2,16,40,128]{3,2,1,0:T(8,128)(2,1)}, bf16[2,16,40,128]{3,2,1,0:T(8,128)(2,1)S(1)}, u32[]{:S(2)}, u32[]{:S(2)}) collective-permute-start(bf16[2,16,40,128]{3,2,1,0:T(8,128)(2,1)} %pad_maximum_fusion.1), channel_id=1, source_target_pairs={{0,480},{8,488},{16,496},{24,504},{32,0},{40,8},{48,16},{56,24},{6... | collective-permute-start | bytes 983048 | tf_op jit(solution)/shard_map/ppermute | solution.py:391
  71.3 29.0 %collective-permute-start.7 = (bf16[2,16,40,128]{3,2,1,0:T(8,128)(2,1)}, bf16[2,16,40,128]{3,2,1,0:T(8,128)(2,1)}, u32[]{:S(2)}, u32[]{:S(2)}) collective-permute-start(bf16[2,16,40,128]{3,2,1,0:T(8,128)(2,1)} %pad_maximum_fusion.1), channel_id=1, source_target_pairs={{0,32},{8,40},{16,48},{24,56},{32,64},{40,72},{48,80},{56,88},{64,... | collective-permute-start | bytes 983048 | tf_op jit(solution)/shard_map/ppermute | solution.py:391
  73.2 1.2 copy-start.1
  76.1 0.6 copy-start.9
  77.4 18.8 %all-to-all-start.2 = ((f32[16,2,640]{2,1,0:T(2,128)}), f32[16,2,640]{2,1,0:T(2,128)S(1)}, u32[]{:S(2)}, u32[]{:S(2)}) async-start(f32[16,2,640]{2,1,0:T(2,128)} %broadcast_in_dim.23), calls=%async_computation.2 | async-start | bytes 163840 | tf_op jit(solution)/shard_map/all_to_all | solution.py:22
  84.3 11.9 %copy-start.10 = (bf16[256,128]{1,0:T(8,128)(2,1)S(1)}, bf16[256,128]{1,0:T(8,128)(2,1)}, u32[]{:S(2)}) copy-start(bf16[256,128]{1,0:T(8,128)(2,1)} %copy-done.9) | copy-start | bytes 196612
  85.2 15.1 %collective-permute-start = (bf16[16,2048]{1,0:T(8,128)(2,1)S(1)}, bf16[16,2048]{1,0:T(8,128)(2,1)S(1)}, u32[]{:S(2)}, u32[]{:S(2)}) collective-permute-start(bf16[16,2048]{1,0:T(8,128)(2,1)S(1)} %slice_bitcast_fusion), channel_id=1, source_target_pairs={{0,32},{32,64},{64,96},{96,128},{128,160},{160,192},{192,224},{224... | collective-permute-start | bytes 196616 | tf_op jit(solution)/shard_map/ppermute | solution.py:464
  96.2 1.2 copy-start.2
  104.1 24.3 %all-to-all-start.3 = ((bf16[8,32,2048]{2,1,0:T(8,128)(2,1)}), bf16[8,32,2048]{2,1,0:T(8,128)(2,1)S(1)}, u32[]{:S(2)}, u32[]{:S(2)}) async-start(bf16[8,32,2048]{2,1,0:T(8,128)(2,1)} %bitcast.14), calls=%async_computation.3 | async-start | bytes 2097152 | tf_op jit(solution)/shard_map/all_to_all | solution.py:526

commit v5 on v4

--- a/solution.py
+++ b/solution.py
@@ -14,12 +14,6 @@
 HALO = 16
 PACKED = 16
 NT = (((1,), (1,)), ((), ()))
-
-
-def spread(x, axis):
-    copies = lax.axis_size(axis)
-    many = jnp.broadcast_to(x[None], (copies, *x.shape))
-    return lax.all_to_all(many, axis, 0, 0, tiled=True)
 
 
 def complex_product(left_real, left_imag, right_real, right_imag):
@@ -162,9 +156,11 @@
     (decay,) = flattened(decay_ref[...], groups)
     (freq,) = flattened(freq_ref[...], groups)
     scale = spread_steps(log_ref, groups, states)
+    top = in_real_ref.shape[0] // 2
     for at, ref in enumerate((in_real_ref, in_imag_ref, out_real_ref, out_imag_ref)):
-        pack_ref[: ref.shape[0], at * states : (at + 1) * states] = ref[...]
-    width = taps_ref.shape[1]
+        for i in range(2):
+            lanes = slice((2 * at + i) * states, (2 * at + i + 1) * states)
+            pack_ref[:top, lanes] = ref[i * top : (i + 1) * top]
     (skip,) = flattened(skip_ref[...], groups)
     gain_rows = gain_ref.shape[1] // flat
     for at, row in enumerate(
@@ -178,7 +174,7 @@
             *(taps_ref[i : i + 1] for i in range(taps_ref.shape[0])),
         )
     ):
-        pack_ref[width + at : width + at + 1, : row.shape[1]] = row
+        pack_ref[top + at : top + at + 1, : row.shape[1]] = row
     steps = rows // CHUNKS
 
     def advance(j, carry):
@@ -200,7 +196,9 @@
 
 
 def matrix(pack_ref, at, states):
-    return pack_ref[: pack_ref.shape[0] - PACKED, at * states : (at + 1) * states]
+    top = pack_ref.shape[0] - PACKED
+    halves = [pack_ref[:top, (2 * at + i) * states : (2 * at + i + 1) * states] for i in range(2)]
+    return jnp.concatenate(halves, axis=0)
 
 
 def driven(chan, pack_ref, bar_ref, groups, push_ref):
@@ -269,9 +267,19 @@
         moved_real, moved_imag = complex_product(end_real[c : c + 1], end_imag[c : c + 1], real, imag)
         real = moved_real + last_real[c : c + 1]
         imag = moved_imag + last_imag[c : c + 1]
-    end_ref[:, :flat] = jnp.concatenate([real, imag], axis=0)
+    end = jnp.concatenate([real, imag], axis=0)
     whole = jnp.sum(rate_ref[...], axis=1, keepdims=True)
-    end_ref[:, flat:] = jnp.broadcast_to(whole, (2, end_ref.shape[1] - flat))
+    whole = jnp.broadcast_to(whole, (2, end_ref.shape[2] - flat))
+    for z in range(end_ref.shape[0]):
+        end_ref[z, :, :flat] = end
+        end_ref[z, :, flat:] = whole
+
+
+def split_kernel(far_ref, many_ref, rest_ref):
+    tall = many_ref.shape[2]
+    rest_ref[...] = far_ref[:, tall:]
+    for copy in range(many_ref.shape[0]):
+        many_ref[copy] = far_ref[:, :tall]
 
 
 def gelu(v):
@@ -459,14 +467,21 @@
         limit=None,
     )
     far = lax.all_to_all(shards, "sp", 0, 0, tiled=True)
-    state_weights = spread(far[:, : 4 * part], "fs")
-    own, up, down, left, right = all_shards(far[:, 4 * part :])
+    fs = lax.axis_size("fs")
+    many, rest = call(
+        split_kernel,
+        (shape((fs, count, 4 * part, width), BF16), shape((count, 5 * part, width), BF16)),
+        1 << 20,
+        far,
+    )
+    state_weights = lax.all_to_all(many, "fs", 0, 0, tiled=True)
+    own, up, down, left, right = all_shards(rest)
     edge = lax.ppermute(tokens[0, rows - HALO :], "sp", [(i, i + 1) for i in range(count - 1)])
     gain = norm_gain[None]
     into = [jnp.swapaxes(x, 1, 2).reshape(width, states) for x in (input_real, input_imag)]
     normed, bar, pack = call(
         prep_kernel,
-        (shape((rows, features), BF16), shape((2, rows, flat)), shape((width + PACKED, flat))),
+        (shape((rows, features), BF16), shape((2, rows, flat)), shape((width // 2 + PACKED, flat))),
         1 << 30,
         log_step,
         tokens[0],
@@ -485,7 +500,7 @@
     )
     chan, end = call(
         functools.partial(local_kernel, groups),
-        (shape((rows, width), BF16), shape((2, flat + 128))),
+        (shape((rows, width), BF16), shape((count, 2, flat + 128))),
         1 << 29,
         normed,
         state_weights,
@@ -494,7 +509,7 @@
         step_rate,
         scratch=(pltpu.VMEM((2, rows, flat), F32),),
     )
-    ends = spread(end, "sp")
+    ends = lax.all_to_all(end, "sp", 0, 0, tiled=True)
     conv_mix, out_weights = call(
         conv_kernel,
         (shape((rows, width), BF16), shape((features // part, part, 2 * width), BF16)),

time: 130 us -> 131 us (level)
  local copies, waits for them, and re-layouts: 8.1 us -> 5.64 us
  Pallas kernels: 14.5 us -> 16.4 us
    pallas_call x6 -> x7, Pallas kernels: 14.5 us -> 16.4 us  [call(): pl.pallas_call(kernel, out_shape=out_shape, in_specs=first + [vmem] * (le...]
    broadcast_in_dim x2 -> x0, local copies, waits for them, and re-layouts: 1.54 us -> none  [spread(): many = jnp.broadcast_to(x[None], (copies, *x.shape))]
  transfers between devices with their start and end apart: 11 -> 11, of which waited for: 2 -> 2; matrix products, arithmetic and copies ran while one was open for 3% -> 3% of each run, Pallas kernels for 7% -> 8%
where the time goes in v5:
time: 131 us; the launch traced here: 130 us
  starting transfers between devices  52 us (40%)
  blocking collectives  29.9 us (23%)
  waiting for transfers between devices  22.1 us (17%)
  Pallas kernels  16.4 us (13%)
  local copies, waits for them, and re-layouts  5.64 us (4%)
  other arithmetic  2.78 us (2%)
    all_to_all x1, blocking collectives, body(): far = lax.all_to_all(shards, 'sp', 0, 0, tiled=True)  29.9 us
    ppermute x7, starting transfers between devices, moved(): return lax.ppermute(x, ('sp', 'fs'), pairs)  28.8 us
    pallas_call x7, Pallas kernels, call(): pl.pallas_call(kernel, out_shape=out_shape, in_specs=first + [vmem] * (le...  16.4 us
    all_to_all x1, waiting for transfers between devices, body(): lax.all_to_all(partial.reshape(tp, rows // tp, features), 'tp', 0, 0, til...  14.3 us
    all_to_all x1, starting transfers between devices, body(): lax.all_to_all(partial.reshape(tp, rows // tp, features), 'tp', 0, 0, til...  9.31 us
    all_to_all x1, waiting for transfers between devices, body(): ends = lax.all_to_all(end, 'sp', 0, 0, tiled=True)  7.77 us
    all_to_all x1, starting transfers between devices, body(): ends = lax.all_to_all(end, 'sp', 0, 0, tiled=True)  7.02 us
    unnamed x36, local copies, waits for them, and re-layouts  4.12 us
  transfers between devices with their start and end apart: 11, of which 2 were waited for; matrix products, arithmetic and copies ran while one was open for 3% of the time, Pallas kernels for 8%

profile of v5, /device:TPU:1, one launch (start us, length us, event | category | flops | bytes accessed | tf_op | source)
XLA Modules:
  0.0 129.8 jit_solution(7301503211335680258)
XLA Ops:
  0.6 1.6 %shard_map.195 = bf16[16,72,128]{2,1,0:T(8,128)(2,1)} custom-call(bf16[32,128]{1,0:T(8,128)(2,1)} %refs_0_.1, bf16[32,128]{1,0:T(8,128)(2,1)} %refs_1_.1, bf16[32,128]{1,0:T(8,128)(2,1)} %refs_2_.1, bf16[32,128]{1,0:T(8,128)(2,1)} %refs_3_.1, bf16[32,128]{1,0:T(8,128)(2,1)} %refs_4_.1, bf16[32,128]{1,0:T(8,128)(2,1)} %refs_5_.1), custom_call_target="tpu_custom_call" | custom-call | flops 1048576 | bytes 1048576 | tf_op jit(solution)/shard_map/pallas_call | solution.py:412
  2.2 29.9 %all_to_all.20.far_ref = bf16[16,72,128]{2,1,0:T(8,128)(2,1)S(1)} all-to-all(bf16[16,72,128]{2,1,0:T(8,128)(2,1)} %shard_map.195), channel_id=1, replica_groups=mesh['sp'=16,'fs'=4,'tp'=8] {'sp'}, dimensions={0} | all-to-all | bytes 589824 | tf_op jit(solution)/shard_map/all_to_all | solution.py:469
  32.1 0.9 shard_map.196
  33.0 10.4 %collective-permute-start.3 = (bf16[16,40,128]{2,1,0:T(8,128)(2,1)S(1)}, bf16[16,40,128]{2,1,0:T(8,128)(2,1)}, u32[]{:S(2)}, u32[]{:S(2)}) collective-permute-start(bf16[16,40,128]{2,1,0:T(8,128)(2,1)S(1)} %get-tuple-element.20), channel_id=1, source_target_pairs={{0,48},{8,56},{16,32},{24,40},{32,80},{40,88},{48,64},{56,72},{64,... | collective-permute-start | bytes 491528 | tf_op jit(solution)/shard_map/ppermute | solution.py:399
  43.4 3.7 %collective-permute-start.2 = (bf16[16,40,128]{2,1,0:T(8,128)(2,1)S(1)}, bf16[16,40,128]{2,1,0:T(8,128)(2,1)}, u32[]{:S(2)}, u32[]{:S(2)}) collective-permute-start(bf16[16,40,128]{2,1,0:T(8,128)(2,1)S(1)} %get-tuple-element.20), channel_id=1, source_target_pairs={{0,448},{8,456},{16,464},{24,472},{32,480},{40,488},{48,496},{56,5... | collective-permute-start | bytes 491528 | tf_op jit(solution)/shard_map/ppermute | solution.py:399
  47.2 2.4 %collective-permute-start.1 = (bf16[16,40,128]{2,1,0:T(8,128)(2,1)S(1)}, bf16[16,40,128]{2,1,0:T(8,128)(2,1)S(1)}, u32[]{:S(2)}, u32[]{:S(2)}) collective-permute-start(bf16[16,40,128]{2,1,0:T(8,128)(2,1)S(1)} %get-tuple-element.20), channel_id=1, source_target_pairs={{0,496},{8,504},{16,480},{24,488},{32,16},{40,24},{48,0},{56,8},{6... | collective-permute-start | bytes 491528 | tf_op jit(solution)/shard_map/ppermute | solution.py:399
  49.7 3.6 %all-to-all-start.1 = ((bf16[4,16,32,128]{3,2,1,0:T(8,128)(2,1)}), bf16[4,16,32,128]{3,2,1,0:T(8,128)(2,1)S(1)}, u32[]{:S(2)}, u32[]{:S(2)}) async-start(bf16[4,16,32,128]{3,2,1,0:T(8,128)(2,1)} %get-tuple-element.14), calls=%async_computation.1 | async-start | bytes 1048576 | tf_op jit(solution)/shard_map/all_to_all | solution.py:477
  53.5 0.6 copy-done.9
  54.1 0.0 copy-done.4
  54.1 1.2 copy-done.3
  55.3 4.6 %shard_map.194 = (bf16[256,2048]{1,0:T(8,128)(2,1)S(1)}, f32[2,256,512]{2,1,0:T(8,128)S(1)}, f32[80,512]{1,0:T(8,128)S(1)}) custom-call(f32[8]{0:T(128)S(1)} %copy-done.15, bf16[256,2048]{1,0:T(8,128)(2,1)S(1)} %bitcast.22, f32[1,2048]{1,0:T(1,128)S(1)} %bitcast.27, f32[1,256]{1,0:T(1,128)S(1)} %copy-done.4, f32[8,64]{1,0:T(8,128)S(1)} %copy-done.11, ...), custom_call_target="tpu_custom_call" | custom-call | flops 1073741824 | bytes 1048576 | tf_op jit(solution)/shard_map/pallas_call | solution.py:412
  60.0 0.7 copy-done
  60.7 0.6 copy-done.16
  61.3 1.2 pad_maximum_fusion.own_ref
  62.5 4.5 %collective-permute-start.4 = (bf16[4,16,40,128]{3,2,1,0:T(8,128)(2,1)S(1)}, bf16[4,16,40,128]{3,2,1,0:T(8,128)(2,1)}, u32[]{:S(2)}, u32[]{:S(2)}) collective-permute-start(bf16[4,16,40,128]{3,2,1,0:T(8,128)(2,1)S(1)} %pad_maximum_fusion.own_ref), channel_id=1, source_target_pairs={{0,24},{8,0},{16,8},{24,16},{32,56},{40,32},{48,40},{56,48},{64,88... | collective-permute-start | bytes 1966088 | tf_op jit(solution)/shard_map/ppermute | solution.py:399
  67.1 1.9 %collective-permute-start.5 = (bf16[4,16,40,128]{3,2,1,0:T(8,128)(2,1)S(1)}, bf16[4,16,40,128]{3,2,1,0:T(8,128)(2,1)}, u32[]{:S(2)}, u32[]{:S(2)}) collective-permute-start(bf16[4,16,40,128]{3,2,1,0:T(8,128)(2,1)S(1)} %pad_maximum_fusion.own_ref), channel_id=1, source_target_pairs={{0,8},{8,16},{16,24},{24,0},{32,40},{40,48},{48,56},{56,32},{64,72... | collective-permute-start | bytes 1966088 | tf_op jit(solution)/shard_map/ppermute | solution.py:399
  69.0 0.8 pad_maximum_fusion.1
  69.8 3.9 %collective-permute-start.6 = (bf16[2,16,40,128]{3,2,1,0:T(8,128)(2,1)}, bf16[2,16,40,128]{3,2,1,0:T(8,128)(2,1)}, u32[]{:S(2)}, u32[]{:S(2)}) collective-permute-start(bf16[2,16,40,128]{3,2,1,0:T(8,128)(2,1)} %pad_maximum_fusion.1), channel_id=1, source_target_pairs={{0,480},{8,488},{16,496},{24,504},{32,0},{40,8},{48,16},{56,24},{6... | collective-permute-start | bytes 983048 | tf_op jit(solution)/shard_map/ppermute | solution.py:399
  73.6 1.9 %collective-permute-start.7 = (bf16[2,16,40,128]{3,2,1,0:T(8,128)(2,1)}, bf16[2,16,40,128]{3,2,1,0:T(8,128)(2,1)}, u32[]{:S(2)}, u32[]{:S(2)}) collective-permute-start(bf16[2,16,40,128]{3,2,1,0:T(8,128)(2,1)} %pad_maximum_fusion.1), channel_id=1, source_target_pairs={{0,32},{8,40},{16,48},{24,56},{32,64},{40,72},{48,80},{56,88},{64,... | collective-permute-start | bytes 983048 | tf_op jit(solution)/shard_map/ppermute | solution.py:399
  75.6 0.9 copy-done.1
  76.5 2.3 %shard_map.197 = (bf16[256,128]{1,0:T(8,128)(2,1)S(1)}, f32[16,2,640]{2,1,0:T(2,128)}) custom-call(bf16[256,2048]{1,0:T(8,128)(2,1)S(1)} %get-tuple-element.13.normed_ref, bf16[4,16,32,128]{3,2,1,0:T(8,128)(2,1)S(1)} %all-to-all-done.1.w_ref, f32[2,256,512]{2,1,0:T(8,128)S(1)} %get-tuple-element.15.bar_ref, f32[80,512]{1,0:T(8,128)S(1)} %copy-done.1, ...), custom_call_target="tpu_custom_call" | custom-call | flops 536870912 | bytes 1048576 | tf_op jit(solution)/shard_map/pallas_call | solution.py:412
  78.8 7.0 %all-to-all-start.2 = ((f32[16,2,640]{2,1,0:T(2,128)}), f32[16,2,640]{2,1,0:T(2,128)S(1)}, u32[]{:S(2)}, u32[]{:S(2)}) async-start(f32[16,2,640]{2,1,0:T(2,128)} %get-tuple-element.17), calls=%async_computation.2 | async-start | bytes 163840 | tf_op jit(solution)/shard_map/all_to_all | solution.py:512
  85.8 0.8 slice_bitcast_fusion
  86.7 3.3 %collective-permute-start = (bf16[16,2048]{1,0:T(8,128)(2,1)S(1)}, bf16[16,2048]{1,0:T(8,128)(2,1)S(1)}, u32[]{:S(2)}, u32[]{:S(2)}) collective-permute-start(bf16[16,2048]{1,0:T(8,128)(2,1)S(1)} %slice_bitcast_fusion), channel_id=1, source_target_pairs={{0,32},{32,64},{64,96},{96,128},{128,160},{160,192},{192,224},{224... | collective-permute-start | bytes 196616 | tf_op jit(solution)/shard_map/ppermute | solution.py:479
  89.9 7.8 %all-to-all-done.2.ends_ref = f32[16,2,640]{2,1,0:T(2,128)S(1)} async-done(((f32[16,2,640]{2,1,0:T(2,128)}), f32[16,2,640]{2,1,0:T(2,128)S(1)}, u32[]{:S(2)}, u32[]{:S(2)}) %all-to-all-start.2) | async-done | bytes 81952 | tf_op jit(solution)/shard_map/all_to_all | solution.py:512
  97.7 2.9 %shard_map.198 = (bf16[256,128]{1,0:T(8,128)(2,1)S(1)}, f32[2,8,4]{2,1,0:T(8,128)S(1)}) custom-call(f32[16,2,640]{2,1,0:T(2,128)S(1)} %all-to-all-done.2.ends_ref, f32[2,256,512]{2,1,0:T(8,128)S(1)} %get-tuple-element.15.bar_ref, bf16[256,128]{1,0:T(8,128)(2,1)S(1)} %get-tuple-element.18.chan_ref, f32[80,512]{1,0:T(8,128)S(1)} %copy-done.2), custom_call_target="tpu_custom_call" | custom-call | flops 536870912 | bytes 1048576 | tf_op jit(solution)/shard_map/pallas_call | solution.py:412
  100.7 2.6 %shard_map.199 = (bf16[256,128]{1,0:T(8,128)(2,1)S(1)}, bf16[256,8,256]{2,1,0:T(8,128)(2,1)S(1)}) custom-call(bf16[256,2048]{1,0:T(8,128)(2,1)S(1)} %get-tuple-element.13.normed_ref, bf16[16,2048]{1,0:T(8,128)(2,1)S(1)} %collective-permute-done.halo_ref, bf16[4,16,40,128]{3,2,1,0:T(8,128)(2,1)S(1)} %pad_maximum_fusion.own_ref, ...), custom_call_target="tpu_custom_call" | custom-call | flops 536870912 | bytes 1048576 | tf_op jit(solution)/shard_map/pallas_call | solution.py:412
  103.3 1.5 %shard_map.200 = bf16[256,2048]{1,0:T(8,128)(2,1)} custom-call(bf16[256,128]{1,0:T(8,128)(2,1)S(1)} %get-tuple-element.19.state_ref, bf16[256,128]{1,0:T(8,128)(2,1)S(1)} %get-tuple-element.21.conv_ref, bf16[256,8,256]{2,1,0:T(8,128)(2,1)S(1)} %get-tuple-element.22.w_ref), custom_call_target="tpu_custom_call" | custom-call | flops 536870912 | bytes 1048576 | tf_op jit(solution)/shard_map/pallas_call | solution.py:412
  104.7 9.3 %all-to-all-start.3 = ((bf16[8,32,2048]{2,1,0:T(8,128)(2,1)}), bf16[8,32,2048]{2,1,0:T(8,128)(2,1)S(1)}, u32[]{:S(2)}, u32[]{:S(2)}) async-start(bf16[8,32,2048]{2,1,0:T(8,128)(2,1)} %bitcast.14), calls=%async_computation.3 | async-start | bytes 2097152 | tf_op jit(solution)/shard_map/all_to_all | solution.py:541
  114.0 0.7 copy.21
  114.7 14.3 %all-to-all-done.3 = bf16[8,32,2048]{2,1,0:T(8,128)(2,1)S(1)} async-done(((bf16[8,32,2048]{2,1,0:T(8,128)(2,1)}), bf16[8,32,2048]{2,1,0:T(8,128)(2,1)S(1)}, u32[]{:S(2)}, u32[]{:S(2)}) %all-to-all-start.3) | async-done | bytes 1048608 | tf_op jit(solution)/shard_map/all_to_all | solution.py:541
  129.0 0.8 reduce_sum.12
  (39 shorter events, 0.1 us)
Async XLA Ops:
  33.0 27.6 %collective-permute-start.3 = (bf16[16,40,128]{2,1,0:T(8,128)(2,1)S(1)}, bf16[16,40,128]{2,1,0:T(8,128)(2,1)}, u32[]{:S(2)}, u32[]{:S(2)}) collective-permute-start(bf16[16,40,128]{2,1,0:T(8,128)(2,1)S(1)} %get-tuple-element.20), channel_id=1, source_target_pairs={{0,48},{8,56},{16,32},{24,40},{32,80},{40,88},{48,64},{56,72},{64,... | collective-permute-start | bytes 491528 | tf_op jit(solution)/shard_map/ppermute | solution.py:399
  43.4 17.2 %collective-permute-start.2 = (bf16[16,40,128]{2,1,0:T(8,128)(2,1)S(1)}, bf16[16,40,128]{2,1,0:T(8,128)(2,1)}, u32[]{:S(2)}, u32[]{:S(2)}) collective-permute-start(bf16[16,40,128]{2,1,0:T(8,128)(2,1)S(1)} %get-tuple-element.20), channel_id=1, source_target_pairs={{0,448},{8,456},{16,464},{24,472},{32,480},{40,488},{48,496},{56,5... | collective-permute-start | bytes 491528 | tf_op jit(solution)/shard_map/ppermute | solution.py:399
  47.2 13.5 %collective-permute-start.1 = (bf16[16,40,128]{2,1,0:T(8,128)(2,1)S(1)}, bf16[16,40,128]{2,1,0:T(8,128)(2,1)S(1)}, u32[]{:S(2)}, u32[]{:S(2)}) collective-permute-start(bf16[16,40,128]{2,1,0:T(8,128)(2,1)S(1)} %get-tuple-element.20), channel_id=1, source_target_pairs={{0,496},{8,504},{16,480},{24,488},{32,16},{40,24},{48,0},{56,8},{6... | collective-permute-start | bytes 491528 | tf_op jit(solution)/shard_map/ppermute | solution.py:399
  49.6 3.8 %copy-start.5 = (f32[8,64,16]{1,2,0:T(8,128)S(1)}, f32[8,64,16]{1,2,0:T(8,128)}, u32[]{:S(2)}) copy-start(f32[8,64,16]{1,2,0:T(8,128)} %param.31) | copy-start | bytes 98308
  49.7 3.8 %copy-start.6 = (f32[8,64,16]{1,2,0:T(8,128)S(1)}, f32[8,64,16]{1,2,0:T(8,128)}, u32[]{:S(2)}) copy-start(f32[8,64,16]{1,2,0:T(8,128)} %param.32) | copy-start | bytes 98308
  49.7 3.8 %copy-start.7 = (f32[8,16,64]{2,1,0:T(8,128)S(1)}, f32[8,16,64]{2,1,0:T(8,128)}, u32[]{:S(2)}) copy-start(f32[8,16,64]{2,1,0:T(8,128)} %param.33) | copy-start | bytes 98308
  49.7 3.8 %copy-start.8 = (f32[8,16,64]{2,1,0:T(8,128)S(1)}, f32[8,16,64]{2,1,0:T(8,128)}, u32[]{:S(2)}) copy-start(f32[8,16,64]{2,1,0:T(8,128)} %param.34) | copy-start | bytes 98308
  49.7 3.8 %copy-start.10 = (f32[1,2,8,64]{3,2,1,0:T(8,128)S(1)}, f32[1,2,8,64]{3,2,1,0:T(8,128)}, u32[]{:S(2)}) copy-start(f32[1,2,8,64]{3,2,1,0:T(8,128)} %param.37) | copy-start | bytes 12292
  49.7 3.8 %copy-start.12 = (f32[8,64]{1,0:T(8,128)S(1)}, f32[8,64]{1,0:T(8,128)}, u32[]{:S(2)}) copy-start(f32[8,64]{1,0:T(8,128)} %freq_ref.1) | copy-start | bytes 6148
  49.7 3.8 %copy-start.13 = (f32[8,16]{1,0:T(8,128)S(1)}, f32[8,16]{1,0:T(8,128)}, u32[]{:S(2)}) copy-start(f32[8,16]{1,0:T(8,128)} %skip_ref.1) | copy-start | bytes 1540
  49.7 3.8 %copy-start.14 = (f32[3,128]{1,0:T(4,128)S(1)}, f32[3,128]{1,0:T(4,128)}, u32[]{:S(2)}) copy-start(f32[3,128]{1,0:T(4,128)} %taps_ref.1) | copy-start | bytes 4612
  49.7 3.8 %copy-start.15 = (f32[8]{0:T(128)S(1)}, f32[8]{0:T(128)}, u32[]{:S(2)}) copy-start(f32[8]{0:T(128)} %log_ref.1) | copy-start | bytes 100
  49.7 25.8 %all-to-all-start.1 = ((bf16[4,16,32,128]{3,2,1,0:T(8,128)(2,1)}), bf16[4,16,32,128]{3,2,1,0:T(8,128)(2,1)S(1)}, u32[]{:S(2)}, u32[]{:S(2)}) async-start(bf16[4,16,32,128]{3,2,1,0:T(8,128)(2,1)} %get-tuple-element.14), calls=%async_computation.1 | async-start | bytes 1048576 | tf_op jit(solution)/shard_map/all_to_all | solution.py:477
  53.4 0.7 copy-start.9
  53.4 0.7 copy-start.11
  53.4 0.7 copy-start.4
  54.1 1.2 copy-start.3
  60.0 0.7 copy-start
  60.6 0.7 copy-start.16
  61.3 7.7 %copy-start.17 = (bf16[16,40,128]{2,1,0:T(8,128)(2,1)S(1)}, bf16[16,40,128]{2,1,0:T(8,128)(2,1)}, u32[]{:S(2)}) copy-start(bf16[16,40,128]{2,1,0:T(8,128)(2,1)} %copy-done.16) | copy-start | bytes 491524
  62.5 38.1 %collective-permute-start.4 = (bf16[4,16,40,128]{3,2,1,0:T(8,128)(2,1)S(1)}, bf16[4,16,40,128]{3,2,1,0:T(8,128)(2,1)}, u32[]{:S(2)}, u32[]{:S(2)}) collective-permute-start(bf16[4,16,40,128]{3,2,1,0:T(8,128)(2,1)S(1)} %pad_maximum_fusion.own_ref), channel_id=1, source_target_pairs={{0,24},{8,0},{16,8},{24,16},{32,56},{40,32},{48,40},{56,48},{64,88... | collective-permute-start | bytes 1966088 | tf_op jit(solution)/shard_map/ppermute | solution.py:399
  67.1 33.6 %collective-permute-start.5 = (bf16[4,16,40,128]{3,2,1,0:T(8,128)(2,1)S(1)}, bf16[4,16,40,128]{3,2,1,0:T(8,128)(2,1)}, u32[]{:S(2)}, u32[]{:S(2)}) collective-permute-start(bf16[4,16,40,128]{3,2,1,0:T(8,128)(2,1)S(1)} %pad_maximum_fusion.own_ref), channel_id=1, source_target_pairs={{0,8},{8,16},{16,24},{24,0},{32,40},{40,48},{48,56},{56,32},{64,72... | collective-permute-start | bytes 1966088 | tf_op jit(solution)/shard_map/ppermute | solution.py:399
  69.8 30.8 %collective-permute-start.6 = (bf16[2,16,40,128]{3,2,1,0:T(8,128)(2,1)}, bf16[2,16,40,128]{3,2,1,0:T(8,128)(2,1)}, u32[]{:S(2)}, u32[]{:S(2)}) collective-permute-start(bf16[2,16,40,128]{3,2,1,0:T(8,128)(2,1)} %pad_maximum_fusion.1), channel_id=1, source_target_pairs={{0,480},{8,488},{16,496},{24,504},{32,0},{40,8},{48,16},{56,24},{6... | collective-permute-start | bytes 983048 | tf_op jit(solution)/shard_map/ppermute | solution.py:399
  73.6 27.0 %collective-permute-start.7 = (bf16[2,16,40,128]{3,2,1,0:T(8,128)(2,1)}, bf16[2,16,40,128]{3,2,1,0:T(8,128)(2,1)}, u32[]{:S(2)}, u32[]{:S(2)}) collective-permute-start(bf16[2,16,40,128]{3,2,1,0:T(8,128)(2,1)} %pad_maximum_fusion.1), channel_id=1, source_target_pairs={{0,32},{8,40},{16,48},{24,56},{32,64},{40,72},{48,80},{56,88},{64,... | collective-permute-start | bytes 983048 | tf_op jit(solution)/shard_map/ppermute | solution.py:399
  75.6 0.9 copy-start.1
  78.8 18.9 %copy-start.2 = (f32[80,512]{1,0:T(8,128)S(1)}, f32[80,512]{1,0:T(8,128)}, u32[]{:S(2)}) copy-start(f32[80,512]{1,0:T(8,128)} %copy-done) | copy-start | bytes 491524
  78.8 18.9 %all-to-all-start.2 = ((f32[16,2,640]{2,1,0:T(2,128)}), f32[16,2,640]{2,1,0:T(2,128)S(1)}, u32[]{:S(2)}, u32[]{:S(2)}) async-start(f32[16,2,640]{2,1,0:T(2,128)} %get-tuple-element.17), calls=%async_computation.2 | async-start | bytes 163840 | tf_op jit(solution)/shard_map/all_to_all | solution.py:512
  86.7 13.9 %collective-permute-start = (bf16[16,2048]{1,0:T(8,128)(2,1)S(1)}, bf16[16,2048]{1,0:T(8,128)(2,1)S(1)}, u32[]{:S(2)}, u32[]{:S(2)}) collective-permute-start(bf16[16,2048]{1,0:T(8,128)(2,1)S(1)} %slice_bitcast_fusion), channel_id=1, source_target_pairs={{0,32},{32,64},{64,96},{96,128},{128,160},{160,192},{192,224},{224... | collective-permute-start | bytes 196616 | tf_op jit(solution)/shard_map/ppermute | solution.py:479
  104.7 24.3 %all-to-all-start.3 = ((bf16[8,32,2048]{2,1,0:T(8,128)(2,1)}), bf16[8,32,2048]{2,1,0:T(8,128)(2,1)S(1)}, u32[]{:S(2)}, u32[]{:S(2)}) async-start(bf16[8,32,2048]{2,1,0:T(8,128)(2,1)} %bitcast.14), calls=%async_computation.3 | async-start | bytes 2097152 | tf_op jit(solution)/shard_map/all_to_all | solution.py:541

commit v6 on v5

--- a/solution.py
+++ b/solution.py
@@ -368,27 +368,42 @@
     taps = [packed(pack_ref, 10 + at, width) for at in range(3)]
     gain = jnp.concatenate([packed(pack_ref, 5 + at) for at in range(4)], axis=1)
     reach = len(taps) - 1
-    here = jnp.dot(normed_ref[...], w, preferred_element_type=F32).astype(BF16).astype(F32)
-    halo = normalized(halo_ref[...], gain)
-    before = jnp.dot(halo, w[:, : 2 * width], preferred_element_type=F32).astype(BF16).astype(F32)
-    gated = (here[:, :width] * here[:, width : 2 * width]).astype(BF16).astype(F32)
-    gated_before = (before[:, :width] * before[:, width:]).astype(BF16).astype(F32)
-    extended = jnp.concatenate([gated_before, gated], axis=0)
-    filtered = taps[reach] * gated
+    inputs = jnp.concatenate([normalized(halo_ref[...], gain), normed_ref[...]], axis=0)
+    here = jnp.dot(inputs, w, preferred_element_type=F32).astype(BF16).astype(F32)
+    extended = (here[:, :width] * here[:, width : 2 * width]).astype(BF16).astype(F32)
+    filtered = taps[reach] * extended[HALO:]
     for tap in range(reach):
         at = HALO - reach + tap
         filtered = filtered + taps[tap] * extended[at : at + rows]
-    mix_ref[...] = (here[:, 2 * width :] * filtered).astype(BF16)
-
-
-def out_kernel(state_ref, conv_ref, w_ref, out_ref):
-    mixes = jnp.concatenate([state_ref[...], conv_ref[...]], axis=1)
+    mix_ref[...] = (here[HALO:, 2 * width :] * filtered).astype(BF16)
+
+
+def out_kernel(state_ref, conv_ref, w_ref, mine_ref, theirs_ref):
+    chips, rows = mine_ref.shape[:2]
+    core = lax.axis_index("tp") & 1
+
+    def rows_of(ref, parity):
+        return [ref[pl.ds(pl.multiple_of((2 * x + parity) * rows, rows), rows), :] for x in range(chips)]
+
+    mixes = jnp.concatenate(
+        [
+            jnp.concatenate([*rows_of(ref, core), *rows_of(ref, 1 - core)], axis=0)
+            for ref in (state_ref, conv_ref)
+        ],
+        axis=1,
+    )
     per = 512
     tall, part, wide = w_ref.shape
     for at in range(0, tall * part, per):
         w = w_ref[at // part : (at + per) // part].reshape(per, wide)
-        product = lax.dot_general(mixes, w, NT, preferred_element_type=F32)
-        out_ref[:, at : at + per] = product.astype(BF16)
+        product = lax.dot_general(mixes, w, NT, preferred_element_type=F32).astype(BF16)
+        for x in range(chips):
+            mine_ref[x, :, at : at + per] = product[x * rows : (x + 1) * rows]
+            theirs_ref[x, :, at : at + per] = product[(chips + x) * rows : (chips + x + 1) * rows]
+
+
+def add_kernel(left_ref, right_ref, sum_ref):
+    sum_ref[...] = (left_ref[...].astype(F32) + right_ref[...].astype(F32)).astype(BF16)
 
 
 def moved(x, dz, dy):
@@ -469,10 +484,7 @@
     far = lax.all_to_all(shards, "sp", 0, 0, tiled=True)
     fs = lax.axis_size("fs")
     many, rest = call(
-        split_kernel,
-        (shape((fs, count, 4 * part, width), BF16), shape((count, 5 * part, width), BF16)),
-        1 << 20,
-        far,
+        split_kernel, (shape((fs, count, 4 * part, width), BF16), shape((count, 5 * part, width), BF16)), 1 << 20, far
     )
     state_weights = lax.all_to_all(many, "fs", 0, 0, tiled=True)
     own, up, down, left, right = all_shards(rest)
@@ -534,11 +546,13 @@
         pack,
         scratch=(pltpu.VMEM((2, rows, flat), F32),),
     )
-    partial = call(
-        out_kernel, shape((rows, features), BF16), 1 << 29, state_mix, conv_mix, out_weights
-    )
     tp = lax.axis_size("tp")
-    parts = lax.all_to_all(partial.reshape(tp, rows // tp, features), "tp", 0, 0, tiled=True)
+    piece = shape((tp // 2, rows // tp, features), BF16)
+    mine, theirs = call(out_kernel, (piece, piece), 1 << 29, state_mix, conv_mix, out_weights)
+    theirs = lax.ppermute(theirs, "tp", [(i, i ^ 1) for i in range(tp)])
+    pair = call(add_kernel, piece, 1 << 20, mine, theirs)
+    same_core = [[i for i in range(core, tp, 2)] for core in range(2)]
+    parts = lax.all_to_all(pair, "tp", 0, 0, tiled=True, axis_index_groups=same_core)
     mixed = jnp.sum(parts.astype(F32), axis=0).astype(BF16)
     return (mixed[None], closing[None])
 

time: 131 us -> 128 us (0.977)
  waiting for transfers between devices: 22.1 us -> 17.6 us
  starting transfers between devices: 52 us -> 53.7 us
    ppermute x0 -> x1, starting transfers between devices: none -> 6.91 us  [body(): theirs = lax.ppermute(theirs, 'tp', [(i, i ^ 1) for i in range(tp)])]
    all_to_all x1, waiting for transfers between devices: 14.3 us -> 8.25 us  [body(): lax.all_to_all(pair, 'tp', 0, 0, tiled=True, axis_index_groups=same_core)]
    all_to_all x1, starting transfers between devices: 9.31 us -> 4.03 us  [body(): lax.all_to_all(pair, 'tp', 0, 0, tiled=True, axis_index_groups=same_core)]
    ppermute x0 -> x1, waiting for transfers between devices: none -> 1.51 us  [body(): theirs = lax.ppermute(theirs, 'tp', [(i, i ^ 1) for i in range(tp)])]
    pallas_call x7 -> x8, Pallas kernels: 16.4 us -> 16.3 us  [call(): pl.pallas_call(kernel, out_shape=out_shape, in_specs=first + [vmem] * (le...]
  transfers between devices with their start and end apart: 11 -> 12, of which waited for: 2 -> 3; matrix products, arithmetic and copies ran while one was open for 3% -> 3% of each run, Pallas kernels for 8% -> 8%
where the time goes in v6:
time: 128 us; the launch traced here: 127 us
  starting transfers between devices  53.7 us (42%)
  blocking collectives  29.9 us (23%)
  waiting for transfers between devices  17.6 us (14%)
  Pallas kernels  16.3 us (13%)
  local copies, waits for them, and re-layouts  5.64 us (4%)
  other arithmetic  2.72 us (2%)
    all_to_all x1, blocking collectives, body(): far = lax.all_to_all(shards, 'sp', 0, 0, tiled=True)  29.9 us
    ppermute x7, starting transfers between devices, moved(): return lax.ppermute(x, ('sp', 'fs'), pairs)  28.8 us
    pallas_call x8, Pallas kernels, call(): pl.pallas_call(kernel, out_shape=out_shape, in_specs=first + [vmem] * (le...  16.3 us
    all_to_all x1, waiting for transfers between devices, body(): lax.all_to_all(pair, 'tp', 0, 0, tiled=True, axis_index_groups=same_core)  8.25 us
    all_to_all x1, waiting for transfers between devices, body(): ends = lax.all_to_all(end, 'sp', 0, 0, tiled=True)  7.77 us
    all_to_all x1, starting transfers between devices, body(): ends = lax.all_to_all(end, 'sp', 0, 0, tiled=True)  7.02 us
    ppermute x1, starting transfers between devices, body(): theirs = lax.ppermute(theirs, 'tp', [(i, i ^ 1) for i in range(tp)])  6.91 us
    unnamed x36, local copies, waits for them, and re-layouts  4.12 us
  transfers between devices with their start and end apart: 12, of which 3 were waited for; matrix products, arithmetic and copies ran while one was open for 3% of the time, Pallas kernels for 8%

profile of v6, /device:TPU:1, one launch (start us, length us, event | category | flops | bytes accessed | tf_op | source)
XLA Modules:
  0.0 126.8 jit_solution(14103782990511896995)
XLA Ops:
  0.6 1.6 %shard_map.195 = bf16[16,72,128]{2,1,0:T(8,128)(2,1)} custom-call(bf16[32,128]{1,0:T(8,128)(2,1)} %refs_0_.1, bf16[32,128]{1,0:T(8,128)(2,1)} %refs_1_.1, bf16[32,128]{1,0:T(8,128)(2,1)} %refs_2_.1, bf16[32,128]{1,0:T(8,128)(2,1)} %refs_3_.1, bf16[32,128]{1,0:T(8,128)(2,1)} %refs_4_.1, bf16[32,128]{1,0:T(8,128)(2,1)} %refs_5_.1), custom_call_target="tpu_custom_call" | custom-call | flops 1048576 | bytes 1048576 | tf_op jit(solution)/shard_map/pallas_call | solution.py:427
  2.2 29.9 %all_to_all.20.far_ref = bf16[16,72,128]{2,1,0:T(8,128)(2,1)S(1)} all-to-all(bf16[16,72,128]{2,1,0:T(8,128)(2,1)} %shard_map.195), channel_id=1, replica_groups=mesh['sp'=16,'fs'=4,'tp'=8] {'sp'}, dimensions={0} | all-to-all | bytes 589824 | tf_op jit(solution)/shard_map/all_to_all | solution.py:484
  32.1 0.9 shard_map.196
  33.1 10.4 %collective-permute-start.3 = (bf16[16,40,128]{2,1,0:T(8,128)(2,1)S(1)}, bf16[16,40,128]{2,1,0:T(8,128)(2,1)}, u32[]{:S(2)}, u32[]{:S(2)}) collective-permute-start(bf16[16,40,128]{2,1,0:T(8,128)(2,1)S(1)} %get-tuple-element.22), channel_id=1, source_target_pairs={{0,48},{8,56},{16,32},{24,40},{32,80},{40,88},{48,64},{56,72},{64,... | collective-permute-start | bytes 491528 | tf_op jit(solution)/shard_map/ppermute | solution.py:414
  43.5 3.7 %collective-permute-start.2 = (bf16[16,40,128]{2,1,0:T(8,128)(2,1)S(1)}, bf16[16,40,128]{2,1,0:T(8,128)(2,1)}, u32[]{:S(2)}, u32[]{:S(2)}) collective-permute-start(bf16[16,40,128]{2,1,0:T(8,128)(2,1)S(1)} %get-tuple-element.22), channel_id=1, source_target_pairs={{0,448},{8,456},{16,464},{24,472},{32,480},{40,488},{48,496},{56,5... | collective-permute-start | bytes 491528 | tf_op jit(solution)/shard_map/ppermute | solution.py:414
  47.2 2.4 %collective-permute-start.1 = (bf16[16,40,128]{2,1,0:T(8,128)(2,1)S(1)}, bf16[16,40,128]{2,1,0:T(8,128)(2,1)S(1)}, u32[]{:S(2)}, u32[]{:S(2)}) collective-permute-start(bf16[16,40,128]{2,1,0:T(8,128)(2,1)S(1)} %get-tuple-element.22), channel_id=1, source_target_pairs={{0,496},{8,504},{16,480},{24,488},{32,16},{40,24},{48,0},{56,8},{6... | collective-permute-start | bytes 491528 | tf_op jit(solution)/shard_map/ppermute | solution.py:414
  49.8 3.6 %all-to-all-start.1 = ((bf16[4,16,32,128]{3,2,1,0:T(8,128)(2,1)}), bf16[4,16,32,128]{3,2,1,0:T(8,128)(2,1)S(1)}, u32[]{:S(2)}, u32[]{:S(2)}) async-start(bf16[4,16,32,128]{3,2,1,0:T(8,128)(2,1)} %get-tuple-element.16), calls=%async_computation.1 | async-start | bytes 1048576 | tf_op jit(solution)/shard_map/all_to_all | solution.py:489
  54.1 1.2 copy-done.3
  55.3 4.6 %shard_map.194 = (bf16[256,2048]{1,0:T(8,128)(2,1)S(1)}, f32[2,256,512]{2,1,0:T(8,128)S(1)}, f32[80,512]{1,0:T(8,128)S(1)}) custom-call(f32[8]{0:T(128)S(1)} %copy-done.15, bf16[256,2048]{1,0:T(8,128)(2,1)S(1)} %bitcast.21, f32[1,2048]{1,0:T(1,128)S(1)} %bitcast.26, f32[1,256]{1,0:T(1,128)S(1)} %copy-done.4, f32[8,64]{1,0:T(8,128)S(1)} %copy-done.11, ...), custom_call_target="tpu_custom_call" | custom-call | flops 1073741824 | bytes 1048576 | tf_op jit(solution)/shard_map/pallas_call | solution.py:427
  60.0 0.7 copy-done
  60.7 0.7 copy-done.16
  61.3 1.2 pad_maximum_fusion.own_ref
  62.5 4.5 %collective-permute-start.4 = (bf16[4,16,40,128]{3,2,1,0:T(8,128)(2,1)S(1)}, bf16[4,16,40,128]{3,2,1,0:T(8,128)(2,1)}, u32[]{:S(2)}, u32[]{:S(2)}) collective-permute-start(bf16[4,16,40,128]{3,2,1,0:T(8,128)(2,1)S(1)} %pad_maximum_fusion.own_ref), channel_id=1, source_target_pairs={{0,24},{8,0},{16,8},{24,16},{32,56},{40,32},{48,40},{56,48},{64,88... | collective-permute-start | bytes 1966088 | tf_op jit(solution)/shard_map/ppermute | solution.py:414
  67.1 1.9 %collective-permute-start.5 = (bf16[4,16,40,128]{3,2,1,0:T(8,128)(2,1)S(1)}, bf16[4,16,40,128]{3,2,1,0:T(8,128)(2,1)}, u32[]{:S(2)}, u32[]{:S(2)}) collective-permute-start(bf16[4,16,40,128]{3,2,1,0:T(8,128)(2,1)S(1)} %pad_maximum_fusion.own_ref), channel_id=1, source_target_pairs={{0,8},{8,16},{16,24},{24,0},{32,40},{40,48},{48,56},{56,32},{64,72... | collective-permute-start | bytes 1966088 | tf_op jit(solution)/shard_map/ppermute | solution.py:414
  69.0 0.8 pad_maximum_fusion.1
  69.8 3.9 %collective-permute-start.6 = (bf16[2,16,40,128]{3,2,1,0:T(8,128)(2,1)}, bf16[2,16,40,128]{3,2,1,0:T(8,128)(2,1)}, u32[]{:S(2)}, u32[]{:S(2)}) collective-permute-start(bf16[2,16,40,128]{3,2,1,0:T(8,128)(2,1)} %pad_maximum_fusion.1), channel_id=1, source_target_pairs={{0,480},{8,488},{16,496},{24,504},{32,0},{40,8},{48,16},{56,24},{6... | collective-permute-start | bytes 983048 | tf_op jit(solution)/shard_map/ppermute | solution.py:414
  73.7 1.9 %collective-permute-start.7 = (bf16[2,16,40,128]{3,2,1,0:T(8,128)(2,1)}, bf16[2,16,40,128]{3,2,1,0:T(8,128)(2,1)}, u32[]{:S(2)}, u32[]{:S(2)}) collective-permute-start(bf16[2,16,40,128]{3,2,1,0:T(8,128)(2,1)} %pad_maximum_fusion.1), channel_id=1, source_target_pairs={{0,32},{8,40},{16,48},{24,56},{32,64},{40,72},{48,80},{56,88},{64,... | collective-permute-start | bytes 983048 | tf_op jit(solution)/shard_map/ppermute | solution.py:414
  75.6 0.9 copy-done.1
  76.6 2.3 %shard_map.197 = (bf16[256,128]{1,0:T(8,128)(2,1)S(1)}, f32[16,2,640]{2,1,0:T(2,128)}) custom-call(bf16[256,2048]{1,0:T(8,128)(2,1)S(1)} %get-tuple-element.15.normed_ref, bf16[4,16,32,128]{3,2,1,0:T(8,128)(2,1)S(1)} %all-to-all-done.1.w_ref, f32[2,256,512]{2,1,0:T(8,128)S(1)} %get-tuple-element.17.bar_ref, f32[80,512]{1,0:T(8,128)S(1)} %copy-done.1, ...), custom_call_target="tpu_custom_call" | custom-call | flops 536870912 | bytes 1048576 | tf_op jit(solution)/shard_map/pallas_call | solution.py:427
  78.8 7.0 %all-to-all-start.2 = ((f32[16,2,640]{2,1,0:T(2,128)}), f32[16,2,640]{2,1,0:T(2,128)S(1)}, u32[]{:S(2)}, u32[]{:S(2)}) async-start(f32[16,2,640]{2,1,0:T(2,128)} %get-tuple-element.19), calls=%async_computation.2 | async-start | bytes 163840 | tf_op jit(solution)/shard_map/all_to_all | solution.py:524
  85.9 0.8 slice_bitcast_fusion
  86.7 3.3 %collective-permute-start = (bf16[16,2048]{1,0:T(8,128)(2,1)S(1)}, bf16[16,2048]{1,0:T(8,128)(2,1)S(1)}, u32[]{:S(2)}, u32[]{:S(2)}) collective-permute-start(bf16[16,2048]{1,0:T(8,128)(2,1)S(1)} %slice_bitcast_fusion), channel_id=1, source_target_pairs={{0,32},{32,64},{64,96},{96,128},{128,160},{160,192},{192,224},{224... | collective-permute-start | bytes 196616 | tf_op jit(solution)/shard_map/ppermute | solution.py:491
  90.0 7.8 %all-to-all-done.2.ends_ref = f32[16,2,640]{2,1,0:T(2,128)S(1)} async-done(((f32[16,2,640]{2,1,0:T(2,128)}), f32[16,2,640]{2,1,0:T(2,128)S(1)}, u32[]{:S(2)}, u32[]{:S(2)}) %all-to-all-start.2) | async-done | bytes 81952 | tf_op jit(solution)/shard_map/all_to_all | solution.py:524
  97.7 2.9 %shard_map.198 = (bf16[256,128]{1,0:T(8,128)(2,1)S(1)}, f32[2,8,4]{2,1,0:T(8,128)S(1)}) custom-call(f32[16,2,640]{2,1,0:T(2,128)S(1)} %all-to-all-done.2.ends_ref, f32[2,256,512]{2,1,0:T(8,128)S(1)} %get-tuple-element.17.bar_ref, bf16[256,128]{1,0:T(8,128)(2,1)S(1)} %get-tuple-element.20.chan_ref, f32[80,512]{1,0:T(8,128)S(1)} %copy-done.2), custom_call_target="tpu_custom_call" | custom-call | flops 536870912 | bytes 1048576 | tf_op jit(solution)/shard_map/pallas_call | solution.py:427
  100.7 2.6 %shard_map.199 = (bf16[256,128]{1,0:T(8,128)(2,1)S(1)}, bf16[256,8,256]{2,1,0:T(8,128)(2,1)S(1)}) custom-call(bf16[256,2048]{1,0:T(8,128)(2,1)S(1)} %get-tuple-element.15.normed_ref, bf16[16,2048]{1,0:T(8,128)(2,1)S(1)} %collective-permute-done.halo_ref, bf16[4,16,40,128]{3,2,1,0:T(8,128)(2,1)S(1)} %pad_maximum_fusion.own_ref, ...), custom_call_target="tpu_custom_call" | custom-call | flops 536870912 | bytes 1048576 | tf_op jit(solution)/shard_map/pallas_call | solution.py:427
  103.7 6.9 %collective-permute-start.8 = (bf16[4,32,2048]{2,1,0:T(8,128)(2,1)S(1)}, bf16[4,32,2048]{2,1,0:T(8,128)(2,1)S(1)}, u32[]{:S(2)}, u32[]{:S(2)}) collective-permute-start(bf16[4,32,2048]{2,1,0:T(8,128)(2,1)S(1)} %get-tuple-element.26), channel_id=1, source_target_pairs={{0,1},{1,0},{2,3},{3,2},{4,5},{5,4},{6,7},{7,6},{8,9},{9,8},{10,11... | collective-permute-start | bytes 1572872 | tf_op jit(solution)/shard_map/ppermute | solution.py:552
  110.7 1.5 %collective-permute-done.8.right_ref = bf16[4,32,2048]{2,1,0:T(8,128)(2,1)S(1)} collective-permute-done((bf16[4,32,2048]{2,1,0:T(8,128)(2,1)S(1)}, bf16[4,32,2048]{2,1,0:T(8,128)(2,1)S(1)}, u32[]{:S(2)}, u32[]{:S(2)}) %collective-permute-start.8) | collective-permute-done | bytes 524320 | tf_op jit(solution)/shard_map/ppermute | solution.py:552
  112.2 0.9 shard_map.201
  113.1 4.0 %all-to-all-start.3 = ((bf16[4,32,2048]{2,1,0:T(8,128)(2,1)}), bf16[4,32,2048]{2,1,0:T(8,128)(2,1)S(1)}, u32[]{:S(2)}, u32[]{:S(2)}) async-start(bf16[4,32,2048]{2,1,0:T(8,128)(2,1)} %shard_map.201), calls=%async_computation.3 | async-start | bytes 1048576 | tf_op jit(solution)/shard_map/all_to_all | solution.py:555
  117.1 0.7 copy.21
  117.8 8.2 %all-to-all-done.3 = bf16[4,32,2048]{2,1,0:T(8,128)(2,1)S(1)} async-done(((bf16[4,32,2048]{2,1,0:T(8,128)(2,1)}), bf16[4,32,2048]{2,1,0:T(8,128)(2,1)S(1)}, u32[]{:S(2)}, u32[]{:S(2)}) %all-to-all-start.3) | async-done | bytes 524320 | tf_op jit(solution)/shard_map/all_to_all | solution.py:555
  126.0 0.7 reduce_sum.12
  (42 shorter events, 1.2 us)
Async XLA Ops:
  33.1 27.6 %collective-permute-start.3 = (bf16[16,40,128]{2,1,0:T(8,128)(2,1)S(1)}, bf16[16,40,128]{2,1,0:T(8,128)(2,1)}, u32[]{:S(2)}, u32[]{:S(2)}) collective-permute-start(bf16[16,40,128]{2,1,0:T(8,128)(2,1)S(1)} %get-tuple-element.22), channel_id=1, source_target_pairs={{0,48},{8,56},{16,32},{24,40},{32,80},{40,88},{48,64},{56,72},{64,... | collective-permute-start | bytes 491528 | tf_op jit(solution)/shard_map/ppermute | solution.py:414
  43.5 17.2 %collective-permute-start.2 = (bf16[16,40,128]{2,1,0:T(8,128)(2,1)S(1)}, bf16[16,40,128]{2,1,0:T(8,128)(2,1)}, u32[]{:S(2)}, u32[]{:S(2)}) collective-permute-start(bf16[16,40,128]{2,1,0:T(8,128)(2,1)S(1)} %get-tuple-element.22), channel_id=1, source_target_pairs={{0,448},{8,456},{16,464},{24,472},{32,480},{40,488},{48,496},{56,5... | collective-permute-start | bytes 491528 | tf_op jit(solution)/shard_map/ppermute | solution.py:414
  47.2 13.5 %collective-permute-start.1 = (bf16[16,40,128]{2,1,0:T(8,128)(2,1)S(1)}, bf16[16,40,128]{2,1,0:T(8,128)(2,1)S(1)}, u32[]{:S(2)}, u32[]{:S(2)}) collective-permute-start(bf16[16,40,128]{2,1,0:T(8,128)(2,1)S(1)} %get-tuple-element.22), channel_id=1, source_target_pairs={{0,496},{8,504},{16,480},{24,488},{32,16},{40,24},{48,0},{56,8},{6... | collective-permute-start | bytes 491528 | tf_op jit(solution)/shard_map/ppermute | solution.py:414
  49.7 3.8 %copy-start.5 = (f32[8,64,16]{1,2,0:T(8,128)S(1)}, f32[8,64,16]{1,2,0:T(8,128)}, u32[]{:S(2)}) copy-start(f32[8,64,16]{1,2,0:T(8,128)} %param.31) | copy-start | bytes 98308
  49.7 3.8 %copy-start.6 = (f32[8,64,16]{1,2,0:T(8,128)S(1)}, f32[8,64,16]{1,2,0:T(8,128)}, u32[]{:S(2)}) copy-start(f32[8,64,16]{1,2,0:T(8,128)} %param.32) | copy-start | bytes 98308
  49.7 3.8 %copy-start.7 = (f32[8,16,64]{2,1,0:T(8,128)S(1)}, f32[8,16,64]{2,1,0:T(8,128)}, u32[]{:S(2)}) copy-start(f32[8,16,64]{2,1,0:T(8,128)} %param.33) | copy-start | bytes 98308
  49.7 3.8 %copy-start.8 = (f32[8,16,64]{2,1,0:T(8,128)S(1)}, f32[8,16,64]{2,1,0:T(8,128)}, u32[]{:S(2)}) copy-start(f32[8,16,64]{2,1,0:T(8,128)} %param.34) | copy-start | bytes 98308
  49.7 3.8 %copy-start.10 = (f32[1,2,8,64]{3,2,1,0:T(8,128)S(1)}, f32[1,2,8,64]{3,2,1,0:T(8,128)}, u32[]{:S(2)}) copy-start(f32[1,2,8,64]{3,2,1,0:T(8,128)} %param.37) | copy-start | bytes 12292
  49.7 3.8 %copy-start.12 = (f32[8,64]{1,0:T(8,128)S(1)}, f32[8,64]{1,0:T(8,128)}, u32[]{:S(2)}) copy-start(f32[8,64]{1,0:T(8,128)} %freq_ref.1) | copy-start | bytes 6148
  49.7 3.8 %copy-start.13 = (f32[8,16]{1,0:T(8,128)S(1)}, f32[8,16]{1,0:T(8,128)}, u32[]{:S(2)}) copy-start(f32[8,16]{1,0:T(8,128)} %skip_ref.1) | copy-start | bytes 1540
  49.8 3.8 %copy-start.14 = (f32[3,128]{1,0:T(4,128)S(1)}, f32[3,128]{1,0:T(4,128)}, u32[]{:S(2)}) copy-start(f32[3,128]{1,0:T(4,128)} %taps_ref.1) | copy-start | bytes 4612
  49.8 3.8 %copy-start.15 = (f32[8]{0:T(128)S(1)}, f32[8]{0:T(128)}, u32[]{:S(2)}) copy-start(f32[8]{0:T(128)} %log_ref.1) | copy-start | bytes 100
  49.8 25.8 %all-to-all-start.1 = ((bf16[4,16,32,128]{3,2,1,0:T(8,128)(2,1)}), bf16[4,16,32,128]{3,2,1,0:T(8,128)(2,1)S(1)}, u32[]{:S(2)}, u32[]{:S(2)}) async-start(bf16[4,16,32,128]{3,2,1,0:T(8,128)(2,1)} %get-tuple-element.16), calls=%async_computation.1 | async-start | bytes 1048576 | tf_op jit(solution)/shard_map/all_to_all | solution.py:489
  53.4 0.7 copy-start.9
  53.4 0.7 copy-start.11
  53.4 0.7 copy-start.4
  54.1 1.2 copy-start.3
  60.0 0.7 copy-start
  60.7 0.7 copy-start.16
  61.3 7.7 %copy-start.17 = (bf16[16,40,128]{2,1,0:T(8,128)(2,1)S(1)}, bf16[16,40,128]{2,1,0:T(8,128)(2,1)}, u32[]{:S(2)}) copy-start(bf16[16,40,128]{2,1,0:T(8,128)(2,1)} %copy-done.16) | copy-start | bytes 491524
  62.5 38.2 %collective-permute-start.4 = (bf16[4,16,40,128]{3,2,1,0:T(8,128)(2,1)S(1)}, bf16[4,16,40,128]{3,2,1,0:T(8,128)(2,1)}, u32[]{:S(2)}, u32[]{:S(2)}) collective-permute-start(bf16[4,16,40,128]{3,2,1,0:T(8,128)(2,1)S(1)} %pad_maximum_fusion.own_ref), channel_id=1, source_target_pairs={{0,24},{8,0},{16,8},{24,16},{32,56},{40,32},{48,40},{56,48},{64,88... | collective-permute-start | bytes 1966088 | tf_op jit(solution)/shard_map/ppermute | solution.py:414
  67.1 33.6 %collective-permute-start.5 = (bf16[4,16,40,128]{3,2,1,0:T(8,128)(2,1)S(1)}, bf16[4,16,40,128]{3,2,1,0:T(8,128)(2,1)}, u32[]{:S(2)}, u32[]{:S(2)}) collective-permute-start(bf16[4,16,40,128]{3,2,1,0:T(8,128)(2,1)S(1)} %pad_maximum_fusion.own_ref), channel_id=1, source_target_pairs={{0,8},{8,16},{16,24},{24,0},{32,40},{40,48},{48,56},{56,32},{64,72... | collective-permute-start | bytes 1966088 | tf_op jit(solution)/shard_map/ppermute | solution.py:414
  69.8 30.9 %collective-permute-start.6 = (bf16[2,16,40,128]{3,2,1,0:T(8,128)(2,1)}, bf16[2,16,40,128]{3,2,1,0:T(8,128)(2,1)}, u32[]{:S(2)}, u32[]{:S(2)}) collective-permute-start(bf16[2,16,40,128]{3,2,1,0:T(8,128)(2,1)} %pad_maximum_fusion.1), channel_id=1, source_target_pairs={{0,480},{8,488},{16,496},{24,504},{32,0},{40,8},{48,16},{56,24},{6... | collective-permute-start | bytes 983048 | tf_op jit(solution)/shard_map/ppermute | solution.py:414
  73.7 27.0 %collective-permute-start.7 = (bf16[2,16,40,128]{3,2,1,0:T(8,128)(2,1)}, bf16[2,16,40,128]{3,2,1,0:T(8,128)(2,1)}, u32[]{:S(2)}, u32[]{:S(2)}) collective-permute-start(bf16[2,16,40,128]{3,2,1,0:T(8,128)(2,1)} %pad_maximum_fusion.1), channel_id=1, source_target_pairs={{0,32},{8,40},{16,48},{24,56},{32,64},{40,72},{48,80},{56,88},{64,... | collective-permute-start | bytes 983048 | tf_op jit(solution)/shard_map/ppermute | solution.py:414
  75.6 0.9 copy-start.1
  78.8 18.9 %copy-start.2 = (f32[80,512]{1,0:T(8,128)S(1)}, f32[80,512]{1,0:T(8,128)}, u32[]{:S(2)}) copy-start(f32[80,512]{1,0:T(8,128)} %copy-done) | copy-start | bytes 491524
  78.8 18.9 %all-to-all-start.2 = ((f32[16,2,640]{2,1,0:T(2,128)}), f32[16,2,640]{2,1,0:T(2,128)S(1)}, u32[]{:S(2)}, u32[]{:S(2)}) async-start(f32[16,2,640]{2,1,0:T(2,128)} %get-tuple-element.19), calls=%async_computation.2 | async-start | bytes 163840 | tf_op jit(solution)/shard_map/all_to_all | solution.py:524
  86.7 13.9 %collective-permute-start = (bf16[16,2048]{1,0:T(8,128)(2,1)S(1)}, bf16[16,2048]{1,0:T(8,128)(2,1)S(1)}, u32[]{:S(2)}, u32[]{:S(2)}) collective-permute-start(bf16[16,2048]{1,0:T(8,128)(2,1)S(1)} %slice_bitcast_fusion), channel_id=1, source_target_pairs={{0,32},{32,64},{64,96},{96,128},{128,160},{160,192},{192,224},{224... | collective-permute-start | bytes 196616 | tf_op jit(solution)/shard_map/ppermute | solution.py:491
  103.7 8.4 %collective-permute-start.8 = (bf16[4,32,2048]{2,1,0:T(8,128)(2,1)S(1)}, bf16[4,32,2048]{2,1,0:T(8,128)(2,1)S(1)}, u32[]{:S(2)}, u32[]{:S(2)}) collective-permute-start(bf16[4,32,2048]{2,1,0:T(8,128)(2,1)S(1)} %get-tuple-element.26), channel_id=1, source_target_pairs={{0,1},{1,0},{2,3},{3,2},{4,5},{5,4},{6,7},{7,6},{8,9},{9,8},{10,11... | collective-permute-start | bytes 1572872 | tf_op jit(solution)/shard_map/ppermute | solution.py:552
  113.1 12.9 %all-to-all-start.3 = ((bf16[4,32,2048]{2,1,0:T(8,128)(2,1)}), bf16[4,32,2048]{2,1,0:T(8,128)(2,1)S(1)}, u32[]{:S(2)}, u32[]{:S(2)}) async-start(bf16[4,32,2048]{2,1,0:T(8,128)(2,1)} %shard_map.201), calls=%async_computation.3 | async-start | bytes 1048576 | tf_op jit(solution)/shard_map/all_to_all | solution.py:555

commit v7 on v6

--- a/solution.py
+++ b/solution.py
@@ -337,7 +337,8 @@
 
 
 def conv_kernel(
-    normed_ref, halo_ref, own_ref, up_ref, down_ref, left_ref, right_ref, pack_ref, mix_ref, weights_ref, w_ref
+    state_ref, normed_ref, halo_ref, own_ref, up_ref, down_ref, left_ref, right_ref, pack_ref,
+    mine_ref, theirs_ref, mix_ref, weights_ref, w_ref,
 ):
     width = mix_ref.shape[1]
     rows = normed_ref.shape[0]
@@ -376,9 +377,10 @@
         at = HALO - reach + tap
         filtered = filtered + taps[tap] * extended[at : at + rows]
     mix_ref[...] = (here[HALO:, 2 * width :] * filtered).astype(BF16)
-
-
-def out_kernel(state_ref, conv_ref, w_ref, mine_ref, theirs_ref):
+    output(state_ref, mix_ref, weights_ref, mine_ref, theirs_ref)
+
+
+def output(state_ref, conv_ref, w_ref, mine_ref, theirs_ref):
     chips, rows = mine_ref.shape[:2]
     core = lax.axis_index("tp") & 1
 
@@ -402,8 +404,12 @@
             theirs_ref[x, :, at : at + per] = product[(chips + x) * rows : (chips + x + 1) * rows]
 
 
-def add_kernel(left_ref, right_ref, sum_ref):
-    sum_ref[...] = (left_ref[...].astype(F32) + right_ref[...].astype(F32)).astype(BF16)
+def add_kernel(left_ref, right_ref, *out_refs):
+    chips = len(out_refs)
+    chip = lax.axis_index("tp") >> 1
+    for k, ref in enumerate(out_refs):
+        to = (chip + k) & (chips - 1)
+        ref[...] = (left_ref[to].astype(F32) + right_ref[to].astype(F32)).astype(BF16)
 
 
 def moved(x, dz, dy):
@@ -484,7 +490,10 @@
     far = lax.all_to_all(shards, "sp", 0, 0, tiled=True)
     fs = lax.axis_size("fs")
     many, rest = call(
-        split_kernel, (shape((fs, count, 4 * part, width), BF16), shape((count, 5 * part, width), BF16)), 1 << 20, far
+        split_kernel,
+        (shape((fs, count, 4 * part, width), BF16), shape((count, 5 * part, width), BF16)),
+        1 << 20,
+        far,
     )
     state_weights = lax.all_to_all(many, "fs", 0, 0, tiled=True)
     own, up, down, left, right = all_shards(rest)
@@ -522,20 +531,6 @@
         scratch=(pltpu.VMEM((2, rows, flat), F32),),
     )
     ends = lax.all_to_all(end, "sp", 0, 0, tiled=True)
-    conv_mix, out_weights = call(
-        conv_kernel,
-        (shape((rows, width), BF16), shape((features // part, part, 2 * width), BF16)),
-        1 << 29,
-        normed,
-        edge,
-        own,
-        up,
-        down,
-        left,
-        right,
-        pack,
-        scratch=(pltpu.VMEM((features // part, part, 3 * width), BF16),),
-    )
     state_mix, closing = call(
         functools.partial(read_kernel, groups),
         (shape((rows, width), BF16), shape((2, groups, states // count))),
@@ -547,13 +542,34 @@
         scratch=(pltpu.VMEM((2, rows, flat), F32),),
     )
     tp = lax.axis_size("tp")
-    piece = shape((tp // 2, rows // tp, features), BF16)
-    mine, theirs = call(out_kernel, (piece, piece), 1 << 29, state_mix, conv_mix, out_weights)
+    chips = tp // 2
+    piece = shape((chips, rows // tp, features), BF16)
+    mine, theirs = call(
+        conv_kernel,
+        (piece, piece),
+        1 << 29,
+        state_mix,
+        normed,
+        edge,
+        own,
+        up,
+        down,
+        left,
+        right,
+        pack,
+        scratch=(
+            pltpu.VMEM((rows, width), BF16),
+            pltpu.VMEM((features // part, part, 2 * width), BF16),
+            pltpu.VMEM((features // part, part, 3 * width), BF16),
+        ),
+    )
     theirs = lax.ppermute(theirs, "tp", [(i, i ^ 1) for i in range(tp)])
-    pair = call(add_kernel, piece, 1 << 20, mine, theirs)
-    same_core = [[i for i in range(core, tp, 2)] for core in range(2)]
-    parts = lax.all_to_all(pair, "tp", 0, 0, tiled=True, axis_index_groups=same_core)
-    mixed = jnp.sum(parts.astype(F32), axis=0).astype(BF16)
+    sent = call(add_kernel, (shape((rows // tp, features), BF16),) * chips, 1 << 20, mine, theirs)
+    total = sent[0].astype(F32)
+    for k in range(1, chips):
+        pairs = [(i, (i + 2 * k) % tp) for i in range(tp)]
+        total = total + lax.ppermute(sent[k], "tp", pairs).astype(F32)
+    mixed = total.astype(BF16)
     return (mixed[None], closing[None])
 
 

time: 128 us -> 128 us (level)
  starting transfers between devices: 53.7 us -> 60.5 us
  waiting for transfers between devices: 17.6 us -> 13.3 us
  local copies, waits for them, and re-layouts: 5.64 us -> 4.06 us
    ppermute x0 -> x3, starting transfers between devices: none -> 9.94 us  [body(): total = total + lax.ppermute(sent[k], 'tp', pairs).astype(F32)]
    all_to_all x1 -> x0, waiting for transfers between devices: 8.25 us -> none  [body(): lax.all_to_all(pair, 'tp', 0, 0, tiled=True, axis_index_groups=same_core)]
    all_to_all x1 -> x0, starting transfers between devices: 4.03 us -> none  [body(): lax.all_to_all(pair, 'tp', 0, 0, tiled=True, axis_index_groups=same_core)]
    ppermute x0 -> x3, waiting for transfers between devices: none -> 4.02 us  [body(): total = total + lax.ppermute(sent[k], 'tp', pairs).astype(F32)]
    unnamed x36 -> x34, local copies, waits for them, and re-layouts: 4.12 us -> 2.54 us
    pallas_call x8 -> x7, Pallas kernels: 16.3 us -> 15.3 us  [call(): pl.pallas_call(kernel, out_shape=out_shape, in_specs=first + [vmem] * (le...]
  transfers between devices with their start and end apart: 12 -> 14, of which waited for: 3 -> 4; matrix products, arithmetic and copies ran while one was open for 3% -> 3% of each run, Pallas kernels for 8% -> 8%
where the time goes in v7:
time: 128 us; the launch traced here: 127 us
  starting transfers between devices  60.5 us (47%)
  blocking collectives  29.9 us (23%)
  Pallas kernels  15.3 us (12%)
  waiting for transfers between devices  13.3 us (10%)
  local copies, waits for them, and re-layouts  4.06 us (3%)
  other arithmetic  2.68 us (2%)
    ppermute x7, starting transfers between devices, moved(): return lax.ppermute(x, ('sp', 'fs'), pairs)  30.1 us
    all_to_all x1, blocking collectives, body(): far = lax.all_to_all(shards, 'sp', 0, 0, tiled=True)  29.9 us
    pallas_call x7, Pallas kernels, call(): pl.pallas_call(kernel, out_shape=out_shape, in_specs=first + [vmem] * (le...  15.3 us
    ppermute x3, starting transfers between devices, body(): total = total + lax.ppermute(sent[k], 'tp', pairs).astype(F32)  9.94 us
    all_to_all x1, waiting for transfers between devices, body(): ends = lax.all_to_all(end, 'sp', 0, 0, tiled=True)  7.77 us
    ppermute x1, starting transfers between devices, body(): theirs = lax.ppermute(theirs, 'tp', [(i, i ^ 1) for i in range(tp)])  6.91 us
    all_to_all x1, starting transfers between devices, body(): ends = lax.all_to_all(end, 'sp', 0, 0, tiled=True)  6.69 us
    ppermute x3, waiting for transfers between devices, body(): total = total + lax.ppermute(sent[k], 'tp', pairs).astype(F32)  4.02 us
  transfers between devices with their start and end apart: 14, of which 4 were waited for; matrix products, arithmetic and copies ran while one was open for 3% of the time, Pallas kernels for 8%

profile of v7, /device:TPU:1, one launch (start us, length us, event | category | flops | bytes accessed | tf_op | source)
XLA Modules:
  0.0 126.8 jit_solution(11454416464594247960)
XLA Ops:
  0.6 1.6 %shard_map.195 = bf16[16,72,128]{2,1,0:T(8,128)(2,1)} custom-call(bf16[32,128]{1,0:T(8,128)(2,1)} %refs_0_.1, bf16[32,128]{1,0:T(8,128)(2,1)} %refs_1_.1, bf16[32,128]{1,0:T(8,128)(2,1)} %refs_2_.1, bf16[32,128]{1,0:T(8,128)(2,1)} %refs_3_.1, bf16[32,128]{1,0:T(8,128)(2,1)} %refs_4_.1, bf16[32,128]{1,0:T(8,128)(2,1)} %refs_5_.1), custom_call_target="tpu_custom_call" | custom-call | flops 1048576 | bytes 1048576 | tf_op jit(solution)/shard_map/pallas_call | solution.py:433
  2.2 29.9 %all_to_all.15.far_ref = bf16[16,72,128]{2,1,0:T(8,128)(2,1)S(1)} all-to-all(bf16[16,72,128]{2,1,0:T(8,128)(2,1)} %shard_map.195), channel_id=1, replica_groups=mesh['sp'=16,'fs'=4,'tp'=8] {'sp'}, dimensions={0} | all-to-all | bytes 589824 | tf_op jit(solution)/shard_map/all_to_all | solution.py:490
  32.1 0.9 shard_map.196
  33.0 11.1 %collective-permute-start.1 = (bf16[16,40,128]{2,1,0:T(8,128)(2,1)S(1)}, bf16[16,40,128]{2,1,0:T(8,128)(2,1)S(1)}, u32[]{:S(2)}, u32[]{:S(2)}) collective-permute-start(bf16[16,40,128]{2,1,0:T(8,128)(2,1)S(1)} %get-tuple-element.24), channel_id=1, source_target_pairs={{0,496},{8,504},{16,480},{24,488},{32,16},{40,24},{48,0},{56,8},{6... | collective-permute-start | bytes 491528 | tf_op jit(solution)/shard_map/ppermute | solution.py:420
  44.1 3.6 %collective-permute-start.2 = (bf16[16,40,128]{2,1,0:T(8,128)(2,1)S(1)}, bf16[16,40,128]{2,1,0:T(8,128)(2,1)}, u32[]{:S(2)}, u32[]{:S(2)}) collective-permute-start(bf16[16,40,128]{2,1,0:T(8,128)(2,1)S(1)} %get-tuple-element.24), channel_id=1, source_target_pairs={{0,448},{8,456},{16,464},{24,472},{32,480},{40,488},{48,496},{56,5... | collective-permute-start | bytes 491528 | tf_op jit(solution)/shard_map/ppermute | solution.py:420
  47.7 1.9 %collective-permute-start.3 = (bf16[16,40,128]{2,1,0:T(8,128)(2,1)S(1)}, bf16[16,40,128]{2,1,0:T(8,128)(2,1)}, u32[]{:S(2)}, u32[]{:S(2)}) collective-permute-start(bf16[16,40,128]{2,1,0:T(8,128)(2,1)S(1)} %get-tuple-element.24), channel_id=1, source_target_pairs={{0,48},{8,56},{16,32},{24,40},{32,80},{40,88},{48,64},{56,72},{64,... | collective-permute-start | bytes 491528 | tf_op jit(solution)/shard_map/ppermute | solution.py:420
  49.8 3.6 %all-to-all-start.1 = ((bf16[4,16,32,128]{3,2,1,0:T(8,128)(2,1)}), bf16[4,16,32,128]{3,2,1,0:T(8,128)(2,1)S(1)}, u32[]{:S(2)}, u32[]{:S(2)}) async-start(bf16[4,16,32,128]{3,2,1,0:T(8,128)(2,1)} %get-tuple-element.18), calls=%async_computation.1 | async-start | bytes 1048576 | tf_op jit(solution)/shard_map/all_to_all | solution.py:498
  53.5 0.6 copy-done.8
  54.1 1.2 copy-done.2
  55.3 4.6 %shard_map.194 = (bf16[256,2048]{1,0:T(8,128)(2,1)S(1)}, f32[2,256,512]{2,1,0:T(8,128)S(1)}, f32[80,512]{1,0:T(8,128)S(1)}) custom-call(f32[8]{0:T(128)S(1)} %copy-done.14, bf16[256,2048]{1,0:T(8,128)(2,1)S(1)} %bitcast.22, f32[1,2048]{1,0:T(1,128)S(1)} %bitcast.27, f32[1,256]{1,0:T(1,128)S(1)} %copy-done.3, f32[8,64]{1,0:T(8,128)S(1)} %copy-done.10, ...), custom_call_target="tpu_custom_call" | custom-call | flops 1073741824 | bytes 1048576 | tf_op jit(solution)/shard_map/pallas_call | solution.py:433
  60.0 0.6 copy-done.15
  60.7 1.2 pad_maximum_fusion.own_ref
  61.9 4.5 %collective-permute-start.4 = (bf16[4,16,40,128]{3,2,1,0:T(8,128)(2,1)S(1)}, bf16[4,16,40,128]{3,2,1,0:T(8,128)(2,1)}, u32[]{:S(2)}, u32[]{:S(2)}) collective-permute-start(bf16[4,16,40,128]{3,2,1,0:T(8,128)(2,1)S(1)} %pad_maximum_fusion.own_ref), channel_id=1, source_target_pairs={{0,24},{8,0},{16,8},{24,16},{32,56},{40,32},{48,40},{56,48},{64,88... | collective-permute-start | bytes 1966088 | tf_op jit(solution)/shard_map/ppermute | solution.py:420
  66.4 1.9 %collective-permute-start.5 = (bf16[4,16,40,128]{3,2,1,0:T(8,128)(2,1)S(1)}, bf16[4,16,40,128]{3,2,1,0:T(8,128)(2,1)}, u32[]{:S(2)}, u32[]{:S(2)}) collective-permute-start(bf16[4,16,40,128]{3,2,1,0:T(8,128)(2,1)S(1)} %pad_maximum_fusion.own_ref), channel_id=1, source_target_pairs={{0,8},{8,16},{16,24},{24,0},{32,40},{40,48},{48,56},{56,32},{64,72... | collective-permute-start | bytes 1966088 | tf_op jit(solution)/shard_map/ppermute | solution.py:420
  68.4 0.8 pad_maximum_fusion.1
  69.1 5.1 %collective-permute-start.6 = (bf16[2,16,40,128]{3,2,1,0:T(8,128)(2,1)}, bf16[2,16,40,128]{3,2,1,0:T(8,128)(2,1)}, u32[]{:S(2)}, u32[]{:S(2)}) collective-permute-start(bf16[2,16,40,128]{3,2,1,0:T(8,128)(2,1)} %pad_maximum_fusion.1), channel_id=1, source_target_pairs={{0,480},{8,488},{16,496},{24,504},{32,0},{40,8},{48,16},{56,24},{6... | collective-permute-start | bytes 983048 | tf_op jit(solution)/shard_map/ppermute | solution.py:420
  74.2 1.9 %collective-permute-start.7 = (bf16[2,16,40,128]{3,2,1,0:T(8,128)(2,1)}, bf16[2,16,40,128]{3,2,1,0:T(8,128)(2,1)}, u32[]{:S(2)}, u32[]{:S(2)}) collective-permute-start(bf16[2,16,40,128]{3,2,1,0:T(8,128)(2,1)} %pad_maximum_fusion.1), channel_id=1, source_target_pairs={{0,32},{8,40},{16,48},{24,56},{32,64},{40,72},{48,80},{56,88},{64,... | collective-permute-start | bytes 983048 | tf_op jit(solution)/shard_map/ppermute | solution.py:420
  76.2 2.3 %shard_map.197 = (bf16[256,128]{1,0:T(8,128)(2,1)S(1)}, f32[16,2,640]{2,1,0:T(2,128)}) custom-call(bf16[256,2048]{1,0:T(8,128)(2,1)S(1)} %get-tuple-element.17.normed_ref, bf16[4,16,32,128]{3,2,1,0:T(8,128)(2,1)S(1)} %all-to-all-done.1.w_ref, f32[2,256,512]{2,1,0:T(8,128)S(1)} %get-tuple-element.19.bar_ref, f32[80,512]{1,0:T(8,128)S(1)} %get-tuple-element.20.pack_ref, ...), custom_call_target="tpu_custom_call" | custom-call | flops 536870912 | bytes 1048576 | tf_op jit(solution)/shard_map/pallas_call | solution.py:433
  78.4 6.7 %all-to-all-start.2 = ((f32[16,2,640]{2,1,0:T(2,128)}), f32[16,2,640]{2,1,0:T(2,128)S(1)}, u32[]{:S(2)}, u32[]{:S(2)}) async-start(f32[16,2,640]{2,1,0:T(2,128)} %get-tuple-element.21), calls=%async_computation.2 | async-start | bytes 163840 | tf_op jit(solution)/shard_map/all_to_all | solution.py:533
  85.1 0.8 slice_bitcast_fusion
  86.0 3.3 %collective-permute-start = (bf16[16,2048]{1,0:T(8,128)(2,1)S(1)}, bf16[16,2048]{1,0:T(8,128)(2,1)S(1)}, u32[]{:S(2)}, u32[]{:S(2)}) collective-permute-start(bf16[16,2048]{1,0:T(8,128)(2,1)S(1)} %slice_bitcast_fusion), channel_id=1, source_target_pairs={{0,32},{32,64},{64,96},{96,128},{128,160},{160,192},{192,224},{224... | collective-permute-start | bytes 196616 | tf_op jit(solution)/shard_map/ppermute | solution.py:500
  89.3 7.8 %all-to-all-done.2.ends_ref = f32[16,2,640]{2,1,0:T(2,128)S(1)} async-done(((f32[16,2,640]{2,1,0:T(2,128)}), f32[16,2,640]{2,1,0:T(2,128)S(1)}, u32[]{:S(2)}, u32[]{:S(2)}) %all-to-all-start.2) | async-done | bytes 81952 | tf_op jit(solution)/shard_map/all_to_all | solution.py:533
  97.0 2.9 %shard_map.198 = (bf16[256,128]{1,0:T(8,128)(2,1)S(1)}, f32[2,8,4]{2,1,0:T(8,128)S(1)}) custom-call(f32[16,2,640]{2,1,0:T(2,128)S(1)} %all-to-all-done.2.ends_ref, f32[2,256,512]{2,1,0:T(8,128)S(1)} %get-tuple-element.19.bar_ref, bf16[256,128]{1,0:T(8,128)(2,1)S(1)} %get-tuple-element.22.chan_ref, f32[80,512]{1,0:T(8,128)S(1)} %get-tuple-element.20.pack_ref), custom_call_target="tpu_custom_call" | custom-call | flops 536870912 | bytes 1048576 | tf_op jit(solution)/shard_map/pallas_call | solution.py:433
  100.0 2.9 %shard_map.199 = (bf16[4,32,2048]{2,1,0:T(8,128)(2,1)S(1)}, bf16[4,32,2048]{2,1,0:T(8,128)(2,1)S(1)}) custom-call(bf16[256,128]{1,0:T(8,128)(2,1)S(1)} %get-tuple-element.23.state_ref, bf16[256,2048]{1,0:T(8,128)(2,1)S(1)} %get-tuple-element.17.normed_ref, bf16[16,2048]{1,0:T(8,128)(2,1)S(1)} %collective-permute-done.halo_ref, ...), custom_call_target="tpu_custom_call" | custom-call | flops 536870912 | bytes 1048576 | tf_op jit(solution)/shard_map/pallas_call | solution.py:433
  102.8 6.9 %collective-permute-start.8 = (bf16[4,32,2048]{2,1,0:T(8,128)(2,1)S(1)}, bf16[4,32,2048]{2,1,0:T(8,128)(2,1)S(1)}, u32[]{:S(2)}, u32[]{:S(2)}) collective-permute-start(bf16[4,32,2048]{2,1,0:T(8,128)(2,1)S(1)} %get-tuple-element.26), channel_id=1, source_target_pairs={{0,1},{1,0},{2,3},{3,2},{4,5},{5,4},{6,7},{7,6},{8,9},{9,8},{10,11... | collective-permute-start | bytes 1572872 | tf_op jit(solution)/shard_map/ppermute | solution.py:566
  109.8 1.5 %collective-permute-done.8.right_ref = bf16[4,32,2048]{2,1,0:T(8,128)(2,1)S(1)} collective-permute-done((bf16[4,32,2048]{2,1,0:T(8,128)(2,1)S(1)}, bf16[4,32,2048]{2,1,0:T(8,128)(2,1)S(1)}, u32[]{:S(2)}, u32[]{:S(2)}) %collective-permute-start.8) | collective-permute-done | bytes 524320 | tf_op jit(solution)/shard_map/ppermute | solution.py:566
  111.4 4.7 %collective-permute-start.10 = (bf16[32,2048]{1,0:T(8,128)(2,1)S(1)}, bf16[32,2048]{1,0:T(8,128)(2,1)S(1)}, u32[]{:S(2)}, u32[]{:S(2)}) collective-permute-start(bf16[32,2048]{1,0:T(8,128)(2,1)S(1)} %get-tuple-element.29), channel_id=1, source_target_pairs={{0,4},{1,5},{2,6},{3,7},{4,0},{5,1},{6,2},{7,3},{8,12},{9,13},{10,... | collective-permute-start | bytes 393224 | tf_op jit(solution)/shard_map/ppermute | solution.py:571
  116.1 2.8 %collective-permute-start.11 = (bf16[32,2048]{1,0:T(8,128)(2,1)S(1)}, bf16[32,2048]{1,0:T(8,128)(2,1)S(1)}, u32[]{:S(2)}, u32[]{:S(2)}) collective-permute-start(bf16[32,2048]{1,0:T(8,128)(2,1)S(1)} %get-tuple-element.30), channel_id=1, source_target_pairs={{0,6},{1,7},{2,0},{3,1},{4,2},{5,3},{6,4},{7,5},{8,14},{9,15},{10,... | collective-permute-start | bytes 393224 | tf_op jit(solution)/shard_map/ppermute | solution.py:571
  118.8 2.5 %collective-permute-start.9 = (bf16[32,2048]{1,0:T(8,128)(2,1)S(1)}, bf16[32,2048]{1,0:T(8,128)(2,1)S(1)}, u32[]{:S(2)}, u32[]{:S(2)}) collective-permute-start(bf16[32,2048]{1,0:T(8,128)(2,1)S(1)} %get-tuple-element.28), channel_id=1, source_target_pairs={{0,2},{1,3},{2,4},{3,5},{4,6},{5,7},{6,0},{7,1},{8,10},{9,11},{10,... | collective-permute-start | bytes 393224 | tf_op jit(solution)/shard_map/ppermute | solution.py:571
  121.4 0.7 copy.21
  122.4 3.7 %collective-permute-done.9 = bf16[32,2048]{1,0:T(8,128)(2,1)S(1)} collective-permute-done((bf16[32,2048]{1,0:T(8,128)(2,1)S(1)}, bf16[32,2048]{1,0:T(8,128)(2,1)S(1)}, u32[]{:S(2)}, u32[]{:S(2)}) %collective-permute-start.9) | collective-permute-done | bytes 131104 | tf_op jit(solution)/shard_map/ppermute | solution.py:571
  126.1 0.7 fusion
  (43 shorter events, 0.6 us)
Async XLA Ops:
  33.0 16.7 %copy-start = (bf16[16,40,128]{2,1,0:T(8,128)(2,1)}, bf16[16,40,128]{2,1,0:T(8,128)(2,1)S(1)}, u32[]{:S(2)}) copy-start(bf16[16,40,128]{2,1,0:T(8,128)(2,1)S(1)} %get-tuple-element.24) | copy-start | bytes 491524
  33.0 26.9 %collective-permute-start.1 = (bf16[16,40,128]{2,1,0:T(8,128)(2,1)S(1)}, bf16[16,40,128]{2,1,0:T(8,128)(2,1)S(1)}, u32[]{:S(2)}, u32[]{:S(2)}) collective-permute-start(bf16[16,40,128]{2,1,0:T(8,128)(2,1)S(1)} %get-tuple-element.24), channel_id=1, source_target_pairs={{0,496},{8,504},{16,480},{24,488},{32,16},{40,24},{48,0},{56,8},{6... | collective-permute-start | bytes 491528 | tf_op jit(solution)/shard_map/ppermute | solution.py:420
  44.1 15.9 %collective-permute-start.2 = (bf16[16,40,128]{2,1,0:T(8,128)(2,1)S(1)}, bf16[16,40,128]{2,1,0:T(8,128)(2,1)}, u32[]{:S(2)}, u32[]{:S(2)}) collective-permute-start(bf16[16,40,128]{2,1,0:T(8,128)(2,1)S(1)} %get-tuple-element.24), channel_id=1, source_target_pairs={{0,448},{8,456},{16,464},{24,472},{32,480},{40,488},{48,496},{56,5... | collective-permute-start | bytes 491528 | tf_op jit(solution)/shard_map/ppermute | solution.py:420
  47.7 12.3 %collective-permute-start.3 = (bf16[16,40,128]{2,1,0:T(8,128)(2,1)S(1)}, bf16[16,40,128]{2,1,0:T(8,128)(2,1)}, u32[]{:S(2)}, u32[]{:S(2)}) collective-permute-start(bf16[16,40,128]{2,1,0:T(8,128)(2,1)S(1)} %get-tuple-element.24), channel_id=1, source_target_pairs={{0,48},{8,56},{16,32},{24,40},{32,80},{40,88},{48,64},{56,72},{64,... | collective-permute-start | bytes 491528 | tf_op jit(solution)/shard_map/ppermute | solution.py:420
  49.7 3.8 %copy-start.4 = (f32[8,64,16]{1,2,0:T(8,128)S(1)}, f32[8,64,16]{1,2,0:T(8,128)}, u32[]{:S(2)}) copy-start(f32[8,64,16]{1,2,0:T(8,128)} %param.31) | copy-start | bytes 98308
  49.7 3.8 %copy-start.5 = (f32[8,64,16]{1,2,0:T(8,128)S(1)}, f32[8,64,16]{1,2,0:T(8,128)}, u32[]{:S(2)}) copy-start(f32[8,64,16]{1,2,0:T(8,128)} %param.32) | copy-start | bytes 98308
  49.7 3.8 %copy-start.6 = (f32[8,16,64]{2,1,0:T(8,128)S(1)}, f32[8,16,64]{2,1,0:T(8,128)}, u32[]{:S(2)}) copy-start(f32[8,16,64]{2,1,0:T(8,128)} %param.33) | copy-start | bytes 98308
  49.7 3.8 %copy-start.7 = (f32[8,16,64]{2,1,0:T(8,128)S(1)}, f32[8,16,64]{2,1,0:T(8,128)}, u32[]{:S(2)}) copy-start(f32[8,16,64]{2,1,0:T(8,128)} %param.34) | copy-start | bytes 98308
  49.7 3.8 %copy-start.9 = (f32[1,2,8,64]{3,2,1,0:T(8,128)S(1)}, f32[1,2,8,64]{3,2,1,0:T(8,128)}, u32[]{:S(2)}) copy-start(f32[1,2,8,64]{3,2,1,0:T(8,128)} %param.37) | copy-start | bytes 12292
  49.7 3.8 %copy-start.11 = (f32[8,64]{1,0:T(8,128)S(1)}, f32[8,64]{1,0:T(8,128)}, u32[]{:S(2)}) copy-start(f32[8,64]{1,0:T(8,128)} %freq_ref.1) | copy-start | bytes 6148
  49.7 3.8 %copy-start.12 = (f32[8,16]{1,0:T(8,128)S(1)}, f32[8,16]{1,0:T(8,128)}, u32[]{:S(2)}) copy-start(f32[8,16]{1,0:T(8,128)} %skip_ref.1) | copy-start | bytes 1540
  49.7 3.8 %copy-start.13 = (f32[3,128]{1,0:T(4,128)S(1)}, f32[3,128]{1,0:T(4,128)}, u32[]{:S(2)}) copy-start(f32[3,128]{1,0:T(4,128)} %taps_ref.1) | copy-start | bytes 4612
  49.8 3.8 %copy-start.14 = (f32[8]{0:T(128)S(1)}, f32[8]{0:T(128)}, u32[]{:S(2)}) copy-start(f32[8]{0:T(128)} %log_ref.1) | copy-start | bytes 100
  49.8 26.4 %all-to-all-start.1 = ((bf16[4,16,32,128]{3,2,1,0:T(8,128)(2,1)}), bf16[4,16,32,128]{3,2,1,0:T(8,128)(2,1)S(1)}, u32[]{:S(2)}, u32[]{:S(2)}) async-start(bf16[4,16,32,128]{3,2,1,0:T(8,128)(2,1)} %get-tuple-element.18), calls=%async_computation.1 | async-start | bytes 1048576 | tf_op jit(solution)/shard_map/all_to_all | solution.py:498
  53.4 0.7 copy-start.8
  53.4 0.7 copy-start.10
  53.4 0.7 copy-start.3
  54.1 1.2 copy-start.2
  55.3 5.3 %copy-start.1 = (bf16[16,40,128]{2,1,0:T(8,128)(2,1)S(1)}, bf16[16,40,128]{2,1,0:T(8,128)(2,1)}, u32[]{:S(2)}) copy-start(bf16[16,40,128]{2,1,0:T(8,128)(2,1)} %copy-done) | copy-start | bytes 491524
  60.0 0.7 copy-start.15
  60.7 7.7 %copy-start.16 = (bf16[16,40,128]{2,1,0:T(8,128)(2,1)S(1)}, bf16[16,40,128]{2,1,0:T(8,128)(2,1)}, u32[]{:S(2)}) copy-start(bf16[16,40,128]{2,1,0:T(8,128)(2,1)} %copy-done.15) | copy-start | bytes 491524
  61.9 38.1 %collective-permute-start.4 = (bf16[4,16,40,128]{3,2,1,0:T(8,128)(2,1)S(1)}, bf16[4,16,40,128]{3,2,1,0:T(8,128)(2,1)}, u32[]{:S(2)}, u32[]{:S(2)}) collective-permute-start(bf16[4,16,40,128]{3,2,1,0:T(8,128)(2,1)S(1)} %pad_maximum_fusion.own_ref), channel_id=1, source_target_pairs={{0,24},{8,0},{16,8},{24,16},{32,56},{40,32},{48,40},{56,48},{64,88... | collective-permute-start | bytes 1966088 | tf_op jit(solution)/shard_map/ppermute | solution.py:420
  66.4 33.5 %collective-permute-start.5 = (bf16[4,16,40,128]{3,2,1,0:T(8,128)(2,1)S(1)}, bf16[4,16,40,128]{3,2,1,0:T(8,128)(2,1)}, u32[]{:S(2)}, u32[]{:S(2)}) collective-permute-start(bf16[4,16,40,128]{3,2,1,0:T(8,128)(2,1)S(1)} %pad_maximum_fusion.own_ref), channel_id=1, source_target_pairs={{0,8},{8,16},{16,24},{24,0},{32,40},{40,48},{48,56},{56,32},{64,72... | collective-permute-start | bytes 1966088 | tf_op jit(solution)/shard_map/ppermute | solution.py:420
  69.1 30.8 %collective-permute-start.6 = (bf16[2,16,40,128]{3,2,1,0:T(8,128)(2,1)}, bf16[2,16,40,128]{3,2,1,0:T(8,128)(2,1)}, u32[]{:S(2)}, u32[]{:S(2)}) collective-permute-start(bf16[2,16,40,128]{3,2,1,0:T(8,128)(2,1)} %pad_maximum_fusion.1), channel_id=1, source_target_pairs={{0,480},{8,488},{16,496},{24,504},{32,0},{40,8},{48,16},{56,24},{6... | collective-permute-start | bytes 983048 | tf_op jit(solution)/shard_map/ppermute | solution.py:420
  74.2 25.7 %collective-permute-start.7 = (bf16[2,16,40,128]{3,2,1,0:T(8,128)(2,1)}, bf16[2,16,40,128]{3,2,1,0:T(8,128)(2,1)}, u32[]{:S(2)}, u32[]{:S(2)}) collective-permute-start(bf16[2,16,40,128]{3,2,1,0:T(8,128)(2,1)} %pad_maximum_fusion.1), channel_id=1, source_target_pairs={{0,32},{8,40},{16,48},{24,56},{32,64},{40,72},{48,80},{56,88},{64,... | collective-permute-start | bytes 983048 | tf_op jit(solution)/shard_map/ppermute | solution.py:420
  78.4 18.6 %all-to-all-start.2 = ((f32[16,2,640]{2,1,0:T(2,128)}), f32[16,2,640]{2,1,0:T(2,128)S(1)}, u32[]{:S(2)}, u32[]{:S(2)}) async-start(f32[16,2,640]{2,1,0:T(2,128)} %get-tuple-element.21), calls=%async_computation.2 | async-start | bytes 163840 | tf_op jit(solution)/shard_map/all_to_all | solution.py:533
  86.0 13.9 %collective-permute-start = (bf16[16,2048]{1,0:T(8,128)(2,1)S(1)}, bf16[16,2048]{1,0:T(8,128)(2,1)S(1)}, u32[]{:S(2)}, u32[]{:S(2)}) collective-permute-start(bf16[16,2048]{1,0:T(8,128)(2,1)S(1)} %slice_bitcast_fusion), channel_id=1, source_target_pairs={{0,32},{32,64},{64,96},{96,128},{128,160},{160,192},{192,224},{224... | collective-permute-start | bytes 196616 | tf_op jit(solution)/shard_map/ppermute | solution.py:500
  102.8 8.4 %collective-permute-start.8 = (bf16[4,32,2048]{2,1,0:T(8,128)(2,1)S(1)}, bf16[4,32,2048]{2,1,0:T(8,128)(2,1)S(1)}, u32[]{:S(2)}, u32[]{:S(2)}) collective-permute-start(bf16[4,32,2048]{2,1,0:T(8,128)(2,1)S(1)} %get-tuple-element.26), channel_id=1, source_target_pairs={{0,1},{1,0},{2,3},{3,2},{4,5},{5,4},{6,7},{7,6},{8,9},{9,8},{10,11... | collective-permute-start | bytes 1572872 | tf_op jit(solution)/shard_map/ppermute | solution.py:566
  111.4 10.6 %collective-permute-start.10 = (bf16[32,2048]{1,0:T(8,128)(2,1)S(1)}, bf16[32,2048]{1,0:T(8,128)(2,1)S(1)}, u32[]{:S(2)}, u32[]{:S(2)}) collective-permute-start(bf16[32,2048]{1,0:T(8,128)(2,1)S(1)} %get-tuple-element.29), channel_id=1, source_target_pairs={{0,4},{1,5},{2,6},{3,7},{4,0},{5,1},{6,2},{7,3},{8,12},{9,13},{10,... | collective-permute-start | bytes 393224 | tf_op jit(solution)/shard_map/ppermute | solution.py:571
  116.1 6.3 %collective-permute-start.11 = (bf16[32,2048]{1,0:T(8,128)(2,1)S(1)}, bf16[32,2048]{1,0:T(8,128)(2,1)S(1)}, u32[]{:S(2)}, u32[]{:S(2)}) collective-permute-start(bf16[32,2048]{1,0:T(8,128)(2,1)S(1)} %get-tuple-element.30), channel_id=1, source_target_pairs={{0,6},{1,7},{2,0},{3,1},{4,2},{5,3},{6,4},{7,5},{8,14},{9,15},{10,... | collective-permute-start | bytes 393224 | tf_op jit(solution)/shard_map/ppermute | solution.py:571
  118.8 7.2 %collective-permute-start.9 = (bf16[32,2048]{1,0:T(8,128)(2,1)S(1)}, bf16[32,2048]{1,0:T(8,128)(2,1)S(1)}, u32[]{:S(2)}, u32[]{:S(2)}) collective-permute-start(bf16[32,2048]{1,0:T(8,128)(2,1)S(1)} %get-tuple-element.28), channel_id=1, source_target_pairs={{0,2},{1,3},{2,4},{3,5},{4,6},{5,7},{6,0},{7,1},{8,10},{9,11},{10,... | collective-permute-start | bytes 393224 | tf_op jit(solution)/shard_map/ppermute | solution.py:571

commit v8 on v7

--- a/solution.py
+++ b/solution.py
@@ -13,6 +13,8 @@
 CHUNKS = 8
 HALO = 16
 PACKED = 16
+CLASS = ((0, 0), (2, 1), (-2, -1), (0, 2))
+NEAR = ((1, 0), (-1, 0), (0, 1), (0, -1))
 NT = (((1,), (1,)), ((), ()))
 
 
@@ -203,12 +205,11 @@
 
 def driven(chan, pack_ref, bar_ref, groups, push_ref):
     flat = bar_ref.shape[2]
+    twice = jnp.concatenate([chan, chan], axis=1)
     drives = []
     for at in range(2):
-        high, low = block_diagonal(matrix(pack_ref, at, flat // groups), groups)
-        drives.append(
-            jnp.dot(chan, high, preferred_element_type=F32) + jnp.dot(chan, low, preferred_element_type=F32)
-        )
+        both = jnp.concatenate(block_diagonal(matrix(pack_ref, at, flat // groups), groups), axis=0)
+        drives.append(jnp.dot(twice, both, preferred_element_type=F32))
     decay, freq = (packed(pack_ref, 0), packed(pack_ref, 1))
     inverse = 1.0 / (decay * decay + freq * freq)
     bar_imag = bar_ref[1]
@@ -342,29 +343,26 @@
 ):
     width = mix_ref.shape[1]
     rows = normed_ref.shape[0]
-    near, far = own_ref.shape[:2]
+    far = own_ref.shape[1]
     part = w_ref.shape[1]
     z, y = (lax.axis_index("sp"), lax.axis_index("fs"))
 
-    def put(j, turn, ref, at_j):
-        at_q = (z + j) & 3
-        at_y = (y + 2 * j + turn) & 3
-        for k in range(far):
-            at = (k * 4 + at_y) * 4 + at_q
-            for i in range(5):
-                piece = ref[at_j, k, i * part : (i + 1) * part]
-                if i < 3:
-                    w_ref[at, :, i * width : (i + 1) * width] = piece
-                else:
-                    weights_ref[at, :, (i - 3) * width : (i - 2) * width] = piece
-
-    for j in range(near):
-        put(j, 0, own_ref, j)
-        put(j, 1, up_ref, j)
-        put(j, 3, down_ref, j)
-    for j in range(near // 2):
-        put(j + 1, 2, left_ref, j)
-        put(j - 1, 2, right_ref, j)
+    def put(dz, dy, ref):
+        for j in range(ref.shape[0]):
+            at_q = (z + dz + CLASS[j][0]) & 3
+            at_y = (y + dy + CLASS[j][1]) & 3
+            for k in range(far):
+                at = (k * 4 + at_y) * 4 + at_q
+                for i in range(5):
+                    piece = ref[j, k, i * part : (i + 1) * part]
+                    if i < 3:
+                        w_ref[at, :, i * width : (i + 1) * width] = piece
+                    else:
+                        weights_ref[at, :, (i - 3) * width : (i - 2) * width] = piece
+
+    for (dz, dy), ref in zip(NEAR, (up_ref, down_ref, left_ref, right_ref)):
+        put(dz, dy, ref)
+    put(0, 0, own_ref)
     w = w_ref[...].reshape(normed_ref.shape[1], 3 * width)
     taps = [packed(pack_ref, 10 + at, width) for at in range(3)]
     gain = jnp.concatenate([packed(pack_ref, 5 + at) for at in range(4)], axis=1)
@@ -404,12 +402,8 @@
             theirs_ref[x, :, at : at + per] = product[(chips + x) * rows : (chips + x + 1) * rows]
 
 
-def add_kernel(left_ref, right_ref, *out_refs):
-    chips = len(out_refs)
-    chip = lax.axis_index("tp") >> 1
-    for k, ref in enumerate(out_refs):
-        to = (chip + k) & (chips - 1)
-        ref[...] = (left_ref[to].astype(F32) + right_ref[to].astype(F32)).astype(BF16)
+def add_kernel(left_ref, right_ref, sum_ref):
+    sum_ref[...] = (left_ref[...].astype(F32) + right_ref[...].astype(F32)).astype(BF16)
 
 
 def moved(x, dz, dy):
@@ -421,10 +415,9 @@
 
 
 def all_shards(far):
-    near = [far] + [moved(far, dz, dy) for dz, dy in ((1, 2), (2, 0), (-1, 2))]
-    own = jnp.stack(near)
+    own = jnp.stack([far] + [moved(far, dz, dy) for dz, dy in CLASS[1:]])
     half = own[:2]
-    return (own, moved(own, 0, 1), moved(own, 0, -1), moved(half, 1, 0), moved(half, -1, 0))
+    return (own, *(moved(own if dz else half, dz, dy) for dz, dy in NEAR))
 
 
 def call(kernel, out_shape, flops, *args, smem=0, anywhere=0, scratch=(), limit=20 << 20):
@@ -564,12 +557,10 @@
         ),
     )
     theirs = lax.ppermute(theirs, "tp", [(i, i ^ 1) for i in range(tp)])
-    sent = call(add_kernel, (shape((rows // tp, features), BF16),) * chips, 1 << 20, mine, theirs)
-    total = sent[0].astype(F32)
-    for k in range(1, chips):
-        pairs = [(i, (i + 2 * k) % tp) for i in range(tp)]
-        total = total + lax.ppermute(sent[k], "tp", pairs).astype(F32)
-    mixed = total.astype(BF16)
+    pair = call(add_kernel, piece, 1 << 20, mine, theirs)
+    same_core = [[i for i in range(core, tp, 2)] for core in range(2)]
+    parts = lax.all_to_all(pair, "tp", 0, 0, tiled=True, axis_index_groups=same_core)
+    mixed = jnp.sum(parts.astype(F32), axis=0).astype(BF16)
     return (mixed[None], closing[None])
 
 

time: 128 us -> 126 us (0.984)
  starting transfers between devices: 60.5 us -> 54.3 us
  waiting for transfers between devices: 13.3 us -> 17.6 us
    ppermute x3 -> x0, starting transfers between devices: 9.94 us -> none  [body(): total = total + lax.ppermute(sent[k], 'tp', pairs).astype(F32)]
    all_to_all x0 -> x1, waiting for transfers between devices: none -> 8.25 us  [body(): lax.all_to_all(pair, 'tp', 0, 0, tiled=True, axis_index_groups=same_core)]
    all_to_all x0 -> x1, starting transfers between devices: none -> 4.02 us  [body(): lax.all_to_all(pair, 'tp', 0, 0, tiled=True, axis_index_groups=same_core)]
    ppermute x3 -> x0, waiting for transfers between devices: 4.02 us -> none  [body(): total = total + lax.ppermute(sent[k], 'tp', pairs).astype(F32)]
  transfers between devices with their start and end apart: 14 -> 12, of which waited for: 4 -> 3; matrix products, arithmetic and copies ran while one was open for 3% -> 3% of each run, Pallas kernels for 8% -> 8%
where the time goes in v8:
time: 126 us; the launch traced here: 125 us
  starting transfers between devices  54.3 us (43%)
  blocking collectives  29.9 us (24%)
  waiting for transfers between devices  17.6 us (14%)
  Pallas kernels  15.8 us (13%)
  local copies, waits for them, and re-layouts  4.05 us (3%)
  other arithmetic  2.71 us (2%)
    all_to_all x1, blocking collectives, body(): far = lax.all_to_all(shards, 'sp', 0, 0, tiled=True)  29.9 us
    ppermute x7, starting transfers between devices, moved(): return lax.ppermute(x, ('sp', 'fs'), pairs)  29.5 us
    pallas_call x7, Pallas kernels, call(): pl.pallas_call(kernel, out_shape=out_shape, in_specs=first + [vmem] * (le...  15.8 us
    all_to_all x1, waiting for transfers between devices, body(): lax.all_to_all(pair, 'tp', 0, 0, tiled=True, axis_index_groups=same_core)  8.25 us
    all_to_all x1, waiting for transfers between devices, body(): ends = lax.all_to_all(end, 'sp', 0, 0, tiled=True)  7.81 us
    all_to_all x1, starting transfers between devices, body(): ends = lax.all_to_all(end, 'sp', 0, 0, tiled=True)  7.41 us
    ppermute x1, starting transfers between devices, body(): theirs = lax.ppermute(theirs, 'tp', [(i, i ^ 1) for i in range(tp)])  6.04 us
    all_to_all x1, starting transfers between devices, body(): state_weights = lax.all_to_all(many, 'fs', 0, 0, tiled=True)  4.03 us
  transfers between devices with their start and end apart: 12, of which 3 were waited for; matrix products, arithmetic and copies ran while one was open for 3% of the time, Pallas kernels for 8%

profile of v8, /device:TPU:1, one launch (start us, length us, event | category | flops | bytes accessed | tf_op | source)
XLA Modules:
  0.0 125.4 jit_solution(13206072458683312531)
XLA Ops:
  0.6 1.6 %shard_map.195 = bf16[16,72,128]{2,1,0:T(8,128)(2,1)} custom-call(bf16[32,128]{1,0:T(8,128)(2,1)} %refs_0_.1, bf16[32,128]{1,0:T(8,128)(2,1)} %refs_1_.1, bf16[32,128]{1,0:T(8,128)(2,1)} %refs_2_.1, bf16[32,128]{1,0:T(8,128)(2,1)} %refs_3_.1, bf16[32,128]{1,0:T(8,128)(2,1)} %refs_4_.1, bf16[32,128]{1,0:T(8,128)(2,1)} %refs_5_.1), custom_call_target="tpu_custom_call" | custom-call | flops 1048576 | bytes 1048576 | tf_op jit(solution)/shard_map/pallas_call | solution.py:426
  2.2 29.9 %all_to_all.20.far_ref = bf16[16,72,128]{2,1,0:T(8,128)(2,1)S(1)} all-to-all(bf16[16,72,128]{2,1,0:T(8,128)(2,1)} %shard_map.195), channel_id=1, replica_groups=mesh['sp'=16,'fs'=4,'tp'=8] {'sp'}, dimensions={0} | all-to-all | bytes 589824 | tf_op jit(solution)/shard_map/all_to_all | solution.py:483
  32.1 0.9 shard_map.196
  33.0 10.4 %collective-permute-start.1 = (bf16[16,40,128]{2,1,0:T(8,128)(2,1)S(1)}, bf16[16,40,128]{2,1,0:T(8,128)(2,1)S(1)}, u32[]{:S(2)}, u32[]{:S(2)}) collective-permute-start(bf16[16,40,128]{2,1,0:T(8,128)(2,1)S(1)} %get-tuple-element.20), channel_id=1, source_target_pairs={{0,472},{8,448},{16,456},{24,464},{32,504},{40,480},{48,488},{56,4... | collective-permute-start | bytes 491528 | tf_op jit(solution)/shard_map/ppermute | solution.py:414
  43.4 1.9 %collective-permute-start.2 = (bf16[16,40,128]{2,1,0:T(8,128)(2,1)S(1)}, bf16[16,40,128]{2,1,0:T(8,128)(2,1)}, u32[]{:S(2)}, u32[]{:S(2)}) collective-permute-start(bf16[16,40,128]{2,1,0:T(8,128)(2,1)S(1)} %get-tuple-element.20), channel_id=1, source_target_pairs={{0,72},{8,80},{16,88},{24,64},{32,104},{40,112},{48,120},{56,96},{... | collective-permute-start | bytes 491528 | tf_op jit(solution)/shard_map/ppermute | solution.py:414
  45.3 2.3 %collective-permute-start.3 = (bf16[16,40,128]{2,1,0:T(8,128)(2,1)S(1)}, bf16[16,40,128]{2,1,0:T(8,128)(2,1)}, u32[]{:S(2)}, u32[]{:S(2)}) collective-permute-start(bf16[16,40,128]{2,1,0:T(8,128)(2,1)S(1)} %get-tuple-element.20), channel_id=1, source_target_pairs={{0,16},{8,24},{16,0},{24,8},{32,48},{40,56},{48,32},{56,40},{64,80... | collective-permute-start | bytes 491528 | tf_op jit(solution)/shard_map/ppermute | solution.py:414
  47.7 4.0 %all-to-all-start.1 = ((bf16[4,16,32,128]{3,2,1,0:T(8,128)(2,1)}), bf16[4,16,32,128]{3,2,1,0:T(8,128)(2,1)S(1)}, u32[]{:S(2)}, u32[]{:S(2)}) async-start(bf16[4,16,32,128]{3,2,1,0:T(8,128)(2,1)} %get-tuple-element.14), calls=%async_computation.1 | async-start | bytes 1048576 | tf_op jit(solution)/shard_map/all_to_all | solution.py:491
  51.8 0.6 copy-done.8
  52.5 0.0 copy-done.3
  52.5 1.2 copy-done.2
  53.7 4.6 %shard_map.194 = (bf16[256,2048]{1,0:T(8,128)(2,1)S(1)}, f32[2,256,512]{2,1,0:T(8,128)S(1)}, f32[80,512]{1,0:T(8,128)S(1)}) custom-call(f32[8]{0:T(128)S(1)} %copy-done.14, bf16[256,2048]{1,0:T(8,128)(2,1)S(1)} %bitcast.21, f32[1,2048]{1,0:T(1,128)S(1)} %bitcast.26, f32[1,256]{1,0:T(1,128)S(1)} %copy-done.3, f32[8,64]{1,0:T(8,128)S(1)} %copy-done.10, ...), custom_call_target="tpu_custom_call" | custom-call | flops 1073741824 | bytes 1048576 | tf_op jit(solution)/shard_map/pallas_call | solution.py:426
  58.4 0.6 copy-done.15
  59.0 1.2 pad_maximum_fusion.own_ref
  60.2 6.6 %collective-permute-start.4 = (bf16[4,16,40,128]{3,2,1,0:T(8,128)(2,1)S(1)}, bf16[4,16,40,128]{3,2,1,0:T(8,128)(2,1)}, u32[]{:S(2)}, u32[]{:S(2)}) collective-permute-start(bf16[4,16,40,128]{3,2,1,0:T(8,128)(2,1)S(1)} %pad_maximum_fusion.own_ref), channel_id=1, source_target_pairs={{0,480},{8,488},{16,496},{24,504},{32,0},{40,8},{48,16},{56,24},{6... | collective-permute-start | bytes 1966088 | tf_op jit(solution)/shard_map/ppermute | solution.py:414
  66.8 1.9 %collective-permute-start.5 = (bf16[4,16,40,128]{3,2,1,0:T(8,128)(2,1)S(1)}, bf16[4,16,40,128]{3,2,1,0:T(8,128)(2,1)}, u32[]{:S(2)}, u32[]{:S(2)}) collective-permute-start(bf16[4,16,40,128]{3,2,1,0:T(8,128)(2,1)S(1)} %pad_maximum_fusion.own_ref), channel_id=1, source_target_pairs={{0,32},{8,40},{16,48},{24,56},{32,64},{40,72},{48,80},{56,88},{64,... | collective-permute-start | bytes 1966088 | tf_op jit(solution)/shard_map/ppermute | solution.py:414
  68.7 0.8 pad_maximum_fusion.1
  69.5 4.5 %collective-permute-start.6 = (bf16[2,16,40,128]{3,2,1,0:T(8,128)(2,1)}, bf16[2,16,40,128]{3,2,1,0:T(8,128)(2,1)}, u32[]{:S(2)}, u32[]{:S(2)}) collective-permute-start(bf16[2,16,40,128]{3,2,1,0:T(8,128)(2,1)} %pad_maximum_fusion.1), channel_id=1, source_target_pairs={{0,24},{8,0},{16,8},{24,16},{32,56},{40,32},{48,40},{56,48},{64,88... | collective-permute-start | bytes 983048 | tf_op jit(solution)/shard_map/ppermute | solution.py:414
  74.1 1.9 %collective-permute-start.7 = (bf16[2,16,40,128]{3,2,1,0:T(8,128)(2,1)}, bf16[2,16,40,128]{3,2,1,0:T(8,128)(2,1)}, u32[]{:S(2)}, u32[]{:S(2)}) collective-permute-start(bf16[2,16,40,128]{3,2,1,0:T(8,128)(2,1)} %pad_maximum_fusion.1), channel_id=1, source_target_pairs={{0,8},{8,16},{16,24},{24,0},{32,40},{40,48},{48,56},{56,32},{64,72... | collective-permute-start | bytes 983048 | tf_op jit(solution)/shard_map/ppermute | solution.py:414
  76.0 2.2 %shard_map.197 = (bf16[256,128]{1,0:T(8,128)(2,1)S(1)}, f32[16,2,640]{2,1,0:T(2,128)}) custom-call(bf16[256,2048]{1,0:T(8,128)(2,1)S(1)} %get-tuple-element.13.normed_ref, bf16[4,16,32,128]{3,2,1,0:T(8,128)(2,1)S(1)} %all-to-all-done.1.w_ref, f32[2,256,512]{2,1,0:T(8,128)S(1)} %get-tuple-element.15.bar_ref, f32[80,512]{1,0:T(8,128)S(1)} %get-tuple-element.16.pack_ref, ...), custom_call_target="tpu_custom_call" | custom-call | flops 536870912 | bytes 1048576 | tf_op jit(solution)/shard_map/pallas_call | solution.py:426
  78.1 7.4 %all-to-all-start.2 = ((f32[16,2,640]{2,1,0:T(2,128)}), f32[16,2,640]{2,1,0:T(2,128)S(1)}, u32[]{:S(2)}, u32[]{:S(2)}) async-start(f32[16,2,640]{2,1,0:T(2,128)} %get-tuple-element.17), calls=%async_computation.2 | async-start | bytes 163840 | tf_op jit(solution)/shard_map/all_to_all | solution.py:526
  85.6 0.8 slice_bitcast_fusion
  86.4 3.3 %collective-permute-start = (bf16[16,2048]{1,0:T(8,128)(2,1)S(1)}, bf16[16,2048]{1,0:T(8,128)(2,1)S(1)}, u32[]{:S(2)}, u32[]{:S(2)}) collective-permute-start(bf16[16,2048]{1,0:T(8,128)(2,1)S(1)} %slice_bitcast_fusion), channel_id=1, source_target_pairs={{0,32},{32,64},{64,96},{96,128},{128,160},{160,192},{192,224},{224... | collective-permute-start | bytes 196616 | tf_op jit(solution)/shard_map/ppermute | solution.py:493
  89.7 7.8 %all-to-all-done.2.ends_ref = f32[16,2,640]{2,1,0:T(2,128)S(1)} async-done(((f32[16,2,640]{2,1,0:T(2,128)}), f32[16,2,640]{2,1,0:T(2,128)S(1)}, u32[]{:S(2)}, u32[]{:S(2)}) %all-to-all-start.2) | async-done | bytes 81952 | tf_op jit(solution)/shard_map/all_to_all | solution.py:526
  97.5 2.8 %shard_map.198 = (bf16[256,128]{1,0:T(8,128)(2,1)S(1)}, f32[2,8,4]{2,1,0:T(8,128)S(1)}) custom-call(f32[16,2,640]{2,1,0:T(2,128)S(1)} %all-to-all-done.2.ends_ref, f32[2,256,512]{2,1,0:T(8,128)S(1)} %get-tuple-element.15.bar_ref, bf16[256,128]{1,0:T(8,128)(2,1)S(1)} %get-tuple-element.18.chan_ref, f32[80,512]{1,0:T(8,128)S(1)} %get-tuple-element.16.pack_ref), custom_call_target="tpu_custom_call" | custom-call | flops 536870912 | bytes 1048576 | tf_op jit(solution)/shard_map/pallas_call | solution.py:426
  100.3 2.8 %shard_map.199 = (bf16[4,32,2048]{2,1,0:T(8,128)(2,1)S(1)}, bf16[4,32,2048]{2,1,0:T(8,128)(2,1)S(1)}) custom-call(bf16[256,128]{1,0:T(8,128)(2,1)S(1)} %get-tuple-element.19.state_ref, bf16[256,2048]{1,0:T(8,128)(2,1)S(1)} %get-tuple-element.13.normed_ref, bf16[16,2048]{1,0:T(8,128)(2,1)S(1)} %collective-permute-done.halo_ref, ...), custom_call_target="tpu_custom_call" | custom-call | flops 536870912 | bytes 1048576 | tf_op jit(solution)/shard_map/pallas_call | solution.py:426
  103.2 6.0 %collective-permute-start.8 = (bf16[4,32,2048]{2,1,0:T(8,128)(2,1)S(1)}, bf16[4,32,2048]{2,1,0:T(8,128)(2,1)S(1)}, u32[]{:S(2)}, u32[]{:S(2)}) collective-permute-start(bf16[4,32,2048]{2,1,0:T(8,128)(2,1)S(1)} %get-tuple-element.22), channel_id=1, source_target_pairs={{0,1},{1,0},{2,3},{3,2},{4,5},{5,4},{6,7},{7,6},{8,9},{9,8},{10,11... | collective-permute-start | bytes 1572872 | tf_op jit(solution)/shard_map/ppermute | solution.py:559
  109.2 1.5 %collective-permute-done.8.right_ref = bf16[4,32,2048]{2,1,0:T(8,128)(2,1)S(1)} collective-permute-done((bf16[4,32,2048]{2,1,0:T(8,128)(2,1)S(1)}, bf16[4,32,2048]{2,1,0:T(8,128)(2,1)S(1)}, u32[]{:S(2)}, u32[]{:S(2)}) %collective-permute-start.8) | collective-permute-done | bytes 524320 | tf_op jit(solution)/shard_map/ppermute | solution.py:559
  110.8 0.9 shard_map.200
  111.7 4.0 %all-to-all-start.3 = ((bf16[4,32,2048]{2,1,0:T(8,128)(2,1)}), bf16[4,32,2048]{2,1,0:T(8,128)(2,1)S(1)}, u32[]{:S(2)}, u32[]{:S(2)}) async-start(bf16[4,32,2048]{2,1,0:T(8,128)(2,1)} %shard_map.200), calls=%async_computation.3 | async-start | bytes 1048576 | tf_op jit(solution)/shard_map/all_to_all | solution.py:562
  115.7 0.7 copy.21
  116.4 8.2 %all-to-all-done.3 = bf16[4,32,2048]{2,1,0:T(8,128)(2,1)S(1)} async-done(((bf16[4,32,2048]{2,1,0:T(8,128)(2,1)}), bf16[4,32,2048]{2,1,0:T(8,128)(2,1)S(1)}, u32[]{:S(2)}, u32[]{:S(2)}) %all-to-all-start.3) | async-done | bytes 524320 | tf_op jit(solution)/shard_map/all_to_all | solution.py:562
  124.6 0.7 reduce_sum.12
  (39 shorter events, 0.1 us)
Async XLA Ops:
  33.0 14.7 %copy-start = (bf16[16,40,128]{2,1,0:T(8,128)(2,1)}, bf16[16,40,128]{2,1,0:T(8,128)(2,1)S(1)}, u32[]{:S(2)}) copy-start(bf16[16,40,128]{2,1,0:T(8,128)(2,1)S(1)} %get-tuple-element.20) | copy-start | bytes 491524
  33.0 25.3 %collective-permute-start.1 = (bf16[16,40,128]{2,1,0:T(8,128)(2,1)S(1)}, bf16[16,40,128]{2,1,0:T(8,128)(2,1)S(1)}, u32[]{:S(2)}, u32[]{:S(2)}) collective-permute-start(bf16[16,40,128]{2,1,0:T(8,128)(2,1)S(1)} %get-tuple-element.20), channel_id=1, source_target_pairs={{0,472},{8,448},{16,456},{24,464},{32,504},{40,480},{48,488},{56,4... | collective-permute-start | bytes 491528 | tf_op jit(solution)/shard_map/ppermute | solution.py:414
  43.4 15.0 %collective-permute-start.2 = (bf16[16,40,128]{2,1,0:T(8,128)(2,1)S(1)}, bf16[16,40,128]{2,1,0:T(8,128)(2,1)}, u32[]{:S(2)}, u32[]{:S(2)}) collective-permute-start(bf16[16,40,128]{2,1,0:T(8,128)(2,1)S(1)} %get-tuple-element.20), channel_id=1, source_target_pairs={{0,72},{8,80},{16,88},{24,64},{32,104},{40,112},{48,120},{56,96},{... | collective-permute-start | bytes 491528 | tf_op jit(solution)/shard_map/ppermute | solution.py:414
  45.3 13.0 %collective-permute-start.3 = (bf16[16,40,128]{2,1,0:T(8,128)(2,1)S(1)}, bf16[16,40,128]{2,1,0:T(8,128)(2,1)}, u32[]{:S(2)}, u32[]{:S(2)}) collective-permute-start(bf16[16,40,128]{2,1,0:T(8,128)(2,1)S(1)} %get-tuple-element.20), channel_id=1, source_target_pairs={{0,16},{8,24},{16,0},{24,8},{32,48},{40,56},{48,32},{56,40},{64,80... | collective-permute-start | bytes 491528 | tf_op jit(solution)/shard_map/ppermute | solution.py:414
  47.6 4.2 %copy-start.4 = (f32[8,64,16]{1,2,0:T(8,128)S(1)}, f32[8,64,16]{1,2,0:T(8,128)}, u32[]{:S(2)}) copy-start(f32[8,64,16]{1,2,0:T(8,128)} %param.31) | copy-start | bytes 98308
  47.6 4.2 %copy-start.5 = (f32[8,64,16]{1,2,0:T(8,128)S(1)}, f32[8,64,16]{1,2,0:T(8,128)}, u32[]{:S(2)}) copy-start(f32[8,64,16]{1,2,0:T(8,128)} %param.32) | copy-start | bytes 98308
  47.6 4.2 %copy-start.6 = (f32[8,16,64]{2,1,0:T(8,128)S(1)}, f32[8,16,64]{2,1,0:T(8,128)}, u32[]{:S(2)}) copy-start(f32[8,16,64]{2,1,0:T(8,128)} %param.33) | copy-start | bytes 98308
  47.6 4.2 %copy-start.7 = (f32[8,16,64]{2,1,0:T(8,128)S(1)}, f32[8,16,64]{2,1,0:T(8,128)}, u32[]{:S(2)}) copy-start(f32[8,16,64]{2,1,0:T(8,128)} %param.34) | copy-start | bytes 98308
  47.6 4.2 %copy-start.9 = (f32[1,2,8,64]{3,2,1,0:T(8,128)S(1)}, f32[1,2,8,64]{3,2,1,0:T(8,128)}, u32[]{:S(2)}) copy-start(f32[1,2,8,64]{3,2,1,0:T(8,128)} %param.37) | copy-start | bytes 12292
  47.7 4.2 %copy-start.11 = (f32[8,64]{1,0:T(8,128)S(1)}, f32[8,64]{1,0:T(8,128)}, u32[]{:S(2)}) copy-start(f32[8,64]{1,0:T(8,128)} %freq_ref.1) | copy-start | bytes 6148
  47.7 4.2 %copy-start.12 = (f32[8,16]{1,0:T(8,128)S(1)}, f32[8,16]{1,0:T(8,128)}, u32[]{:S(2)}) copy-start(f32[8,16]{1,0:T(8,128)} %skip_ref.1) | copy-start | bytes 1540
  47.7 4.1 %copy-start.13 = (f32[3,128]{1,0:T(4,128)S(1)}, f32[3,128]{1,0:T(4,128)}, u32[]{:S(2)}) copy-start(f32[3,128]{1,0:T(4,128)} %taps_ref.1) | copy-start | bytes 4612
  47.7 4.1 %copy-start.14 = (f32[8]{0:T(128)S(1)}, f32[8]{0:T(128)}, u32[]{:S(2)}) copy-start(f32[8]{0:T(128)} %log_ref.1) | copy-start | bytes 100
  47.7 28.3 %all-to-all-start.1 = ((bf16[4,16,32,128]{3,2,1,0:T(8,128)(2,1)}), bf16[4,16,32,128]{3,2,1,0:T(8,128)(2,1)S(1)}, u32[]{:S(2)}, u32[]{:S(2)}) async-start(bf16[4,16,32,128]{3,2,1,0:T(8,128)(2,1)} %get-tuple-element.14), calls=%async_computation.1 | async-start | bytes 1048576 | tf_op jit(solution)/shard_map/all_to_all | solution.py:491
  51.7 0.7 copy-start.8
  51.7 0.7 copy-start.10
  51.8 0.7 copy-start.3
  52.5 1.2 copy-start.2
  53.7 5.3 %copy-start.1 = (bf16[16,40,128]{2,1,0:T(8,128)(2,1)S(1)}, bf16[16,40,128]{2,1,0:T(8,128)(2,1)}, u32[]{:S(2)}) copy-start(bf16[16,40,128]{2,1,0:T(8,128)(2,1)} %copy-done) | copy-start | bytes 491524
  58.3 0.7 copy-start.15
  59.0 9.7 %copy-start.16 = (bf16[16,40,128]{2,1,0:T(8,128)(2,1)S(1)}, bf16[16,40,128]{2,1,0:T(8,128)(2,1)}, u32[]{:S(2)}) copy-start(bf16[16,40,128]{2,1,0:T(8,128)(2,1)} %copy-done.15) | copy-start | bytes 491524
  60.2 40.1 %collective-permute-start.4 = (bf16[4,16,40,128]{3,2,1,0:T(8,128)(2,1)S(1)}, bf16[4,16,40,128]{3,2,1,0:T(8,128)(2,1)}, u32[]{:S(2)}, u32[]{:S(2)}) collective-permute-start(bf16[4,16,40,128]{3,2,1,0:T(8,128)(2,1)S(1)} %pad_maximum_fusion.own_ref), channel_id=1, source_target_pairs={{0,480},{8,488},{16,496},{24,504},{32,0},{40,8},{48,16},{56,24},{6... | collective-permute-start | bytes 1966088 | tf_op jit(solution)/shard_map/ppermute | solution.py:414
  66.8 33.5 %collective-permute-start.5 = (bf16[4,16,40,128]{3,2,1,0:T(8,128)(2,1)S(1)}, bf16[4,16,40,128]{3,2,1,0:T(8,128)(2,1)}, u32[]{:S(2)}, u32[]{:S(2)}) collective-permute-start(bf16[4,16,40,128]{3,2,1,0:T(8,128)(2,1)S(1)} %pad_maximum_fusion.own_ref), channel_id=1, source_target_pairs={{0,32},{8,40},{16,48},{24,56},{32,64},{40,72},{48,80},{56,88},{64,... | collective-permute-start | bytes 1966088 | tf_op jit(solution)/shard_map/ppermute | solution.py:414
  69.5 30.8 %collective-permute-start.6 = (bf16[2,16,40,128]{3,2,1,0:T(8,128)(2,1)}, bf16[2,16,40,128]{3,2,1,0:T(8,128)(2,1)}, u32[]{:S(2)}, u32[]{:S(2)}) collective-permute-start(bf16[2,16,40,128]{3,2,1,0:T(8,128)(2,1)} %pad_maximum_fusion.1), channel_id=1, source_target_pairs={{0,24},{8,0},{16,8},{24,16},{32,56},{40,32},{48,40},{56,48},{64,88... | collective-permute-start | bytes 983048 | tf_op jit(solution)/shard_map/ppermute | solution.py:414
  74.1 26.3 %collective-permute-start.7 = (bf16[2,16,40,128]{3,2,1,0:T(8,128)(2,1)}, bf16[2,16,40,128]{3,2,1,0:T(8,128)(2,1)}, u32[]{:S(2)}, u32[]{:S(2)}) collective-permute-start(bf16[2,16,40,128]{3,2,1,0:T(8,128)(2,1)} %pad_maximum_fusion.1), channel_id=1, source_target_pairs={{0,8},{8,16},{16,24},{24,0},{32,40},{40,48},{48,56},{56,32},{64,72... | collective-permute-start | bytes 983048 | tf_op jit(solution)/shard_map/ppermute | solution.py:414
  78.1 19.3 %all-to-all-start.2 = ((f32[16,2,640]{2,1,0:T(2,128)}), f32[16,2,640]{2,1,0:T(2,128)S(1)}, u32[]{:S(2)}, u32[]{:S(2)}) async-start(f32[16,2,640]{2,1,0:T(2,128)} %get-tuple-element.17), calls=%async_computation.2 | async-start | bytes 163840 | tf_op jit(solution)/shard_map/all_to_all | solution.py:526
  86.4 13.9 %collective-permute-start = (bf16[16,2048]{1,0:T(8,128)(2,1)S(1)}, bf16[16,2048]{1,0:T(8,128)(2,1)S(1)}, u32[]{:S(2)}, u32[]{:S(2)}) collective-permute-start(bf16[16,2048]{1,0:T(8,128)(2,1)S(1)} %slice_bitcast_fusion), channel_id=1, source_target_pairs={{0,32},{32,64},{64,96},{96,128},{128,160},{160,192},{192,224},{224... | collective-permute-start | bytes 196616 | tf_op jit(solution)/shard_map/ppermute | solution.py:493
  103.2 7.6 %collective-permute-start.8 = (bf16[4,32,2048]{2,1,0:T(8,128)(2,1)S(1)}, bf16[4,32,2048]{2,1,0:T(8,128)(2,1)S(1)}, u32[]{:S(2)}, u32[]{:S(2)}) collective-permute-start(bf16[4,32,2048]{2,1,0:T(8,128)(2,1)S(1)} %get-tuple-element.22), channel_id=1, source_target_pairs={{0,1},{1,0},{2,3},{3,2},{4,5},{5,4},{6,7},{7,6},{8,9},{9,8},{10,11... | collective-permute-start | bytes 1572872 | tf_op jit(solution)/shard_map/ppermute | solution.py:559
  111.7 12.9 %all-to-all-start.3 = ((bf16[4,32,2048]{2,1,0:T(8,128)(2,1)}), bf16[4,32,2048]{2,1,0:T(8,128)(2,1)S(1)}, u32[]{:S(2)}, u32[]{:S(2)}) async-start(bf16[4,32,2048]{2,1,0:T(8,128)(2,1)} %shard_map.200), calls=%async_computation.3 | async-start | bytes 1048576 | tf_op jit(solution)/shard_map/all_to_all | solution.py:562

commit v9 on v8

--- a/solution.py
+++ b/solution.py
@@ -13,6 +13,8 @@
 CHUNKS = 8
 HALO = 16
 PACKED = 16
+PRODUCTS = 2 * CHUNKS
+MATRIX = 64
 CLASS = ((0, 0), (2, 1), (-2, -1), (0, 2))
 NEAR = ((1, 0), (-1, 0), (0, 1), (0, -1))
 NT = (((1,), (1,)), ((), ()))
@@ -158,7 +160,7 @@
     (decay,) = flattened(decay_ref[...], groups)
     (freq,) = flattened(freq_ref[...], groups)
     scale = spread_steps(log_ref, groups, states)
-    top = in_real_ref.shape[0] // 2
+    top = MATRIX
     for at, ref in enumerate((in_real_ref, in_imag_ref, out_real_ref, out_imag_ref)):
         for i in range(2):
             lanes = slice((2 * at + i) * states, (2 * at + i + 1) * states)
@@ -187,18 +189,37 @@
         bar_real, bar_imag = (grow * cosine, grow * sine)
         bar_ref[0, at, :] = bar_real
         bar_ref[1, at, :] = bar_imag
-        return 0
-
-    lax.fori_loop(0, steps, advance, 0)
+        return complex_product(carry[0], carry[1], bar_real, bar_imag)
+
+    one = jnp.ones((CHUNKS, flat), F32)
+    product_real, product_imag = lax.fori_loop(0, steps, advance, (one, jnp.zeros_like(one)))
+    at = MATRIX + PACKED
+    pack_ref[at : at + CHUNKS] = product_real
+    pack_ref[at + CHUNKS : at + 2 * CHUNKS] = product_imag
 
 
 def packed(pack_ref, at, wide=None):
-    top = pack_ref.shape[0] - PACKED
+    top = MATRIX
     return pack_ref[top + at : top + at + 1, : pack_ref.shape[1] if wide is None else wide]
 
 
+def products(pack_ref):
+    at = MATRIX + PACKED
+    return (pack_ref[at : at + CHUNKS], pack_ref[at + CHUNKS : at + 2 * CHUNKS])
+
+
+def chan_blocks(pack_ref, rows):
+    at, wide = (MATRIX + PACKED + PRODUCTS, pack_ref.shape[1])
+    tall = pack_ref.shape[0] - at
+    width = wide * tall // rows
+    return [
+        (slice(i * tall, (i + 1) * tall), slice(at, at + tall), slice(i * width, (i + 1) * width))
+        for i in range(rows // tall)
+    ]
+
+
 def matrix(pack_ref, at, states):
-    top = pack_ref.shape[0] - PACKED
+    top = MATRIX
     halves = [pack_ref[:top, (2 * at + i) * states : (2 * at + i + 1) * states] for i in range(2)]
     return jnp.concatenate(halves, axis=0)
 
@@ -237,32 +258,34 @@
     lax.fori_loop(0, steps, advance, start, unroll=4)
 
 
-def chunk_maps(bar_ref, push_ref):
+def chunk_ends(bar_ref, push_ref):
     steps, flat = (bar_ref.shape[1] // CHUNKS, bar_ref.shape[2])
 
     def advance(j, carry):
         at = pl.ds(pl.multiple_of(j * CHUNKS, CHUNKS), CHUNKS)
-        bar = (bar_ref[0, at, :], bar_ref[1, at, :])
-        product = complex_product(*bar, carry[0], carry[1])
-        real, imag = complex_product(*bar, carry[2], carry[3])
-        return (*product, real + push_ref[0, at, :], imag + push_ref[1, at, :])
-
-    one, zero = (jnp.ones((CHUNKS, flat), F32), jnp.zeros((CHUNKS, flat), F32))
-    return lax.fori_loop(0, steps, advance, (one, zero, zero, zero), unroll=4)
+        real, imag = complex_product(bar_ref[0, at, :], bar_ref[1, at, :], carry[0], carry[1])
+        return (real + push_ref[0, at, :], imag + push_ref[1, at, :])
+
+    zero = jnp.zeros((CHUNKS, flat), F32)
+    return lax.fori_loop(0, steps, advance, (zero, zero), unroll=4)
 
 
 def local_kernel(
-    groups, normed_ref, w_ref, bar_ref, pack_ref, rate_ref, chan_ref, end_ref, push_ref
+    groups, normed_ref, w_ref, bar_ref, pack_ref, rate_ref, kept_ref, end_ref, push_ref
 ):
     rows = normed_ref.shape[0]
     fs, sp = w_ref.shape[:2]
     w = jnp.concatenate([w_ref[f, z] for z in range(sp) for f in range(fs)], axis=0)
     state_in = jnp.dot(normed_ref[...], w, preferred_element_type=F32).astype(BF16)
     chan = jnp.dot(chunk_order(rows, False), state_in, preferred_element_type=F32).astype(BF16)
-    chan_ref[...] = chan
+    top = MATRIX + PACKED + PRODUCTS
+    kept_ref[:top] = pack_ref[:top]
+    for rows_at, to, lanes in chan_blocks(kept_ref, rows):
+        kept_ref[to, lanes] = chan[rows_at].astype(F32)
     flat = bar_ref.shape[2]
     driven(chan, pack_ref, bar_ref, groups, push_ref)
-    end_real, end_imag, last_real, last_imag = chunk_maps(bar_ref, push_ref)
+    end_real, end_imag = products(pack_ref)
+    last_real, last_imag = chunk_ends(bar_ref, push_ref)
     real, imag = (last_real[0:1], last_imag[0:1])
     for c in range(1, CHUNKS):
         moved_real, moved_imag = complex_product(end_real[c : c + 1], end_imag[c : c + 1], real, imag)
@@ -288,7 +311,7 @@
 
 
 def read_kernel(
-    groups, ends_ref, bar_ref, chan_ref, pack_ref, mix_ref, closing_ref, push_ref
+    groups, ends_ref, bar_ref, pack_ref, mix_ref, closing_ref, push_ref
 ):
     flat = bar_ref.shape[2]
     states = flat // groups
@@ -314,9 +337,11 @@
     for at, row in enumerate((real, imag)):
         closing_ref[at] = picked(jnp.where(own, jnp.broadcast_to(row, (groups, flat)), 0.0), wanted)
     rows = bar_ref.shape[1]
-    chan = chan_ref[...]
+    wide = [pack_ref[at, lanes] for _, at, lanes in chan_blocks(pack_ref, rows)]
+    chan = jnp.concatenate(wide, axis=0).astype(BF16)
     driven(chan, pack_ref, bar_ref, groups, push_ref)
-    end_real, end_imag, last_real, last_imag = chunk_maps(bar_ref, push_ref)
+    end_real, end_imag = products(pack_ref)
+    last_real, last_imag = chunk_ends(bar_ref, push_ref)
     in_real, in_imag = ([enter_real], [enter_imag])
     for c in range(CHUNKS - 1):
         moved_real, moved_imag = complex_product(
@@ -420,7 +445,7 @@
     return (own, *(moved(own if dz else half, dz, dy) for dz, dy in NEAR))
 
 
-def call(kernel, out_shape, flops, *args, smem=0, anywhere=0, scratch=(), limit=20 << 20):
+def call(kernel, out_shape, flops, *args, smem=0, anywhere=0, aliases=None, scratch=(), limit=20 << 20):
     vmem = pl.BlockSpec(memory_space=pltpu.VMEM)
     first = [pl.BlockSpec(memory_space=pltpu.SMEM)] * smem + [pl.BlockSpec(memory_space=pl.ANY)] * anywhere
     return pl.pallas_call(
@@ -429,6 +454,7 @@
         in_specs=first + [vmem] * (len(args) - len(first)),
         out_specs=jax.tree.map(lambda _: vmem, out_shape),
         scratch_shapes=list(scratch),
+        input_output_aliases=aliases or {},
         cost_estimate=pl.CostEstimate(flops=flops, bytes_accessed=1 << 20, transcendentals=0),
         compiler_params=pltpu.CompilerParams(vmem_limit_bytes=limit),
     )(*args)
@@ -495,7 +521,7 @@
     into = [jnp.swapaxes(x, 1, 2).reshape(width, states) for x in (input_real, input_imag)]
     normed, bar, pack = call(
         prep_kernel,
-        (shape((rows, features), BF16), shape((2, rows, flat)), shape((width // 2 + PACKED, flat))),
+        (shape((rows, features), BF16), shape((2, rows, flat)), shape((MATRIX + PACKED + PRODUCTS + rows * width // flat, flat))),
         1 << 30,
         log_step,
         tokens[0],
@@ -512,15 +538,16 @@
         smem=1,
         scratch=(pltpu.VMEM((rows, 16), F32),),
     )
-    chan, end = call(
+    pack, end = call(
         functools.partial(local_kernel, groups),
-        (shape((rows, width), BF16), shape((count, 2, flat + 128))),
+        (shape(pack.shape), shape((count, 2, flat + 128))),
         1 << 29,
         normed,
         state_weights,
         bar,
         pack,
         step_rate,
+        aliases={3: 0},
         scratch=(pltpu.VMEM((2, rows, flat), F32),),
     )
     ends = lax.all_to_all(end, "sp", 0, 0, tiled=True)
@@ -530,7 +557,6 @@
         1 << 29,
         ends,
         bar,
-        chan,
         pack,
         scratch=(pltpu.VMEM((2, rows, flat), F32),),
     )

time: 126 us -> 129 us (1.024)
  local copies, waits for them, and re-layouts: 4.05 us -> 6.5 us
    unnamed x34, local copies, waits for them, and re-layouts: 2.54 us -> 4.98 us
  transfers between devices with their start and end apart: 12 -> 12, of which waited for: 3 -> 3; matrix products, arithmetic and copies ran while one was open for 3% -> 3% of each run, Pallas kernels for 8% -> 7%
where the time goes in v9:
time: 129 us; the launch traced here: 128 us
  starting transfers between devices  54.3 us (42%)
  blocking collectives  29.9 us (23%)
  waiting for transfers between devices  17.6 us (14%)
  Pallas kernels  14.8 us (11%)
  local copies, waits for them, and re-layouts  6.5 us (5%)
  other arithmetic  3.61 us (3%)
    all_to_all x1, blocking collectives, body(): far = lax.all_to_all(shards, 'sp', 0, 0, tiled=True)  29.9 us
    ppermute x7, starting transfers between devices, moved(): return lax.ppermute(x, ('sp', 'fs'), pairs)  29.5 us
    pallas_call x7, Pallas kernels, call(): pl.pallas_call(kernel, out_shape=out_shape, in_specs=first + [vmem] * (le...  14.8 us
    all_to_all x1, waiting for transfers between devices, body(): lax.all_to_all(pair, 'tp', 0, 0, tiled=True, axis_index_groups=same_core)  8.25 us
    all_to_all x1, waiting for transfers between devices, body(): ends = lax.all_to_all(end, 'sp', 0, 0, tiled=True)  7.81 us
    all_to_all x1, starting transfers between devices, body(): ends = lax.all_to_all(end, 'sp', 0, 0, tiled=True)  7.42 us
    ppermute x1, starting transfers between devices, body(): theirs = lax.ppermute(theirs, 'tp', [(i, i ^ 1) for i in range(tp)])  6.04 us
    unnamed x34, local copies, waits for them, and re-layouts  4.98 us
  transfers between devices with their start and end apart: 12, of which 3 were waited for; matrix products, arithmetic and copies ran while one was open for 3% of the time, Pallas kernels for 7%

profile of v9, /device:TPU:1, one launch (start us, length us, event | category | flops | bytes accessed | tf_op | source)
XLA Modules:
  0.0 127.7 jit_solution(3875766529053172178)
XLA Ops:
  0.6 1.6 %shard_map.195 = bf16[16,72,128]{2,1,0:T(8,128)(2,1)} custom-call(bf16[32,128]{1,0:T(8,128)(2,1)} %refs_0_.1, bf16[32,128]{1,0:T(8,128)(2,1)} %refs_1_.1, bf16[32,128]{1,0:T(8,128)(2,1)} %refs_2_.1, bf16[32,128]{1,0:T(8,128)(2,1)} %refs_3_.1, bf16[32,128]{1,0:T(8,128)(2,1)} %refs_4_.1, bf16[32,128]{1,0:T(8,128)(2,1)} %refs_5_.1), custom_call_target="tpu_custom_call" | custom-call | flops 1048576 | bytes 1048576 | tf_op jit(solution)/shard_map/pallas_call | solution.py:451
  2.2 29.9 %all_to_all.20.far_ref = bf16[16,72,128]{2,1,0:T(8,128)(2,1)S(1)} all-to-all(bf16[16,72,128]{2,1,0:T(8,128)(2,1)} %shard_map.195), channel_id=1, replica_groups=mesh['sp'=16,'fs'=4,'tp'=8] {'sp'}, dimensions={0} | all-to-all | bytes 589824 | tf_op jit(solution)/shard_map/all_to_all | solution.py:509
  32.1 0.9 shard_map.196
  33.0 10.4 %collective-permute-start.1 = (bf16[16,40,128]{2,1,0:T(8,128)(2,1)S(1)}, bf16[16,40,128]{2,1,0:T(8,128)(2,1)}, u32[]{:S(2)}, u32[]{:S(2)}) collective-permute-start(bf16[16,40,128]{2,1,0:T(8,128)(2,1)S(1)} %get-tuple-element.20), channel_id=1, source_target_pairs={{0,472},{8,448},{16,456},{24,464},{32,504},{40,480},{48,488},{56,4... | collective-permute-start | bytes 491528 | tf_op jit(solution)/shard_map/ppermute | solution.py:439
  43.4 1.9 %collective-permute-start.2 = (bf16[16,40,128]{2,1,0:T(8,128)(2,1)S(1)}, bf16[16,40,128]{2,1,0:T(8,128)(2,1)S(1)}, u32[]{:S(2)}, u32[]{:S(2)}) collective-permute-start(bf16[16,40,128]{2,1,0:T(8,128)(2,1)S(1)} %get-tuple-element.20), channel_id=1, source_target_pairs={{0,72},{8,80},{16,88},{24,64},{32,104},{40,112},{48,120},{56,96},{... | collective-permute-start | bytes 491528 | tf_op jit(solution)/shard_map/ppermute | solution.py:439
  45.3 2.3 %collective-permute-start.3 = (bf16[16,40,128]{2,1,0:T(8,128)(2,1)S(1)}, bf16[16,40,128]{2,1,0:T(8,128)(2,1)S(1)}, u32[]{:S(2)}, u32[]{:S(2)}) collective-permute-start(bf16[16,40,128]{2,1,0:T(8,128)(2,1)S(1)} %get-tuple-element.20), channel_id=1, source_target_pairs={{0,16},{8,24},{16,0},{24,8},{32,48},{40,56},{48,32},{56,40},{64,80... | collective-permute-start | bytes 491528 | tf_op jit(solution)/shard_map/ppermute | solution.py:439
  47.7 4.0 %all-to-all-start.1 = ((bf16[4,16,32,128]{3,2,1,0:T(8,128)(2,1)}), bf16[4,16,32,128]{3,2,1,0:T(8,128)(2,1)S(1)}, u32[]{:S(2)}, u32[]{:S(2)}) async-start(bf16[4,16,32,128]{3,2,1,0:T(8,128)(2,1)} %get-tuple-element.14), calls=%async_computation.1 | async-start | bytes 1048576 | tf_op jit(solution)/shard_map/all_to_all | solution.py:517
  52.4 1.2 copy-done.4
  53.7 4.8 %shard_map.194 = (bf16[256,2048]{1,0:T(8,128)(2,1)S(1)}, f32[2,256,512]{2,1,0:T(8,128)S(1)}, f32[160,512]{1,0:T(8,128)S(1)}) custom-call(f32[8]{0:T(128)S(1)} %copy-done.16, bf16[256,2048]{1,0:T(8,128)(2,1)S(1)} %bitcast.21, f32[1,2048]{1,0:T(1,128)S(1)} %bitcast.26, f32[1,256]{1,0:T(1,128)S(1)} %copy-done.5, f32[8,64]{1,0:T(8,128)S(1)} %copy-done.12, ...), custom_call_target="tpu_custom_call" | custom-call | flops 1073741824 | bytes 1048576 | tf_op jit(solution)/shard_map/pallas_call | solution.py:451
  58.5 1.2 pad_maximum_fusion.own_ref
  59.7 6.6 %collective-permute-start.4 = (bf16[4,16,40,128]{3,2,1,0:T(8,128)(2,1)S(1)}, bf16[4,16,40,128]{3,2,1,0:T(8,128)(2,1)S(1)}, u32[]{:S(2)}, u32[]{:S(2)}) collective-permute-start(bf16[4,16,40,128]{3,2,1,0:T(8,128)(2,1)S(1)} %pad_maximum_fusion.own_ref), channel_id=1, source_target_pairs={{0,480},{8,488},{16,496},{24,504},{32,0},{40,8},{48,16},{56,24},{6... | collective-permute-start | bytes 1966088 | tf_op jit(solution)/shard_map/ppermute | solution.py:439
  66.3 1.9 %collective-permute-start.5 = (bf16[4,16,40,128]{3,2,1,0:T(8,128)(2,1)S(1)}, bf16[4,16,40,128]{3,2,1,0:T(8,128)(2,1)}, u32[]{:S(2)}, u32[]{:S(2)}) collective-permute-start(bf16[4,16,40,128]{3,2,1,0:T(8,128)(2,1)S(1)} %pad_maximum_fusion.own_ref), channel_id=1, source_target_pairs={{0,32},{8,40},{16,48},{24,56},{32,64},{40,72},{48,80},{56,88},{64,... | collective-permute-start | bytes 1966088 | tf_op jit(solution)/shard_map/ppermute | solution.py:439
  68.2 1.7 %pad_maximum_fusion.1 = bf16[2,16,40,128]{3,2,1,0:T(8,128)(2,1)} fusion(bf16[1,16,40,128]{3,2,1,0:T(8,128)(2,1)} %bitcast.11, bf16[1,16,40,128]{3,2,1,0:T(8,128)(2,1)S(1)} %bitcast.20), kind=kLoop, calls=%fused_computation.1 | loop fusion | flops 163840 | bytes 655360 | tf_op jit(solution)/shard_map/stack | solution.py:443
  69.9 4.5 %collective-permute-start.6 = (bf16[2,16,40,128]{3,2,1,0:T(8,128)(2,1)}, bf16[2,16,40,128]{3,2,1,0:T(8,128)(2,1)S(1)}, u32[]{:S(2)}, u32[]{:S(2)}) collective-permute-start(bf16[2,16,40,128]{3,2,1,0:T(8,128)(2,1)} %pad_maximum_fusion.1), channel_id=1, source_target_pairs={{0,24},{8,0},{16,8},{24,16},{32,56},{40,32},{48,40},{56,48},{64,88... | collective-permute-start | bytes 983048 | tf_op jit(solution)/shard_map/ppermute | solution.py:439
  74.4 1.9 %collective-permute-start.7 = (bf16[2,16,40,128]{3,2,1,0:T(8,128)(2,1)}, bf16[2,16,40,128]{3,2,1,0:T(8,128)(2,1)}, u32[]{:S(2)}, u32[]{:S(2)}) collective-permute-start(bf16[2,16,40,128]{3,2,1,0:T(8,128)(2,1)} %pad_maximum_fusion.1), channel_id=1, source_target_pairs={{0,8},{8,16},{16,24},{24,0},{32,40},{40,48},{48,56},{56,32},{64,72... | collective-permute-start | bytes 983048 | tf_op jit(solution)/shard_map/ppermute | solution.py:439
  76.4 1.2 copy-done.1
  77.6 1.5 %shard_map.197 = (f32[160,512]{1,0:T(8,128)S(1)}, f32[16,2,640]{2,1,0:T(2,128)S(1)}) custom-call(bf16[256,2048]{1,0:T(8,128)(2,1)S(1)} %get-tuple-element.13.normed_ref, bf16[4,16,32,128]{3,2,1,0:T(8,128)(2,1)S(1)} %all-to-all-done.1.w_ref, f32[2,256,512]{2,1,0:T(8,128)S(1)} %copy-done.1, ...), custom_call_target="tpu_custom_call", output_to_operand_aliasing={{0}: (3, {})} | custom-call | flops 536870912 | bytes 1048576 | tf_op jit(solution)/shard_map/pallas_call | solution.py:451
  79.1 0.6 copy-done.3
  79.7 7.4 %all-to-all-start.2 = ((f32[16,2,640]{2,1,0:T(2,128)}), f32[16,2,640]{2,1,0:T(2,128)S(1)}, u32[]{:S(2)}, u32[]{:S(2)}) async-start(f32[16,2,640]{2,1,0:T(2,128)} %copy-done.3), calls=%async_computation.2 | async-start | bytes 163840 | tf_op jit(solution)/shard_map/all_to_all | solution.py:553
  87.1 0.8 slice_bitcast_fusion
  88.0 3.3 %collective-permute-start = (bf16[16,2048]{1,0:T(8,128)(2,1)S(1)}, bf16[16,2048]{1,0:T(8,128)(2,1)S(1)}, u32[]{:S(2)}, u32[]{:S(2)}) collective-permute-start(bf16[16,2048]{1,0:T(8,128)(2,1)S(1)} %slice_bitcast_fusion), channel_id=1, source_target_pairs={{0,32},{32,64},{64,96},{96,128},{128,160},{160,192},{192,224},{224... | collective-permute-start | bytes 196616 | tf_op jit(solution)/shard_map/ppermute | solution.py:519
  91.2 7.8 %all-to-all-done.2.ends_ref = f32[16,2,640]{2,1,0:T(2,128)S(1)} async-done(((f32[16,2,640]{2,1,0:T(2,128)}), f32[16,2,640]{2,1,0:T(2,128)S(1)}, u32[]{:S(2)}, u32[]{:S(2)}) %all-to-all-start.2) | async-done | bytes 81952 | tf_op jit(solution)/shard_map/all_to_all | solution.py:553
  99.0 1.2 copy-done.2
  100.3 2.7 %shard_map.198 = (bf16[256,128]{1,0:T(8,128)(2,1)S(1)}, f32[2,8,4]{2,1,0:T(8,128)S(1)}) custom-call(f32[16,2,640]{2,1,0:T(2,128)S(1)} %all-to-all-done.2.ends_ref, f32[2,256,512]{2,1,0:T(8,128)S(1)} %copy-done.2, f32[160,512]{1,0:T(8,128)S(1)} %get-tuple-element.18.pack_ref), custom_call_target="tpu_custom_call" | custom-call | flops 536870912 | bytes 1048576 | tf_op jit(solution)/shard_map/pallas_call | solution.py:451
  103.0 2.5 %shard_map.199 = (bf16[4,32,2048]{2,1,0:T(8,128)(2,1)S(1)}, bf16[4,32,2048]{2,1,0:T(8,128)(2,1)S(1)}) custom-call(bf16[256,128]{1,0:T(8,128)(2,1)S(1)} %get-tuple-element.19.state_ref, bf16[256,2048]{1,0:T(8,128)(2,1)S(1)} %get-tuple-element.13.normed_ref, bf16[16,2048]{1,0:T(8,128)(2,1)S(1)} %collective-permute-done.halo_ref, ...), custom_call_target="tpu_custom_call" | custom-call | flops 536870912 | bytes 1048576 | tf_op jit(solution)/shard_map/pallas_call | solution.py:451
  105.5 6.0 %collective-permute-start.8 = (bf16[4,32,2048]{2,1,0:T(8,128)(2,1)S(1)}, bf16[4,32,2048]{2,1,0:T(8,128)(2,1)S(1)}, u32[]{:S(2)}, u32[]{:S(2)}) collective-permute-start(bf16[4,32,2048]{2,1,0:T(8,128)(2,1)S(1)} %get-tuple-element.22), channel_id=1, source_target_pairs={{0,1},{1,0},{2,3},{3,2},{4,5},{5,4},{6,7},{7,6},{8,9},{9,8},{10,11... | collective-permute-start | bytes 1572872 | tf_op jit(solution)/shard_map/ppermute | solution.py:585
  111.6 1.5 %collective-permute-done.8.right_ref = bf16[4,32,2048]{2,1,0:T(8,128)(2,1)S(1)} collective-permute-done((bf16[4,32,2048]{2,1,0:T(8,128)(2,1)S(1)}, bf16[4,32,2048]{2,1,0:T(8,128)(2,1)S(1)}, u32[]{:S(2)}, u32[]{:S(2)}) %collective-permute-start.8) | collective-permute-done | bytes 524320 | tf_op jit(solution)/shard_map/ppermute | solution.py:585
  113.1 0.9 shard_map.200
  114.0 4.0 %all-to-all-start.3 = ((bf16[4,32,2048]{2,1,0:T(8,128)(2,1)}), bf16[4,32,2048]{2,1,0:T(8,128)(2,1)S(1)}, u32[]{:S(2)}, u32[]{:S(2)}) async-start(bf16[4,32,2048]{2,1,0:T(8,128)(2,1)} %shard_map.200), calls=%async_computation.3 | async-start | bytes 1048576 | tf_op jit(solution)/shard_map/all_to_all | solution.py:588
  118.0 0.7 copy.22
  118.7 8.2 %all-to-all-done.3 = bf16[4,32,2048]{2,1,0:T(8,128)(2,1)S(1)} async-done(((bf16[4,32,2048]{2,1,0:T(8,128)(2,1)}), bf16[4,32,2048]{2,1,0:T(8,128)(2,1)S(1)}, u32[]{:S(2)}, u32[]{:S(2)}) %all-to-all-start.3) | async-done | bytes 524320 | tf_op jit(solution)/shard_map/all_to_all | solution.py:588
  127.0 0.7 reduce_sum.12
  (39 shorter events, 0.7 us)
Async XLA Ops:
  33.0 25.4 %collective-permute-start.1 = (bf16[16,40,128]{2,1,0:T(8,128)(2,1)S(1)}, bf16[16,40,128]{2,1,0:T(8,128)(2,1)}, u32[]{:S(2)}, u32[]{:S(2)}) collective-permute-start(bf16[16,40,128]{2,1,0:T(8,128)(2,1)S(1)} %get-tuple-element.20), channel_id=1, source_target_pairs={{0,472},{8,448},{16,456},{24,464},{32,504},{40,480},{48,488},{56,4... | collective-permute-start | bytes 491528 | tf_op jit(solution)/shard_map/ppermute | solution.py:439
  43.4 15.1 %collective-permute-start.2 = (bf16[16,40,128]{2,1,0:T(8,128)(2,1)S(1)}, bf16[16,40,128]{2,1,0:T(8,128)(2,1)S(1)}, u32[]{:S(2)}, u32[]{:S(2)}) collective-permute-start(bf16[16,40,128]{2,1,0:T(8,128)(2,1)S(1)} %get-tuple-element.20), channel_id=1, source_target_pairs={{0,72},{8,80},{16,88},{24,64},{32,104},{40,112},{48,120},{56,96},{... | collective-permute-start | bytes 491528 | tf_op jit(solution)/shard_map/ppermute | solution.py:439
  45.3 13.1 %collective-permute-start.3 = (bf16[16,40,128]{2,1,0:T(8,128)(2,1)S(1)}, bf16[16,40,128]{2,1,0:T(8,128)(2,1)S(1)}, u32[]{:S(2)}, u32[]{:S(2)}) collective-permute-start(bf16[16,40,128]{2,1,0:T(8,128)(2,1)S(1)} %get-tuple-element.20), channel_id=1, source_target_pairs={{0,16},{8,24},{16,0},{24,8},{32,48},{40,56},{48,32},{56,40},{64,80... | collective-permute-start | bytes 491528 | tf_op jit(solution)/shard_map/ppermute | solution.py:439
  47.6 4.2 %copy-start.6 = (f32[8,64,16]{1,2,0:T(8,128)S(1)}, f32[8,64,16]{1,2,0:T(8,128)}, u32[]{:S(2)}) copy-start(f32[8,64,16]{1,2,0:T(8,128)} %param.31) | copy-start | bytes 98308
  47.6 4.2 %copy-start.7 = (f32[8,64,16]{1,2,0:T(8,128)S(1)}, f32[8,64,16]{1,2,0:T(8,128)}, u32[]{:S(2)}) copy-start(f32[8,64,16]{1,2,0:T(8,128)} %param.32) | copy-start | bytes 98308
  47.6 4.1 %copy-start.8 = (f32[8,16,64]{2,1,0:T(8,128)S(1)}, f32[8,16,64]{2,1,0:T(8,128)}, u32[]{:S(2)}) copy-start(f32[8,16,64]{2,1,0:T(8,128)} %param.33) | copy-start | bytes 98308
  47.6 4.1 %copy-start.9 = (f32[8,16,64]{2,1,0:T(8,128)S(1)}, f32[8,16,64]{2,1,0:T(8,128)}, u32[]{:S(2)}) copy-start(f32[8,16,64]{2,1,0:T(8,128)} %param.34) | copy-start | bytes 98308
  47.6 4.1 %copy-start.11 = (f32[1,2,8,64]{3,2,1,0:T(8,128)S(1)}, f32[1,2,8,64]{3,2,1,0:T(8,128)}, u32[]{:S(2)}) copy-start(f32[1,2,8,64]{3,2,1,0:T(8,128)} %param.37) | copy-start | bytes 12292
  47.6 4.1 %copy-start.13 = (f32[8,64]{1,0:T(8,128)S(1)}, f32[8,64]{1,0:T(8,128)}, u32[]{:S(2)}) copy-start(f32[8,64]{1,0:T(8,128)} %freq_ref.1) | copy-start | bytes 6148
  47.7 4.1 %copy-start.14 = (f32[8,16]{1,0:T(8,128)S(1)}, f32[8,16]{1,0:T(8,128)}, u32[]{:S(2)}) copy-start(f32[8,16]{1,0:T(8,128)} %skip_ref.1) | copy-start | bytes 1540
  47.7 4.1 %copy-start.15 = (f32[3,128]{1,0:T(4,128)S(1)}, f32[3,128]{1,0:T(4,128)}, u32[]{:S(2)}) copy-start(f32[3,128]{1,0:T(4,128)} %taps_ref.1) | copy-start | bytes 4612
  47.7 4.1 %copy-start.16 = (f32[8]{0:T(128)S(1)}, f32[8]{0:T(128)}, u32[]{:S(2)}) copy-start(f32[8]{0:T(128)} %log_ref.1) | copy-start | bytes 100
  47.7 28.7 %all-to-all-start.1 = ((bf16[4,16,32,128]{3,2,1,0:T(8,128)(2,1)}), bf16[4,16,32,128]{3,2,1,0:T(8,128)(2,1)S(1)}, u32[]{:S(2)}, u32[]{:S(2)}) async-start(bf16[4,16,32,128]{3,2,1,0:T(8,128)(2,1)} %get-tuple-element.14), calls=%async_computation.1 | async-start | bytes 1048576 | tf_op jit(solution)/shard_map/all_to_all | solution.py:517
  51.7 0.7 copy-start.10
  51.7 0.7 copy-start.12
  51.7 0.7 copy-start.5
  52.4 1.2 copy-start.4
  58.4 16.0 %copy-start = (f32[2,256,512]{2,1,0:T(8,128)}, f32[2,256,512]{2,1,0:T(8,128)S(1)}, u32[]{:S(2)}) copy-start(f32[2,256,512]{2,1,0:T(8,128)S(1)} %get-tuple-element.15.bar_ref) | copy-start | bytes 3145732
  59.7 43.3 %collective-permute-start.4 = (bf16[4,16,40,128]{3,2,1,0:T(8,128)(2,1)S(1)}, bf16[4,16,40,128]{3,2,1,0:T(8,128)(2,1)S(1)}, u32[]{:S(2)}, u32[]{:S(2)}) collective-permute-start(bf16[4,16,40,128]{3,2,1,0:T(8,128)(2,1)S(1)} %pad_maximum_fusion.own_ref), channel_id=1, source_target_pairs={{0,480},{8,488},{16,496},{24,504},{32,0},{40,8},{48,16},{56,24},{6... | collective-permute-start | bytes 1966088 | tf_op jit(solution)/shard_map/ppermute | solution.py:439
  66.3 36.7 %collective-permute-start.5 = (bf16[4,16,40,128]{3,2,1,0:T(8,128)(2,1)S(1)}, bf16[4,16,40,128]{3,2,1,0:T(8,128)(2,1)}, u32[]{:S(2)}, u32[]{:S(2)}) collective-permute-start(bf16[4,16,40,128]{3,2,1,0:T(8,128)(2,1)S(1)} %pad_maximum_fusion.own_ref), channel_id=1, source_target_pairs={{0,32},{8,40},{16,48},{24,56},{32,64},{40,72},{48,80},{56,88},{64,... | collective-permute-start | bytes 1966088 | tf_op jit(solution)/shard_map/ppermute | solution.py:439
  69.9 33.1 %collective-permute-start.6 = (bf16[2,16,40,128]{3,2,1,0:T(8,128)(2,1)}, bf16[2,16,40,128]{3,2,1,0:T(8,128)(2,1)S(1)}, u32[]{:S(2)}, u32[]{:S(2)}) collective-permute-start(bf16[2,16,40,128]{3,2,1,0:T(8,128)(2,1)} %pad_maximum_fusion.1), channel_id=1, source_target_pairs={{0,24},{8,0},{16,8},{24,16},{32,56},{40,32},{48,40},{56,48},{64,88... | collective-permute-start | bytes 983048 | tf_op jit(solution)/shard_map/ppermute | solution.py:439
  74.4 28.5 %collective-permute-start.7 = (bf16[2,16,40,128]{3,2,1,0:T(8,128)(2,1)}, bf16[2,16,40,128]{3,2,1,0:T(8,128)(2,1)}, u32[]{:S(2)}, u32[]{:S(2)}) collective-permute-start(bf16[2,16,40,128]{3,2,1,0:T(8,128)(2,1)} %pad_maximum_fusion.1), channel_id=1, source_target_pairs={{0,8},{8,16},{16,24},{24,0},{32,40},{40,48},{48,56},{56,32},{64,72... | collective-permute-start | bytes 983048 | tf_op jit(solution)/shard_map/ppermute | solution.py:439
  76.4 1.2 copy-start.1
  79.1 0.6 copy-start.3
  79.7 19.3 %all-to-all-start.2 = ((f32[16,2,640]{2,1,0:T(2,128)}), f32[16,2,640]{2,1,0:T(2,128)S(1)}, u32[]{:S(2)}, u32[]{:S(2)}) async-start(f32[16,2,640]{2,1,0:T(2,128)} %copy-done.3), calls=%async_computation.2 | async-start | bytes 163840 | tf_op jit(solution)/shard_map/all_to_all | solution.py:553
  88.0 15.0 %collective-permute-start = (bf16[16,2048]{1,0:T(8,128)(2,1)S(1)}, bf16[16,2048]{1,0:T(8,128)(2,1)S(1)}, u32[]{:S(2)}, u32[]{:S(2)}) collective-permute-start(bf16[16,2048]{1,0:T(8,128)(2,1)S(1)} %slice_bitcast_fusion), channel_id=1, source_target_pairs={{0,32},{32,64},{64,96},{96,128},{128,160},{160,192},{192,224},{224... | collective-permute-start | bytes 196616 | tf_op jit(solution)/shard_map/ppermute | solution.py:519
  99.0 1.2 copy-start.2
  105.5 7.6 %collective-permute-start.8 = (bf16[4,32,2048]{2,1,0:T(8,128)(2,1)S(1)}, bf16[4,32,2048]{2,1,0:T(8,128)(2,1)S(1)}, u32[]{:S(2)}, u32[]{:S(2)}) collective-permute-start(bf16[4,32,2048]{2,1,0:T(8,128)(2,1)S(1)} %get-tuple-element.22), channel_id=1, source_target_pairs={{0,1},{1,0},{2,3},{3,2},{4,5},{5,4},{6,7},{7,6},{8,9},{9,8},{10,11... | collective-permute-start | bytes 1572872 | tf_op jit(solution)/shard_map/ppermute | solution.py:585
  114.0 12.9 %all-to-all-start.3 = ((bf16[4,32,2048]{2,1,0:T(8,128)(2,1)}), bf16[4,32,2048]{2,1,0:T(8,128)(2,1)S(1)}, u32[]{:S(2)}, u32[]{:S(2)}) async-start(bf16[4,32,2048]{2,1,0:T(8,128)(2,1)} %shard_map.200), calls=%async_computation.3 | async-start | bytes 1048576 | tf_op jit(solution)/shard_map/all_to_all | solution.py:588

commit v10 on v9

--- a/solution.py
+++ b/solution.py
@@ -15,8 +15,8 @@
 PACKED = 16
 PRODUCTS = 2 * CHUNKS
 MATRIX = 64
-CLASS = ((0, 0), (2, 1), (-2, -1), (0, 2))
-NEAR = ((1, 0), (-1, 0), (0, 1), (0, -1))
+CLASSES = (((0, 0), (2, 1), (-2, -1), (0, 2)), ((0, 0), (1, 2), (2, 0), (-1, 2)))
+NEARS = (((1, 0), (-1, 0), (0, 1), (0, -1)), ((0, 1), (0, -1), (1, 0), (-1, 0)))
 NT = (((1,), (1,)), ((), ()))
 
 
@@ -372,10 +372,16 @@
     part = w_ref.shape[1]
     z, y = (lax.axis_index("sp"), lax.axis_index("fs"))
 
-    def put(dz, dy, ref):
+    core = lax.axis_index("tp") & 1
+
+    def by_core(choices):
+        return tuple(core * (b - a) + a for a, b in zip(*choices))
+
+    def put(near, ref):
         for j in range(ref.shape[0]):
-            at_q = (z + dz + CLASS[j][0]) & 3
-            at_y = (y + dy + CLASS[j][1]) & 3
+            far_z, far_y = by_core([offsets[j] for offsets in CLASSES])
+            at_q = (z + near[0] + far_z) & 3
+            at_y = (y + near[1] + far_y) & 3
             for k in range(far):
                 at = (k * 4 + at_y) * 4 + at_q
                 for i in range(5):
@@ -385,9 +391,9 @@
                     else:
                         weights_ref[at, :, (i - 3) * width : (i - 2) * width] = piece
 
-    for (dz, dy), ref in zip(NEAR, (up_ref, down_ref, left_ref, right_ref)):
-        put(dz, dy, ref)
-    put(0, 0, own_ref)
+    for at, ref in enumerate((up_ref, down_ref, left_ref, right_ref)):
+        put(by_core([offsets[at] for offsets in NEARS]), ref)
+    put((0, 0), own_ref)
     w = w_ref[...].reshape(normed_ref.shape[1], 3 * width)
     taps = [packed(pack_ref, 10 + at, width) for at in range(3)]
     gain = jnp.concatenate([packed(pack_ref, 5 + at) for at in range(4)], axis=1)
@@ -431,18 +437,22 @@
     sum_ref[...] = (left_ref[...].astype(F32) + right_ref[...].astype(F32)).astype(BF16)
 
 
-def moved(x, dz, dy):
-    sp, fs = (lax.axis_size("sp"), lax.axis_size("fs"))
-    pairs = [
-        (z * fs + y, ((z - dz) % sp) * fs + (y - dy) % fs) for z in range(sp) for y in range(fs)
-    ]
-    return lax.ppermute(x, ("sp", "fs"), pairs)
+def moved(x, offsets):
+    sp, fs, tp = (lax.axis_size(axis) for axis in ("sp", "fs", "tp"))
+    pairs = []
+    for z in range(sp):
+        for y in range(fs):
+            for t in range(tp):
+                dz, dy = offsets[t % 2]
+                source = ((z + dz) % sp * fs + (y + dy) % fs) * tp + t
+                pairs.append((source, (z * fs + y) * tp + t))
+    return lax.ppermute(x, ("sp", "fs", "tp"), pairs)
 
 
 def all_shards(far):
-    own = jnp.stack([far] + [moved(far, dz, dy) for dz, dy in CLASS[1:]])
+    own = jnp.stack([far] + [moved(far, offsets) for offsets in list(zip(*CLASSES))[1:]])
     half = own[:2]
-    return (own, *(moved(own if dz else half, dz, dy) for dz, dy in NEAR))
+    return (own, *(moved(own if at < 2 else half, offsets) for at, offsets in enumerate(zip(*NEARS))))
 
 
 def call(kernel, out_shape, flops, *args, smem=0, anywhere=0, aliases=None, scratch=(), limit=20 << 20):

time: 129 us -> 129 us (level)
  transfers between devices with their start and end apart: 12 -> 12, of which waited for: 3 -> 4; matrix products, arithmetic and copies ran while one was open for 3% -> 3% of each run, Pallas kernels for 7% -> 7%
where the time goes in v10:
time: 129 us; the launch traced here: 128 us
  starting transfers between devices  54 us (42%)
  blocking collectives  29.9 us (23%)
  waiting for transfers between devices  17.9 us (14%)
  Pallas kernels  14.8 us (11%)
  local copies, waits for them, and re-layouts  6.48 us (5%)
  other arithmetic  3.42 us (3%)
    all_to_all x1, blocking collectives, body(): far = lax.all_to_all(shards, 'sp', 0, 0, tiled=True)  29.9 us
    ppermute x7, starting transfers between devices, moved(): return lax.ppermute(x, ('sp', 'fs', 'tp'), pairs)  29.9 us
    pallas_call x7, Pallas kernels, call(): pl.pallas_call(kernel, out_shape=out_shape, in_specs=first + [vmem] * (le...  14.8 us
    all_to_all x1, waiting for transfers between devices, body(): lax.all_to_all(pair, 'tp', 0, 0, tiled=True, axis_index_groups=same_core)  8.25 us
    all_to_all x1, waiting for transfers between devices, body(): ends = lax.all_to_all(end, 'sp', 0, 0, tiled=True)  7.77 us
    all_to_all x1, starting transfers between devices, body(): ends = lax.all_to_all(end, 'sp', 0, 0, tiled=True)  6.69 us
    ppermute x1, starting transfers between devices, body(): theirs = lax.ppermute(theirs, 'tp', [(i, i ^ 1) for i in range(tp)])  6.5 us
    unnamed x34, local copies, waits for them, and re-layouts  4.96 us
  transfers between devices with their start and end apart: 12, of which 4 were waited for; matrix products, arithmetic and copies ran while one was open for 3% of the time, Pallas kernels for 7%

profile of v10, /device:TPU:1, one launch (start us, length us, event | category | flops | bytes accessed | tf_op | source)
XLA Modules:
  0.0 127.6 jit_solution(1284334841224806393)
XLA Ops:
  0.6 1.6 %shard_map.195 = bf16[16,72,128]{2,1,0:T(8,128)(2,1)} custom-call(bf16[32,128]{1,0:T(8,128)(2,1)} %refs_0_.1, bf16[32,128]{1,0:T(8,128)(2,1)} %refs_1_.1, bf16[32,128]{1,0:T(8,128)(2,1)} %refs_2_.1, bf16[32,128]{1,0:T(8,128)(2,1)} %refs_3_.1, bf16[32,128]{1,0:T(8,128)(2,1)} %refs_4_.1, bf16[32,128]{1,0:T(8,128)(2,1)} %refs_5_.1), custom_call_target="tpu_custom_call" | custom-call | flops 1048576 | bytes 1048576 | tf_op jit(solution)/shard_map/pallas_call | solution.py:461
  2.2 29.9 %all_to_all.20.far_ref = bf16[16,72,128]{2,1,0:T(8,128)(2,1)S(1)} all-to-all(bf16[16,72,128]{2,1,0:T(8,128)(2,1)} %shard_map.195), channel_id=1, replica_groups=mesh['sp'=16,'fs'=4,'tp'=8] {'sp'}, dimensions={0} | all-to-all | bytes 589824 | tf_op jit(solution)/shard_map/all_to_all | solution.py:519
  32.1 0.9 shard_map.196
  33.0 11.1 %collective-permute-start.1 = (bf16[16,40,128]{2,1,0:T(8,128)(2,1)S(1)}, bf16[16,40,128]{2,1,0:T(8,128)(2,1)}, u32[]{:S(2)}, u32[]{:S(2)}) collective-permute-start(bf16[16,40,128]{2,1,0:T(8,128)(2,1)S(1)} %get-tuple-element.20), channel_id=1, source_target_pairs={{72,0},{49,1},{74,2},{51,3},{76,4},{53,5},{78,6},{55,7},{80,8},{57... | collective-permute-start | bytes 491528 | tf_op jit(solution)/shard_map/ppermute | solution.py:449
  44.1 3.6 %collective-permute-start.2 = (bf16[16,40,128]{2,1,0:T(8,128)(2,1)S(1)}, bf16[16,40,128]{2,1,0:T(8,128)(2,1)S(1)}, u32[]{:S(2)}, u32[]{:S(2)}) collective-permute-start(bf16[16,40,128]{2,1,0:T(8,128)(2,1)S(1)} %get-tuple-element.20), channel_id=1, source_target_pairs={{472,0},{65,1},{474,2},{67,3},{476,4},{69,5},{478,6},{71,7},{448,8... | collective-permute-start | bytes 491528 | tf_op jit(solution)/shard_map/ppermute | solution.py:449
  47.7 1.9 %collective-permute-start.3 = (bf16[16,40,128]{2,1,0:T(8,128)(2,1)S(1)}, bf16[16,40,128]{2,1,0:T(8,128)(2,1)S(1)}, u32[]{:S(2)}, u32[]{:S(2)}) collective-permute-start(bf16[16,40,128]{2,1,0:T(8,128)(2,1)S(1)} %get-tuple-element.20), channel_id=1, source_target_pairs={{16,0},{497,1},{18,2},{499,3},{20,4},{501,5},{22,6},{503,7},{24,8}... | collective-permute-start | bytes 491528 | tf_op jit(solution)/shard_map/ppermute | solution.py:449
  49.7 3.6 %all-to-all-start.1 = ((bf16[4,16,32,128]{3,2,1,0:T(8,128)(2,1)}), bf16[4,16,32,128]{3,2,1,0:T(8,128)(2,1)S(1)}, u32[]{:S(2)}, u32[]{:S(2)}) async-start(bf16[4,16,32,128]{3,2,1,0:T(8,128)(2,1)} %get-tuple-element.14), calls=%async_computation.1 | async-start | bytes 1048576 | tf_op jit(solution)/shard_map/all_to_all | solution.py:527
  54.1 1.2 copy-done.4
  55.3 4.8 %shard_map.194 = (bf16[256,2048]{1,0:T(8,128)(2,1)S(1)}, f32[2,256,512]{2,1,0:T(8,128)S(1)}, f32[160,512]{1,0:T(8,128)S(1)}) custom-call(f32[8]{0:T(128)S(1)} %copy-done.16, bf16[256,2048]{1,0:T(8,128)(2,1)S(1)} %bitcast.21, f32[1,2048]{1,0:T(1,128)S(1)} %bitcast.26, f32[1,256]{1,0:T(1,128)S(1)} %copy-done.5, f32[8,64]{1,0:T(8,128)S(1)} %copy-done.12, ...), custom_call_target="tpu_custom_call" | custom-call | flops 1073741824 | bytes 1048576 | tf_op jit(solution)/shard_map/pallas_call | solution.py:461
  60.5 1.0 pad_maximum_fusion.own_ref
  61.5 4.4 %collective-permute-start.4 = (bf16[4,16,40,128]{3,2,1,0:T(8,128)(2,1)S(1)}, bf16[4,16,40,128]{3,2,1,0:T(8,128)(2,1)S(1)}, u32[]{:S(2)}, u32[]{:S(2)}) collective-permute-start(bf16[4,16,40,128]{3,2,1,0:T(8,128)(2,1)S(1)} %pad_maximum_fusion.own_ref), channel_id=1, source_target_pairs={{32,0},{9,1},{34,2},{11,3},{36,4},{13,5},{38,6},{15,7},{40,8},{17,... | collective-permute-start | bytes 1966088 | tf_op jit(solution)/shard_map/ppermute | solution.py:449
  65.9 1.9 %collective-permute-start.5 = (bf16[4,16,40,128]{3,2,1,0:T(8,128)(2,1)S(1)}, bf16[4,16,40,128]{3,2,1,0:T(8,128)(2,1)}, u32[]{:S(2)}, u32[]{:S(2)}) collective-permute-start(bf16[4,16,40,128]{3,2,1,0:T(8,128)(2,1)S(1)} %pad_maximum_fusion.own_ref), channel_id=1, source_target_pairs={{480,0},{25,1},{482,2},{27,3},{484,4},{29,5},{486,6},{31,7},{488,8... | collective-permute-start | bytes 1966088 | tf_op jit(solution)/shard_map/ppermute | solution.py:449
  67.8 1.7 %pad_maximum_fusion.1 = bf16[2,16,40,128]{3,2,1,0:T(8,128)(2,1)} fusion(bf16[1,16,40,128]{3,2,1,0:T(8,128)(2,1)} %bitcast.11, bf16[1,16,40,128]{3,2,1,0:T(8,128)(2,1)S(1)} %bitcast.20), kind=kLoop, calls=%fused_computation.1 | loop fusion | flops 163840 | bytes 655360 | tf_op jit(solution)/shard_map/stack | solution.py:453
  69.5 5.1 %collective-permute-start.6 = (bf16[2,16,40,128]{3,2,1,0:T(8,128)(2,1)}, bf16[2,16,40,128]{3,2,1,0:T(8,128)(2,1)S(1)}, u32[]{:S(2)}, u32[]{:S(2)}) collective-permute-start(bf16[2,16,40,128]{3,2,1,0:T(8,128)(2,1)} %pad_maximum_fusion.1), channel_id=1, source_target_pairs={{8,0},{33,1},{10,2},{35,3},{12,4},{37,5},{14,6},{39,7},{16,8},{41,... | collective-permute-start | bytes 983048 | tf_op jit(solution)/shard_map/ppermute | solution.py:449
  74.6 1.9 %collective-permute-start.7 = (bf16[2,16,40,128]{3,2,1,0:T(8,128)(2,1)}, bf16[2,16,40,128]{3,2,1,0:T(8,128)(2,1)}, u32[]{:S(2)}, u32[]{:S(2)}) collective-permute-start(bf16[2,16,40,128]{3,2,1,0:T(8,128)(2,1)} %pad_maximum_fusion.1), channel_id=1, source_target_pairs={{24,0},{481,1},{26,2},{483,3},{28,4},{485,5},{30,6},{487,7},{0,8},... | collective-permute-start | bytes 983048 | tf_op jit(solution)/shard_map/ppermute | solution.py:449
  76.5 1.2 copy-done.1
  77.7 1.5 %shard_map.197 = (f32[160,512]{1,0:T(8,128)S(1)}, f32[16,2,640]{2,1,0:T(2,128)S(1)}) custom-call(bf16[256,2048]{1,0:T(8,128)(2,1)S(1)} %get-tuple-element.13.normed_ref, bf16[4,16,32,128]{3,2,1,0:T(8,128)(2,1)S(1)} %all-to-all-done.1.w_ref, f32[2,256,512]{2,1,0:T(8,128)S(1)} %copy-done.1, ...), custom_call_target="tpu_custom_call", output_to_operand_aliasing={{0}: (3, {})} | custom-call | flops 536870912 | bytes 1048576 | tf_op jit(solution)/shard_map/pallas_call | solution.py:461
  79.2 0.6 copy-done.3
  79.8 6.7 %all-to-all-start.2 = ((f32[16,2,640]{2,1,0:T(2,128)}), f32[16,2,640]{2,1,0:T(2,128)S(1)}, u32[]{:S(2)}, u32[]{:S(2)}) async-start(f32[16,2,640]{2,1,0:T(2,128)} %copy-done.3), calls=%async_computation.2 | async-start | bytes 163840 | tf_op jit(solution)/shard_map/all_to_all | solution.py:563
  86.5 0.8 slice_bitcast_fusion
  87.4 3.3 %collective-permute-start = (bf16[16,2048]{1,0:T(8,128)(2,1)S(1)}, bf16[16,2048]{1,0:T(8,128)(2,1)S(1)}, u32[]{:S(2)}, u32[]{:S(2)}) collective-permute-start(bf16[16,2048]{1,0:T(8,128)(2,1)S(1)} %slice_bitcast_fusion), channel_id=1, source_target_pairs={{0,32},{32,64},{64,96},{96,128},{128,160},{160,192},{192,224},{224... | collective-permute-start | bytes 196616 | tf_op jit(solution)/shard_map/ppermute | solution.py:529
  90.6 7.8 %all-to-all-done.2.ends_ref = f32[16,2,640]{2,1,0:T(2,128)S(1)} async-done(((f32[16,2,640]{2,1,0:T(2,128)}), f32[16,2,640]{2,1,0:T(2,128)S(1)}, u32[]{:S(2)}, u32[]{:S(2)}) %all-to-all-start.2) | async-done | bytes 81952 | tf_op jit(solution)/shard_map/all_to_all | solution.py:563
  98.4 1.2 copy-done.2
  99.6 2.7 %shard_map.198 = (bf16[256,128]{1,0:T(8,128)(2,1)S(1)}, f32[2,8,4]{2,1,0:T(8,128)S(1)}) custom-call(f32[16,2,640]{2,1,0:T(2,128)S(1)} %all-to-all-done.2.ends_ref, f32[2,256,512]{2,1,0:T(8,128)S(1)} %copy-done.2, f32[160,512]{1,0:T(8,128)S(1)} %get-tuple-element.18.pack_ref), custom_call_target="tpu_custom_call" | custom-call | flops 536870912 | bytes 1048576 | tf_op jit(solution)/shard_map/pallas_call | solution.py:461
  102.4 2.5 %shard_map.199 = (bf16[4,32,2048]{2,1,0:T(8,128)(2,1)S(1)}, bf16[4,32,2048]{2,1,0:T(8,128)(2,1)S(1)}) custom-call(bf16[256,128]{1,0:T(8,128)(2,1)S(1)} %get-tuple-element.19.state_ref, bf16[256,2048]{1,0:T(8,128)(2,1)S(1)} %get-tuple-element.13.normed_ref, bf16[16,2048]{1,0:T(8,128)(2,1)S(1)} %collective-permute-done.halo_ref, ...), custom_call_target="tpu_custom_call" | custom-call | flops 536870912 | bytes 1048576 | tf_op jit(solution)/shard_map/pallas_call | solution.py:461
  104.9 6.5 %collective-permute-start.8 = (bf16[4,32,2048]{2,1,0:T(8,128)(2,1)S(1)}, bf16[4,32,2048]{2,1,0:T(8,128)(2,1)S(1)}, u32[]{:S(2)}, u32[]{:S(2)}) collective-permute-start(bf16[4,32,2048]{2,1,0:T(8,128)(2,1)S(1)} %get-tuple-element.22), channel_id=1, source_target_pairs={{0,1},{1,0},{2,3},{3,2},{4,5},{5,4},{6,7},{7,6},{8,9},{9,8},{10,11... | collective-permute-start | bytes 1572872 | tf_op jit(solution)/shard_map/ppermute | solution.py:595
  111.4 1.5 %collective-permute-done.8.right_ref = bf16[4,32,2048]{2,1,0:T(8,128)(2,1)S(1)} collective-permute-done((bf16[4,32,2048]{2,1,0:T(8,128)(2,1)S(1)}, bf16[4,32,2048]{2,1,0:T(8,128)(2,1)S(1)}, u32[]{:S(2)}, u32[]{:S(2)}) %collective-permute-start.8) | collective-permute-done | bytes 524320 | tf_op jit(solution)/shard_map/ppermute | solution.py:595
  112.9 0.9 shard_map.200
  113.8 4.1 %all-to-all-start.3 = ((bf16[4,32,2048]{2,1,0:T(8,128)(2,1)}), bf16[4,32,2048]{2,1,0:T(8,128)(2,1)S(1)}, u32[]{:S(2)}, u32[]{:S(2)}) async-start(bf16[4,32,2048]{2,1,0:T(8,128)(2,1)} %shard_map.200), calls=%async_computation.3 | async-start | bytes 1048576 | tf_op jit(solution)/shard_map/all_to_all | solution.py:598
  117.9 0.7 copy.22
  118.6 8.2 %all-to-all-done.3 = bf16[4,32,2048]{2,1,0:T(8,128)(2,1)S(1)} async-done(((bf16[4,32,2048]{2,1,0:T(8,128)(2,1)}), bf16[4,32,2048]{2,1,0:T(8,128)(2,1)S(1)}, u32[]{:S(2)}, u32[]{:S(2)}) %all-to-all-start.3) | async-done | bytes 524320 | tf_op jit(solution)/shard_map/all_to_all | solution.py:598
  126.8 0.7 reduce_sum.12
  (39 shorter events, 1.1 us)
Async XLA Ops:
  33.0 27.1 %collective-permute-start.1 = (bf16[16,40,128]{2,1,0:T(8,128)(2,1)S(1)}, bf16[16,40,128]{2,1,0:T(8,128)(2,1)}, u32[]{:S(2)}, u32[]{:S(2)}) collective-permute-start(bf16[16,40,128]{2,1,0:T(8,128)(2,1)S(1)} %get-tuple-element.20), channel_id=1, source_target_pairs={{72,0},{49,1},{74,2},{51,3},{76,4},{53,5},{78,6},{55,7},{80,8},{57... | collective-permute-start | bytes 491528 | tf_op jit(solution)/shard_map/ppermute | solution.py:449
  44.1 16.0 %collective-permute-start.2 = (bf16[16,40,128]{2,1,0:T(8,128)(2,1)S(1)}, bf16[16,40,128]{2,1,0:T(8,128)(2,1)S(1)}, u32[]{:S(2)}, u32[]{:S(2)}) collective-permute-start(bf16[16,40,128]{2,1,0:T(8,128)(2,1)S(1)} %get-tuple-element.20), channel_id=1, source_target_pairs={{472,0},{65,1},{474,2},{67,3},{476,4},{69,5},{478,6},{71,7},{448,8... | collective-permute-start | bytes 491528 | tf_op jit(solution)/shard_map/ppermute | solution.py:449
  47.7 12.8 %collective-permute-start.3 = (bf16[16,40,128]{2,1,0:T(8,128)(2,1)S(1)}, bf16[16,40,128]{2,1,0:T(8,128)(2,1)S(1)}, u32[]{:S(2)}, u32[]{:S(2)}) collective-permute-start(bf16[16,40,128]{2,1,0:T(8,128)(2,1)S(1)} %get-tuple-element.20), channel_id=1, source_target_pairs={{16,0},{497,1},{18,2},{499,3},{20,4},{501,5},{22,6},{503,7},{24,8}... | collective-permute-start | bytes 491528 | tf_op jit(solution)/shard_map/ppermute | solution.py:449
  49.6 3.8 %copy-start.6 = (f32[8,64,16]{1,2,0:T(8,128)S(1)}, f32[8,64,16]{1,2,0:T(8,128)}, u32[]{:S(2)}) copy-start(f32[8,64,16]{1,2,0:T(8,128)} %param.31) | copy-start | bytes 98308
  49.6 3.8 %copy-start.7 = (f32[8,64,16]{1,2,0:T(8,128)S(1)}, f32[8,64,16]{1,2,0:T(8,128)}, u32[]{:S(2)}) copy-start(f32[8,64,16]{1,2,0:T(8,128)} %param.32) | copy-start | bytes 98308
  49.7 3.8 %copy-start.8 = (f32[8,16,64]{2,1,0:T(8,128)S(1)}, f32[8,16,64]{2,1,0:T(8,128)}, u32[]{:S(2)}) copy-start(f32[8,16,64]{2,1,0:T(8,128)} %param.33) | copy-start | bytes 98308
  49.7 3.8 %copy-start.9 = (f32[8,16,64]{2,1,0:T(8,128)S(1)}, f32[8,16,64]{2,1,0:T(8,128)}, u32[]{:S(2)}) copy-start(f32[8,16,64]{2,1,0:T(8,128)} %param.34) | copy-start | bytes 98308
  49.7 3.8 %copy-start.11 = (f32[1,2,8,64]{3,2,1,0:T(8,128)S(1)}, f32[1,2,8,64]{3,2,1,0:T(8,128)}, u32[]{:S(2)}) copy-start(f32[1,2,8,64]{3,2,1,0:T(8,128)} %param.37) | copy-start | bytes 12292
  49.7 3.8 %copy-start.13 = (f32[8,64]{1,0:T(8,128)S(1)}, f32[8,64]{1,0:T(8,128)}, u32[]{:S(2)}) copy-start(f32[8,64]{1,0:T(8,128)} %freq_ref.1) | copy-start | bytes 6148
  49.7 3.8 %copy-start.14 = (f32[8,16]{1,0:T(8,128)S(1)}, f32[8,16]{1,0:T(8,128)}, u32[]{:S(2)}) copy-start(f32[8,16]{1,0:T(8,128)} %skip_ref.1) | copy-start | bytes 1540
  49.7 3.8 %copy-start.15 = (f32[3,128]{1,0:T(4,128)S(1)}, f32[3,128]{1,0:T(4,128)}, u32[]{:S(2)}) copy-start(f32[3,128]{1,0:T(4,128)} %taps_ref.1) | copy-start | bytes 4612
  49.7 3.8 %copy-start.16 = (f32[8]{0:T(128)S(1)}, f32[8]{0:T(128)}, u32[]{:S(2)}) copy-start(f32[8]{0:T(128)} %log_ref.1) | copy-start | bytes 100
  49.7 26.8 %all-to-all-start.1 = ((bf16[4,16,32,128]{3,2,1,0:T(8,128)(2,1)}), bf16[4,16,32,128]{3,2,1,0:T(8,128)(2,1)S(1)}, u32[]{:S(2)}, u32[]{:S(2)}) async-start(bf16[4,16,32,128]{3,2,1,0:T(8,128)(2,1)} %get-tuple-element.14), calls=%async_computation.1 | async-start | bytes 1048576 | tf_op jit(solution)/shard_map/all_to_all | solution.py:527
  53.4 0.7 copy-start.10
  53.4 0.7 copy-start.12
  53.4 0.7 copy-start.5
  54.1 1.2 copy-start.4
  60.1 14.5 %copy-start = (f32[2,256,512]{2,1,0:T(8,128)}, f32[2,256,512]{2,1,0:T(8,128)S(1)}, u32[]{:S(2)}) copy-start(f32[2,256,512]{2,1,0:T(8,128)S(1)} %get-tuple-element.15.bar_ref) | copy-start | bytes 3145732
  61.5 40.9 %collective-permute-start.4 = (bf16[4,16,40,128]{3,2,1,0:T(8,128)(2,1)S(1)}, bf16[4,16,40,128]{3,2,1,0:T(8,128)(2,1)S(1)}, u32[]{:S(2)}, u32[]{:S(2)}) collective-permute-start(bf16[4,16,40,128]{3,2,1,0:T(8,128)(2,1)S(1)} %pad_maximum_fusion.own_ref), channel_id=1, source_target_pairs={{32,0},{9,1},{34,2},{11,3},{36,4},{13,5},{38,6},{15,7},{40,8},{17,... | collective-permute-start | bytes 1966088 | tf_op jit(solution)/shard_map/ppermute | solution.py:449
  65.9 36.5 %collective-permute-start.5 = (bf16[4,16,40,128]{3,2,1,0:T(8,128)(2,1)S(1)}, bf16[4,16,40,128]{3,2,1,0:T(8,128)(2,1)}, u32[]{:S(2)}, u32[]{:S(2)}) collective-permute-start(bf16[4,16,40,128]{3,2,1,0:T(8,128)(2,1)S(1)} %pad_maximum_fusion.own_ref), channel_id=1, source_target_pairs={{480,0},{25,1},{482,2},{27,3},{484,4},{29,5},{486,6},{31,7},{488,8... | collective-permute-start | bytes 1966088 | tf_op jit(solution)/shard_map/ppermute | solution.py:449
  69.5 32.9 %collective-permute-start.6 = (bf16[2,16,40,128]{3,2,1,0:T(8,128)(2,1)}, bf16[2,16,40,128]{3,2,1,0:T(8,128)(2,1)S(1)}, u32[]{:S(2)}, u32[]{:S(2)}) collective-permute-start(bf16[2,16,40,128]{3,2,1,0:T(8,128)(2,1)} %pad_maximum_fusion.1), channel_id=1, source_target_pairs={{8,0},{33,1},{10,2},{35,3},{12,4},{37,5},{14,6},{39,7},{16,8},{41,... | collective-permute-start | bytes 983048 | tf_op jit(solution)/shard_map/ppermute | solution.py:449
  74.6 27.8 %collective-permute-start.7 = (bf16[2,16,40,128]{3,2,1,0:T(8,128)(2,1)}, bf16[2,16,40,128]{3,2,1,0:T(8,128)(2,1)}, u32[]{:S(2)}, u32[]{:S(2)}) collective-permute-start(bf16[2,16,40,128]{3,2,1,0:T(8,128)(2,1)} %pad_maximum_fusion.1), channel_id=1, source_target_pairs={{24,0},{481,1},{26,2},{483,3},{28,4},{485,5},{30,6},{487,7},{0,8},... | collective-permute-start | bytes 983048 | tf_op jit(solution)/shard_map/ppermute | solution.py:449
  76.5 1.2 copy-start.1
  79.2 0.6 copy-start.3
  79.8 18.6 %all-to-all-start.2 = ((f32[16,2,640]{2,1,0:T(2,128)}), f32[16,2,640]{2,1,0:T(2,128)S(1)}, u32[]{:S(2)}, u32[]{:S(2)}) async-start(f32[16,2,640]{2,1,0:T(2,128)} %copy-done.3), calls=%async_computation.2 | async-start | bytes 163840 | tf_op jit(solution)/shard_map/all_to_all | solution.py:563
  87.4 14.9 %collective-permute-start = (bf16[16,2048]{1,0:T(8,128)(2,1)S(1)}, bf16[16,2048]{1,0:T(8,128)(2,1)S(1)}, u32[]{:S(2)}, u32[]{:S(2)}) collective-permute-start(bf16[16,2048]{1,0:T(8,128)(2,1)S(1)} %slice_bitcast_fusion), channel_id=1, source_target_pairs={{0,32},{32,64},{64,96},{96,128},{128,160},{160,192},{192,224},{224... | collective-permute-start | bytes 196616 | tf_op jit(solution)/shard_map/ppermute | solution.py:529
  98.4 1.2 copy-start.2
  104.9 8.0 %collective-permute-start.8 = (bf16[4,32,2048]{2,1,0:T(8,128)(2,1)S(1)}, bf16[4,32,2048]{2,1,0:T(8,128)(2,1)S(1)}, u32[]{:S(2)}, u32[]{:S(2)}) collective-permute-start(bf16[4,32,2048]{2,1,0:T(8,128)(2,1)S(1)} %get-tuple-element.22), channel_id=1, source_target_pairs={{0,1},{1,0},{2,3},{3,2},{4,5},{5,4},{6,7},{7,6},{8,9},{9,8},{10,11... | collective-permute-start | bytes 1572872 | tf_op jit(solution)/shard_map/ppermute | solution.py:595
  113.8 13.0 %all-to-all-start.3 = ((bf16[4,32,2048]{2,1,0:T(8,128)(2,1)}), bf16[4,32,2048]{2,1,0:T(8,128)(2,1)S(1)}, u32[]{:S(2)}, u32[]{:S(2)}) async-start(bf16[4,32,2048]{2,1,0:T(8,128)(2,1)} %shard_map.200), calls=%async_computation.3 | async-start | bytes 1048576 | tf_op jit(solution)/shard_map/all_to_all | solution.py:598
